TPU v7x, 128 devices: a whole 4x4x4 slice. The times are simulated.
128 devices in a mesh: sp: 64 (over z, y, x), tp: 2 (over core).
Axes of the slice: x: 4, y: 4, z: 4, core: 2. Of those that a mesh axis runs over, the one named last changes fastest.
Arguments:
- cotangent: bfloat16 [24576, 2048], P('sp'), may hold values from -16 to 16
- routes: int32 [24576, 2], P('sp'), may hold values from 0 to 63, all different within a row; in each aligned block of 384 rows (0 to 383, 384 to 767, ...) at most 18 rows name the same one
- route_weight: float32 [24576, 2], P('sp'), may hold values from 0.1 to 0.9
- expert_rows: bfloat16 [64, 1152, 2048], P('sp'), may hold values from -6 to 6
- gate_w: bfloat16 [64, 2048, 1024], P('sp', None, 'tp'), may hold values from -0.125 to 0.125
- up_w: bfloat16 [64, 2048, 1024], P('sp', None, 'tp'), may hold values from -0.125 to 0.125
- down_w: bfloat16 [64, 1024, 2048], P('sp', 'tp'), may hold values from -0.1875 to 0.1875
- in_x: bfloat16 [24576, 1024], P('sp', 'tp'), may hold values from -6 to 6
- in_y: bfloat16 [24576, 1024], P('sp', 'tp'), may hold values from -6 to 6
- state: bfloat16 [24576, 1024], P('sp', 'tp'), may hold values from -6 to 6
- conv_taps: float32 [4, 1024], P(None, 'tp'), may hold values from -3 to 3
- gate_a: bfloat16 [8, 128, 128], P('tp'), may hold values from -0.5 to 0.5
- gate_x: bfloat16 [8, 128, 128], P('tp'), may hold values from -0.5 to 0.5
- decay_rate: float32 [1024], P('tp'), as said below
- out_weight: bfloat16 [2048, 1024], P(None, 'tp'), may hold values from -0.1875 to 0.1875
Outputs:
- grad_gate: bfloat16 [64, 2048, 1024], P('sp', None, 'tp')
- grad_up: bfloat16 [64, 2048, 1024], P('sp', None, 'tp')
- grad_down: bfloat16 [64, 1024, 2048], P('sp', 'tp')
- grad_proj: float32 [2048, 1024], P('sp', 'tp')
- grad_x: float32 [24576, 1024], P('sp', 'tp')
- grad_y: float32 [24576, 1024], P('sp', 'tp')
Inputs may be any that keep to these rules, and one draw needn't show every extreme that they name: `routes`: among the 768 pairs of one device's rows no expert appears more than 18 times, and some expert appears exactly 18 times; a row's two experts differ. `decay_rate`: positive.
All inputs are finite; a program needn't handle non-finite values.
Results may differ from a plain program's by a relative error of at most 0.0052.
The roundings to bfloat16 on the way count: a program that leaves them out, or rounds other values in their place, can miss the bound.
Values may be sent and summed in bfloat16 or wider, within the bound.
No kernel may reach another device: no remote copies, remote signals or barrier semaphores. Data moves between devices by JAX's collectives and lax.ppermute only.
A program may use at most 128 MiB of HBM per device.

v0:
```python
import jax
import jax.numpy as jnp
from jax import lax
from jax.experimental import pallas as pl
from jax.experimental.pallas import tpu as pltpu
from jax.sharding import PartitionSpec as P

rate_scale = 8.0
floor_square = 0.01
inv_root_two = 0.7071067811865476
inv_root_tau = 0.3989422804014327

f32 = jnp.float32
bf16 = jnp.bfloat16
inner = (((1,), (1,)), ((), ()))
outer = (((0,), (0,)), ((), ()))
plain = (((1,), (0,)), ((), ()))

group = 8
main = 16
extra = 2
main_rows = group * main
group_rows = group * (main + extra)
segments = 8


def dot(a, b, dims):
    return lax.dot_general(a, b, dims, preferred_element_type=f32)


def params(n=1, mb=58):
    return pltpu.CompilerParams(dimension_semantics=("arbitrary",) * n, vmem_limit_bytes=mb << 20)


def whole(shape, memory_space=None):
    return pl.BlockSpec(shape, lambda *_: (0,) * len(shape))


def pack_extras(rows, scratch):
    for j in range(8):
        scratch[pl.ds(j, group * extra, stride=8), :] = rows[:, 128 * j : 128 * (j + 1)]
    return scratch[...]


def unpack_extras(tiles, scratch):
    scratch[...] = tiles
    return jnp.concatenate(
        [scratch[pl.ds(j, group * extra, stride=8), :] for j in range(8)], axis=1
    )


def send_kernel(core_ref, routes_ref, weight_ref, cot_ref, out_ref, target_ref, slot, scratch):
    step = pl.program_id(0)
    tokens = cot_ref.shape[0]
    experts = pl.num_programs(0) * group

    @pl.when(step == 0)
    def _():
        first = routes_ref[0:1, :]
        second = routes_ref[1:2, :]
        expert = lax.broadcasted_iota(jnp.int32, (experts, tokens), 0)
        hit_first = (expert == first).astype(f32)
        hit_second = (expert == second).astype(f32)
        earlier = (
            lax.broadcasted_iota(jnp.int32, (tokens, tokens), 0)
            < lax.broadcasted_iota(jnp.int32, (tokens, tokens), 1)
        ).astype(f32)
        before = dot((hit_first + hit_second).astype(bf16), earlier.astype(bf16), plain)
        place_first = jnp.sum(before * hit_first, axis=0, keepdims=True).astype(jnp.int32)
        place_second = jnp.sum(before * hit_second, axis=0, keepdims=True).astype(jnp.int32)
        place_second = place_second + (first == second).astype(jnp.int32)
        for k, (name, place) in enumerate(((first, place_first), (second, place_second))):
            base = group_rows * (name >> 3)
            inside = name & 7
            slot[k : k + 1, :] = base + jnp.where(
                place < main, main * inside + place, main_rows + extra * inside + place - main
            )
        target_ref[...] = jnp.concatenate(
            [slot[0:2, :], jnp.zeros((6, tokens), jnp.int32)], axis=0
        )

    rows = lax.broadcasted_iota(jnp.int32, (group_rows, tokens), 0) + step * group_rows
    hit_first = rows == slot[0:1, :]
    hit_second = rows == slot[1:2, :]
    chosen = jnp.where(hit_first | hit_second, 1.0, 0.0).astype(bf16)
    weight = jnp.sum(
        jnp.where(hit_first, weight_ref[0:1, :], 0.0)
        + jnp.where(hit_second, weight_ref[1:2, :], 0.0),
        axis=1,
        keepdims=True,
    )
    values = dot(chosen, cot_ref[...], plain) * weight
    width = values.shape[1]
    out_ref[:, :, 0:width] = values[0:main_rows].astype(bf16).reshape(group, main, width)
    tiles = pack_extras(values[main_rows:], scratch)
    out_ref[:, :, width:] = tiles.astype(bf16).reshape(group, main, 128)


def send(core, routes, weight, cotangent, experts):
    tokens, model = cotangent.shape
    half = model // 2
    return pl.pallas_call(
        send_kernel,
        grid_spec=pltpu.PrefetchScalarGridSpec(
            num_scalar_prefetch=1,
            grid=(experts // group,),
            in_specs=[
                whole((2, tokens)),
                whole((2, tokens)),
                pl.BlockSpec((tokens, half), lambda i, c: (0, c[0])),
            ],
            out_specs=[
                pl.BlockSpec((group, main, half + 128), lambda i, c: (i, 0, 0)),
                whole((8, tokens)),
            ],
            scratch_shapes=[pltpu.VMEM((8, tokens), jnp.int32), pltpu.VMEM((128, 128), f32)],
        ),
        out_shape=[
            jax.ShapeDtypeStruct((experts, main, half + 128), bf16),
            jax.ShapeDtypeStruct((8, tokens), jnp.int32),
        ],
        compiler_params=params(),
        name="send",
    )(core, routes, weight, cotangent)


pair = 2


def expert_pre_kernel(rows_ref, gate_ref, up_ref, packed_ref, silu_ref, slope_ref, active_ref):
    out_row = lax.broadcasted_iota(jnp.int32, (group_rows, group_rows), 0)
    column = lax.broadcasted_iota(jnp.int32, (group_rows, group_rows), 1)
    late = out_row - main_rows
    source = jnp.where(
        out_row < main_rows,
        (main + extra) * (out_row >> 4) + (out_row & 15),
        (main + extra) * (late >> 1) + main + (late & 1),
    )
    order = jnp.where(column == source, 1.0, 0.0).astype(bf16)
    for g in range(pair):
        lo = g * group_rows
        packed_ref[lo : lo + group_rows, :] = dot(
            order, rows_ref[lo : lo + group_rows, :], plain
        ).astype(bf16)
    packed = packed_ref[...]
    pre_gate = dot(packed, gate_ref[...], plain)
    pre_up = dot(packed, up_ref[...], plain)
    gate = jax.nn.sigmoid(pre_gate)
    silu = pre_gate * gate
    silu_ref[...] = silu
    slope_ref[...] = pre_up * gate * (1.0 + pre_gate * (1.0 - gate))
    active_ref[...] = (silu * pre_up).astype(bf16)


def expert_pre(rows, gate, up):
    count, model = rows.shape
    hidden = gate.shape[1]
    size = pair * group_rows
    by_row = lambda width: pl.BlockSpec((size, width), lambda i: (i, 0))
    return pl.pallas_call(
        expert_pre_kernel,
        grid=(count // size,),
        in_specs=[by_row(model), whole((model, hidden)), whole((model, hidden))],
        out_specs=[by_row(model), by_row(hidden), by_row(hidden), by_row(hidden)],
        out_shape=[
            jax.ShapeDtypeStruct((count, model), bf16),
            jax.ShapeDtypeStruct((count, hidden), f32),
            jax.ShapeDtypeStruct((count, hidden), f32),
            jax.ShapeDtypeStruct((count, hidden), bf16),
        ],
        compiler_params=params(),
        cost_estimate=pl.CostEstimate(
            flops=4 * count * model * hidden, transcendentals=0, bytes_accessed=20 << 20
        ),
        name="expert_pre",
    )(rows, gate, up)


def recur_pre_kernel(
    x_ref, y_ref, state_ref, edge_ref, taps_ref, a_ref, i_ref, rate_ref,
    mixed_ref, grad_y_ref, gelu_ref, ahead_ref, product_ref, keep_ref, input_ref, direct_ref,
    first_ref, scratch,
):
    tokens = x_ref.shape[0]
    x = x_ref[...].astype(f32)
    edge = edge_ref[...].astype(f32)
    scratch[5:8, :] = edge[0:3]
    scratch[8 : 8 + tokens, :] = x
    conv_x = taps_ref[0:1, :] * scratch[5 : 5 + tokens, :]
    for j in range(1, 4):
        conv_x = conv_x + taps_ref[j : j + 1, :] * scratch[5 + j : 5 + j + tokens, :]
    conv_b = conv_x.astype(bf16)
    keep = jax.nn.sigmoid(dot(conv_b, a_ref[0], plain))
    gate = jax.nn.sigmoid(dot(conv_b, i_ref[0], plain))
    rate = rate_ref[...]
    decay = jnp.exp(-rate_scale * keep * rate)
    norm = jnp.sqrt(1.0 - decay * decay + floor_square)
    state = state_ref[...].astype(f32)
    scratch[7:8, :] = edge[3:4]
    scratch[8 : 8 + tokens, :] = state
    state_prev = scratch[7 : 7 + tokens, :]
    log_part = decay * state_prev - conv_x * gate * decay * decay / norm
    keep_ref[...] = log_part * (-rate_scale * rate) * keep * (1.0 - keep)
    input_ref[...] = conv_x * norm * gate * (1.0 - gate)
    direct_ref[...] = gate * norm
    y = y_ref[...].astype(f32)
    below = 0.5 * (1.0 + lax.erf(y * inv_root_two))
    gelu = y * below
    gelu_ref[...] = gelu
    mixed_ref[...] = (state * gelu).astype(bf16)
    grad_y_ref[...] = state * (below + y * jnp.exp(-0.5 * y * y) * inv_root_tau)
    scratch[0:tokens, :] = decay
    scratch[tokens : tokens + 8, :] = jnp.ones((8, decay.shape[1]), f32)
    ahead_ref[0] = scratch[1 : 1 + tokens, :]
    length = tokens // segments
    product = None
    for j in reversed(range(length)):
        step = scratch[pl.ds(j + 1, segments, stride=length), :]
        product = step if product is None else step * product
        product_ref[0, pl.ds(j, segments, stride=length), :] = product
    total = decay[0:1]
    for s in range(segments):
        total = total * product[s : s + 1]
    first_ref[...] = jnp.concatenate([decay[0:1], total, jnp.zeros_like(decay[0:6])], axis=0)


def recur_pre(in_x, in_y, state, edge, taps, gate_a, gate_x, rate):
    tokens, channels = in_x.shape
    blocks, span = gate_a.shape[:2]
    col = lambda rows: pl.BlockSpec((rows, span), lambda i: (0, i))
    block = pl.BlockSpec((1, span, span), lambda i: (i, 0, 0))
    cube = pl.BlockSpec((1, tokens, span), lambda i: (i, 0, 0))
    big = jax.ShapeDtypeStruct((tokens, channels), f32)
    return pl.pallas_call(
        recur_pre_kernel,
        grid=(blocks,),
        in_specs=[col(tokens), col(tokens), col(tokens), col(4), col(4), block, block, col(1)],
        out_specs=[col(tokens)] * 3 + [cube] * 2 + [col(tokens)] * 3 + [col(8)],
        out_shape=[jax.ShapeDtypeStruct((tokens, channels), bf16)]
        + [big] * 2
        + [jax.ShapeDtypeStruct((blocks, tokens, span), f32)] * 2
        + [big] * 3
        + [jax.ShapeDtypeStruct((8, channels), f32)],
        scratch_shapes=[pltpu.VMEM((tokens + 16, span), f32)],
        compiler_params=params(),
        cost_estimate=pl.CostEstimate(
            flops=2000 * tokens * channels, transcendentals=0, bytes_accessed=8 << 20
        ),
        name="recur_pre",
    )(in_x, in_y, state, edge, taps, gate_a, gate_x, rate)


def unpack(block, scratch):
    width = block.shape[2] - 128
    parts = []
    for g in range(block.shape[0] // group):
        own = block[g * group : (g + 1) * group]
        parts.append(own[:, :, 0:width].reshape(main_rows, width))
        tiles = own[:, :, width:].reshape(128, 128).astype(f32)
        parts.append(unpack_extras(tiles, scratch).astype(bf16))
    return jnp.concatenate(parts, axis=0)


def pack_into(out_ref, values, scratch):
    width = values.shape[1]
    for g in range(out_ref.shape[0] // group):
        lo = g * group_rows
        out_ref[g * group : (g + 1) * group, :, 0:width] = (
            values[lo : lo + main_rows].astype(bf16).reshape(group, main, width)
        )
        tiles = pack_extras(values[lo + main_rows : lo + group_rows], scratch)
        out_ref[g * group : (g + 1) * group, :, width:] = tiles.astype(bf16).reshape(
            group, main, 128
        )


def near_kernel(core_ref, block_ref, down_ref, rows_ref, part_ref, scratch):
    rows = unpack(block_ref[...], scratch)
    rows_ref[...] = rows
    part_ref[...] = dot(rows, down_ref[...], inner)


def near(core, arrived, down):
    experts, _, wide = arrived.shape
    half = wide - 128
    hidden = down.shape[0]
    count = experts * (main + extra)
    size = pair * group_rows
    return pl.pallas_call(
        near_kernel,
        grid_spec=pltpu.PrefetchScalarGridSpec(
            num_scalar_prefetch=1,
            grid=(count // size,),
            in_specs=[
                pl.BlockSpec((pair * group, main, wide), lambda i, c: (i, 0, 0)),
                pl.BlockSpec((hidden, half), lambda i, c: (0, c[0])),
            ],
            out_specs=[
                pl.BlockSpec((size, half), lambda i, c: (i, 0)),
                pl.BlockSpec((size, hidden), lambda i, c: (i, 0)),
            ],
            scratch_shapes=[pltpu.VMEM((128, 128), f32)],
        ),
        out_shape=[
            jax.ShapeDtypeStruct((count, half), bf16),
            jax.ShapeDtypeStruct((count, hidden), f32),
        ],
        compiler_params=params(),
        cost_estimate=pl.CostEstimate(
            flops=2 * count * half * hidden, transcendentals=0, bytes_accessed=9 << 20
        ),
        name="near",
    )(core, arrived, down)


def far_kernel(
    core_ref, block_ref, down_ref, part_ref, silu_ref, slope_ref, gate_ref, up_ref,
    rows_ref, gate_adj_ref, up_adj_ref, back_ref, scratch,
):
    rows = unpack(block_ref[...], scratch)
    rows_ref[...] = rows
    grad = part_ref[...] + dot(rows, down_ref[...], inner)
    gate_adj = (grad * slope_ref[...]).astype(bf16)
    up_adj = (grad * silu_ref[...]).astype(bf16)
    gate_adj_ref[...] = gate_adj
    up_adj_ref[...] = up_adj
    back = dot(gate_adj, gate_ref[...], inner) + dot(up_adj, up_ref[...], inner)
    pack_into(back_ref, back, scratch)


def far(core, arrived, down, part, silu, slope, gate, up):
    experts, _, wide = arrived.shape
    half = wide - 128
    hidden = down.shape[0]
    count = experts * (main + extra)
    size = pair * group_rows
    by_row = lambda width: pl.BlockSpec((size, width), lambda i, c: (i, 0))
    block = pl.BlockSpec((pair * group, main, wide), lambda i, c: (i, 0, 0))
    weight = pl.BlockSpec((half, hidden), lambda i, c: (1 - c[0], 0))
    return pl.pallas_call(
        far_kernel,
        grid_spec=pltpu.PrefetchScalarGridSpec(
            num_scalar_prefetch=1,
            grid=(count // size,),
            in_specs=[
                block,
                pl.BlockSpec((hidden, half), lambda i, c: (0, 1 - c[0])),
                by_row(hidden),
                by_row(hidden),
                by_row(hidden),
                weight,
                weight,
            ],
            out_specs=[by_row(half), by_row(hidden), by_row(hidden), block],
            scratch_shapes=[pltpu.VMEM((128, 128), f32)],
        ),
        out_shape=[
            jax.ShapeDtypeStruct((count, half), bf16),
            jax.ShapeDtypeStruct((count, hidden), bf16),
            jax.ShapeDtypeStruct((count, hidden), bf16),
            jax.ShapeDtypeStruct(arrived.shape, bf16),
        ],
        compiler_params=params(),
        cost_estimate=pl.CostEstimate(
            flops=6 * count * half * hidden, transcendentals=0, bytes_accessed=16 << 20
        ),
        name="far",
    )(core, arrived, down, part, silu, slope, gate, up)


def back_kernel(core_ref, gate_adj_ref, up_adj_ref, gate_ref, up_ref, back_ref, scratch):
    back = dot(gate_adj_ref[...], gate_ref[...], inner) + dot(up_adj_ref[...], up_ref[...], inner)
    pack_into(back_ref, back, scratch)


def back_own(core, gate_adj, up_adj, gate, up, shape):
    experts, _, wide = shape
    half = wide - 128
    count, hidden = gate_adj.shape
    size = pair * group_rows
    by_row = lambda width: pl.BlockSpec((size, width), lambda i, c: (i, 0))
    weight = pl.BlockSpec((half, hidden), lambda i, c: (c[0], 0))
    return pl.pallas_call(
        back_kernel,
        grid_spec=pltpu.PrefetchScalarGridSpec(
            num_scalar_prefetch=1,
            grid=(count // size,),
            in_specs=[by_row(hidden), by_row(hidden), weight, weight],
            out_specs=pl.BlockSpec((pair * group, main, wide), lambda i, c: (i, 0, 0)),
            scratch_shapes=[pltpu.VMEM((128, 128), f32)],
        ),
        out_shape=jax.ShapeDtypeStruct(shape, bf16),
        compiler_params=params(),
        cost_estimate=pl.CostEstimate(
            flops=4 * count * half * hidden, transcendentals=0, bytes_accessed=7 << 20
        ),
        name="back_own",
    )(core, gate_adj, up_adj, gate, up)


def grad_in_kernel(packed_ref, gate_adj_ref, up_adj_ref, gate_ref, up_ref):
    packed = packed_ref[...]
    gate_ref[...] = dot(packed, gate_adj_ref[...], outer).astype(bf16)
    up_ref[...] = dot(packed, up_adj_ref[...], outer).astype(bf16)


def grad_in(packed, gate_adj, up_adj):
    count, model = packed.shape
    hidden = gate_adj.shape[1]
    size = 512
    out = pl.BlockSpec((size, hidden), lambda i: (i, 0))
    return pl.pallas_call(
        grad_in_kernel,
        grid=(model // size,),
        in_specs=[
            pl.BlockSpec((count, size), lambda i: (0, i)),
            whole((count, hidden)),
            whole((count, hidden)),
        ],
        out_specs=[out, out],
        out_shape=[jax.ShapeDtypeStruct((model, hidden), bf16)] * 2,
        compiler_params=params(),
        cost_estimate=pl.CostEstimate(
            flops=4 * count * model * hidden, transcendentals=0, bytes_accessed=11 << 20
        ),
        name="grad_in",
    )(packed, gate_adj, up_adj)


def grad_down_kernel(core_ref, active_ref, near_ref, far_ref, out_ref):
    active = active_ref[...]

    @pl.when(pl.program_id(0) == 0)
    def _():
        out_ref[...] = dot(active, near_ref[...], outer).astype(bf16)

    @pl.when(pl.program_id(0) == 1)
    def _():
        out_ref[...] = dot(active, far_ref[...], outer).astype(bf16)


def grad_down_of(core, active, near_rows, far_rows):
    count, hidden = active.shape
    half = near_rows.shape[1]
    return pl.pallas_call(
        grad_down_kernel,
        grid_spec=pltpu.PrefetchScalarGridSpec(
            num_scalar_prefetch=1,
            grid=(2,),
            in_specs=[whole((count, hidden)), whole((count, half)), whole((count, half))],
            out_specs=pl.BlockSpec((hidden, half), lambda i, c: (0, i + c[0] - 2 * i * c[0])),
        ),
        out_shape=jax.ShapeDtypeStruct((hidden, 2 * half), bf16),
        compiler_params=params(),
        cost_estimate=pl.CostEstimate(
            flops=4 * count * half * hidden, transcendentals=0, bytes_accessed=9 << 20
        ),
        name="grad_down",
    )(core, active, near_rows, far_rows)


def combine_kernel(core_ref, block_ref, target_ref, cot_ref, out_ref, total, scratch):
    step = pl.program_id(0)
    tokens = cot_ref.shape[0]
    rows = unpack(block_ref[...], scratch)
    size = rows.shape[0]
    place = lax.broadcasted_iota(jnp.int32, (tokens, size), 1) + step * size
    chosen = jnp.where(
        (place == target_ref[:, 0:1]) | (place == target_ref[:, 1:2]), 1.0, 0.0
    ).astype(bf16)
    found = dot(chosen, rows, plain)

    @pl.when(step == 0)
    def _():
        total[...] = found

    @pl.when(step > 0)
    def _():
        total[...] = total[...] + found

    @pl.when(step == pl.num_programs(0) - 1)
    def _():
        out_ref[...] = (cot_ref[...].astype(f32) + total[...]).astype(bf16)


def combine(core, returned, target, cotangent):
    experts, _, wide = returned.shape
    half = wide - 128
    tokens = cotangent.shape[0]
    return pl.pallas_call(
        combine_kernel,
        grid_spec=pltpu.PrefetchScalarGridSpec(
            num_scalar_prefetch=1,
            grid=(experts // (pair * group),),
            in_specs=[
                pl.BlockSpec((pair * group, main, wide), lambda i, c: (i, 0, 0)),
                whole((tokens, 8)),
                pl.BlockSpec((tokens, half), lambda i, c: (0, c[0])),
            ],
            out_specs=whole((tokens, half)),
            scratch_shapes=[pltpu.VMEM((tokens, half), f32), pltpu.VMEM((128, 128), f32)],
        ),
        out_shape=jax.ShapeDtypeStruct((tokens, half), bf16),
        compiler_params=params(),
        name="combine",
    )(core, returned, target, cotangent)


def scan_kernel(
    core_ref, own_ref, peer_ref, weight_ref, slope_ref, gelu_ref, ahead_ref, product_ref, first_ref,
    grad_y_ref, local_ref, total_ref, scratch,
):
    tokens, half = own_ref.shape
    core = core_ref[0]
    near_weight = weight_ref[pl.ds(pl.multiple_of(core * half, half), half), :]
    far_weight = weight_ref[pl.ds(pl.multiple_of((1 - core) * half, half), half), :]
    grad = dot(own_ref[...], near_weight, plain) + dot(peer_ref[...], far_weight, plain)
    grad_y_ref[...] = grad * slope_ref[...]
    state_grad = grad * gelu_ref[...]
    length = tokens // segments
    for b in range(scratch.shape[0]):
        at = slice(128 * b, 128 * (b + 1))
        scratch[b] = state_grad[:, at]
    for b in range(scratch.shape[0]):
        at = slice(128 * b, 128 * (b + 1))
        value = None
        for j in reversed(range(length)):
            here = scratch[b, pl.ds(j, segments, stride=length), :]
            if value is None:
                value = here
            else:
                value = here + ahead_ref[b, pl.ds(j, segments, stride=length), :] * value
            local_ref[b, pl.ds(j, segments, stride=length), :] = value
        product = product_ref[b, pl.ds(0, segments, stride=length), :]
        carry = value[segments - 1 : segments]
        for s in reversed(range(segments - 1)):
            carry = value[s : s + 1] + product[s : s + 1] * carry
        total_ref[:, at] = first_ref[0:1, at] * carry


def scan(core, own, peer, weight, slope, gelu, ahead, product, first):
    tokens, half = own.shape
    channels = weight.shape[1]
    return pl.pallas_call(
        scan_kernel,
        grid_spec=pltpu.PrefetchScalarGridSpec(
            num_scalar_prefetch=1,
            grid=(1,),
            in_specs=[
                whole((tokens, half)),
                whole((tokens, half)),
                whole(weight.shape),
                whole((tokens, channels)),
                whole((tokens, channels)),
                whole(ahead.shape),
                whole(ahead.shape),
                whole((8, channels)),
            ],
            out_specs=[whole((tokens, channels)), whole(ahead.shape), whole((1, channels))],
            scratch_shapes=[pltpu.VMEM(ahead.shape, f32)],
        ),
        out_shape=[
            jax.ShapeDtypeStruct((tokens, channels), f32),
            jax.ShapeDtypeStruct(ahead.shape, f32),
            jax.ShapeDtypeStruct((1, channels), f32),
        ],
        compiler_params=params(),
        name="scan",
    )(core, own, peer, weight, slope, gelu, ahead, product, first)


def project_kernel(core_ref, own_ref, peer_ref, mixed_ref, out_ref):
    half = own_ref.shape[1]
    core = core_ref[0]
    mixed = mixed_ref[...]
    near_rows = dot(own_ref[...], mixed, outer).astype(bf16)
    far_rows = dot(peer_ref[...], mixed, outer).astype(bf16)
    out_ref[pl.ds(pl.multiple_of(core * half, half), half), :] = near_rows
    out_ref[pl.ds(pl.multiple_of((1 - core) * half, half), half), :] = far_rows


def project(core, own, peer, mixed):
    tokens, half = own.shape
    channels = mixed.shape[1]
    return pl.pallas_call(
        project_kernel,
        grid_spec=pltpu.PrefetchScalarGridSpec(
            num_scalar_prefetch=1,
            grid=(1,),
            in_specs=[whole((tokens, half)), whole((tokens, half)), whole((tokens, channels))],
            out_specs=whole((2 * half, channels)),
        ),
        out_shape=jax.ShapeDtypeStruct((2 * half, channels), bf16),
        compiler_params=params(),
        name="project",
    )(core, own, peer, mixed)


def adjoint_kernel(
    carry_ref, local_ref, product_ref, keep_ref, input_ref, direct_ref, a_ref, i_ref,
    out_ref, scratch,
):
    tokens = local_ref.shape[1]
    length = tokens // segments
    carry = carry_ref[...]
    for s in reversed(range(segments)):
        lo = s * length
        piece = local_ref[0, lo : lo + length, :] + product_ref[0, lo : lo + length, :] * carry
        scratch[lo : lo + length, :] = piece
        carry = piece[0:1]
    adjoint = scratch[...]
    keep = (adjoint * keep_ref[...]).astype(bf16)
    gate = (adjoint * input_ref[...]).astype(bf16)
    out_ref[...] = adjoint * direct_ref[...] + dot(keep, a_ref[0], inner) + dot(gate, i_ref[0], inner)


def conv_grad_of(carry, local, product, keep, gate, direct, gate_a, gate_x):
    tokens = local.shape[1]
    blocks, span = gate_a.shape[:2]
    channels = blocks * span
    cube = pl.BlockSpec((1, tokens, span), lambda i: (i, 0, 0))
    col = lambda rows: pl.BlockSpec((rows, span), lambda i: (0, i))
    block = pl.BlockSpec((1, span, span), lambda i: (i, 0, 0))
    return pl.pallas_call(
        adjoint_kernel,
        grid=(blocks,),
        in_specs=[col(1), cube, cube] + [col(tokens)] * 3 + [block, block],
        out_specs=col(tokens),
        out_shape=jax.ShapeDtypeStruct((tokens, channels), f32),
        scratch_shapes=[pltpu.VMEM((tokens, span), f32)],
        compiler_params=params(),
        name="adjoint",
    )(carry, local, product, keep, gate, direct, gate_a, gate_x)


def grad_x_kernel(grad_ref, later_ref, taps_ref, out_ref, scratch):
    tokens = grad_ref.shape[0]
    scratch[0:tokens, :] = grad_ref[...]
    scratch[tokens : tokens + 3, :] = later_ref[...]
    total = taps_ref[0:1, :] * scratch[3 : 3 + tokens, :]
    for j in range(1, 4):
        total = total + taps_ref[j : j + 1, :] * scratch[3 - j : 3 - j + tokens, :]
    out_ref[...] = total


def grad_x_of(grad, later, taps):
    tokens, channels = grad.shape
    col = lambda rows: pl.BlockSpec((rows, 128), lambda i: (0, i))
    return pl.pallas_call(
        grad_x_kernel,
        grid=(channels // 128,),
        in_specs=[col(tokens), col(3), col(4)],
        out_specs=col(tokens),
        out_shape=jax.ShapeDtypeStruct((tokens, channels), f32),
        scratch_shapes=[pltpu.VMEM((tokens + 8, 128), f32)],
        compiler_params=params(),
        name="grad_x",
    )(grad, later, taps)


def exchange(value, axis):
    return lax.all_to_all(value, axis, split_axis=0, concat_axis=0, tiled=True)


def swapped(value):
    return lax.ppermute(value, "tp", [(0, 1), (1, 0)])


def shifted(value, axis, by):
    devices = lax.axis_size(axis)
    pairs = [(i, i + by) for i in range(devices) if 0 <= i + by < devices]
    return lax.ppermute(value, axis, pairs)


def sent_to_all(value, axis):
    copies = jnp.broadcast_to(value[None], (lax.axis_size(axis), *value.shape))
    return exchange(copies, axis)


def carry_weights(total_decay):
    devices, place = lax.axis_size("sp"), lax.axis_index("sp")
    number = jnp.arange(devices)[:, None, None]
    factors = jnp.where(number > place, total_decay, 1.0)
    upto = lax.associative_scan(jnp.multiply, factors, axis=0)
    between = jnp.concatenate([jnp.ones_like(upto[:1]), upto[:-1]], axis=0)
    return jnp.where(number > place, between, 0.0)


def body(
    cotangent,
    routes,
    route_weight,
    expert_rows,
    gate_w,
    up_w,
    down_w,
    in_x,
    in_y,
    state,
    conv_taps,
    gate_a,
    gate_x,
    decay_rate,
    out_weight,
):
    tokens = cotangent.shape[0]
    experts = lax.axis_size("sp")
    core = lax.axis_index("tp").astype(jnp.int32).reshape(1)
    taps = conv_taps.shape[0]
    channels = in_x.shape[1]

    outgoing, target = send(core, routes.T, route_weight.T, cotangent, experts)
    arrived = exchange(outgoing, "sp")
    target = target.T

    edge = shifted(
        jnp.concatenate([in_x[tokens - taps + 1 :], state[tokens - 1 :]], axis=0), "sp", 1
    )
    packed, silu, slope, active = expert_pre(expert_rows[0], gate_w[0], up_w[0])
    mixed, y_slope, gelu, ahead, product, keep_part, input_part, direct, first = recur_pre(
        in_x, in_y, state, edge, conv_taps, gate_a, gate_x, decay_rate[None]
    )
    decays = sent_to_all(first[1:2].reshape(channels // 128, 128), "sp")
    weights = carry_weights(decays)

    arrived_far = swapped(arrived)
    near_rows, part = near(core, arrived, down_w[0])
    far_rows, gate_adj, up_adj, back_far = far(
        core, arrived_far, down_w[0], part, silu, slope, gate_w[0], up_w[0]
    )
    back_in = swapped(back_far)
    own = back_own(core, gate_adj, up_adj, gate_w[0], up_w[0], arrived.shape)
    returning = (own.astype(f32) + back_in.astype(f32)).astype(bf16)
    returned = exchange(returning, "sp")

    grad_gate, grad_up = grad_in(packed, gate_adj, up_adj)
    grad_down = grad_down_of(core, active, near_rows, far_rows)

    stream_own = combine(core, returned, target, cotangent)
    stream_peer = swapped(stream_own)
    grad_y, local, total = scan(
        core, stream_own, stream_peer, out_weight, y_slope, gelu, ahead, product, first
    )
    totals = sent_to_all(total.reshape(channels // 128, 128), "sp")
    partial = project(core, stream_own, stream_peer, mixed)
    shares = exchange(partial.reshape(experts, -1, channels), "sp")

    carry = jnp.sum(totals * weights, axis=0).reshape(1, channels)
    conv_grad = conv_grad_of(
        carry, local, product, keep_part, input_part, direct, gate_a, gate_x
    )
    later = shifted(conv_grad[: taps - 1], "sp", -1)
    grad_x = grad_x_of(conv_grad, later, conv_taps)
    grad_proj = jnp.sum(shares.astype(f32), axis=0)
    return (grad_gate[None], grad_up[None], grad_down[None], grad_proj, grad_x, grad_y)


def solution(mesh):
    in_specs = (
        P("sp", None),
        P("sp", None),
        P("sp", None),
        P("sp", None, None),
        P("sp", None, "tp"),
        P("sp", None, "tp"),
        P("sp", "tp", None),
        P("sp", "tp"),
        P("sp", "tp"),
        P("sp", "tp"),
        P(None, "tp"),
        P("tp", None, None),
        P("tp", None, None),
        P("tp"),
        P(None, "tp"),
    )
    out_specs = (
        P("sp", None, "tp"),
        P("sp", None, "tp"),
        P("sp", "tp", None),
        P("sp", "tp"),
        P("sp", "tp"),
        P("sp", "tp"),
    )
    return jax.shard_map(body, mesh=mesh, in_specs=in_specs, out_specs=out_specs, check_vma=False)
```

profile of v0, /device:TPU:32, one launch (start us, length us, event | category | flops | bytes accessed | tf_op | source)
XLA Modules:
  0.0 227.1 jit_solution(4131044691841005049)
XLA Ops:
  0.6 6.2 %send.1 = (bf16[64,16,1152]{2,1,0:T(8,128)(2,1)}, s32[8,384]{1,0:T(8,128)}) custom-call(s32[1]{0:T(128)} %bitcast.3.core_ref, s32[2,384]{1,0:T(2,128)} %bitcast.28, f32[2,384]{1,0:T(2,128)} %bitcast.29, bf16[384,2048]{1,0:T(8,128)(2,1)} %cot_ref.3), custom_call_target="tpu_custom_call" | custom-call | tf_op jit(solution)/shard_map/send/pallas_call | solution.py:102
  6.9 43.1 %all_to_all.25.block_ref = bf16[64,16,1152]{2,1,0:T(8,128)(2,1)S(1)} all-to-all(bf16[64,16,1152]{2,1,0:T(8,128)(2,1)} %get-tuple-element.33), channel_id=1, replica_groups=mesh['sp'=64,'tp'=2] {'sp'}, dimensions={0} | all-to-all | bytes 4718592 | tf_op jit(solution)/shard_map/all_to_all | solution.py:662
  50.0 11.8 %expert_pre.1 = (bf16[1152,2048]{1,0:T(8,128)(2,1)}, f32[1152,512]{1,0:T(8,128)}, f32[1152,512]{1,0:T(8,128)}, bf16[1152,512]{1,0:T(8,128)(2,1)}) custom-call(bf16[1152,2048]{1,0:T(8,128)(2,1)} %bitcast.32, bf16[2048,512]{1,0:T(8,128)(2,1)} %bitcast.19, bf16[2048,512]{1,0:T(8,128)(2,1)} %bitcast.22), custom_call_target="tpu_custom_call" | custom-call | flops 4831838208 | bytes 20971520 | tf_op jit(solution)/shard_map/expert_pre/pallas_call | solution.py:160
  61.9 5.3 %near.1 = (bf16[1152,1024]{1,0:T(8,128)(2,1)}, f32[1152,512]{1,0:T(8,128)}) custom-call(s32[1]{0:T(128)} %bitcast.3.core_ref, bf16[64,16,1152]{2,1,0:T(8,128)(2,1)} %copy-done.3, bf16[512,2048]{1,0:T(8,128)(2,1)} %bitcast.17), custom_call_target="tpu_custom_call" | custom-call | flops 1207959552 | bytes 9437184 | tf_op jit(solution)/shard_map/near/pallas_call | solution.py:289
  67.2 1.4 copy-done.2
  68.6 9.7 %far.1 = (bf16[1152,1024]{1,0:T(8,128)(2,1)}, bf16[1152,512]{1,0:T(8,128)(2,1)}, bf16[1152,512]{1,0:T(8,128)(2,1)}, bf16[64,16,1152]{2,1,0:T(8,128)(2,1)}) custom-call(s32[1]{0:T(128)} %bitcast.3.core_ref, bf16[64,16,1152]{2,1,0:T(8,128)(2,1)} %copy-done.2, bf16[512,2048]{1,0:T(8,128)(2,1)} %bitcast.18, f32[1152,512]{1,0:T(8,128)} %get-tuple-element.34.part_ref, ...), custom_call_target="tpu_custom_call" | custom-call | flops 3623878656 | bytes 16777216 | tf_op jit(solution)/shard_map/far/pallas_call | solution.py:340
  78.3 0.7 slice.101
  79.0 0.7 slice.100
  79.7 2.4 %collective-permute-start.3 = (bf16[4,512]{1,0:T(4,128)(2,1)S(1)}, bf16[4,512]{1,0:T(4,128)(2,1)S(1)}, u32[]{:S(2)}, u32[]{:S(2)}) collective-permute-start(bf16[4,512]{1,0:T(4,128)(2,1)S(1)} %pad_maximum_fusion.4), channel_id=1, source_target_pairs={{0,2},{2,4},{4,6},{6,8},{8,10},{10,12},{12,14},{14,16},{16,18},{18... | collective-permute-start | bytes 12296 | tf_op jit(solution)/shard_map/ppermute | solution.py:672
  82.1 7.3 %collective-permute-done.3.edge_ref = bf16[4,512]{1,0:T(4,128)(2,1)S(1)} collective-permute-done((bf16[4,512]{1,0:T(4,128)(2,1)S(1)}, bf16[4,512]{1,0:T(4,128)(2,1)S(1)}, u32[]{:S(2)}, u32[]{:S(2)}) %collective-permute-start.3) | collective-permute-done | bytes 4128 | tf_op jit(solution)/shard_map/ppermute | solution.py:672
  89.5 0.6 copy-done.7
  90.0 5.3 %recur_pre.1 = (bf16[384,512]{1,0:T(8,128)(2,1)}, f32[384,512]{1,0:T(8,128)}, f32[384,512]{1,0:T(8,128)}, f32[4,384,128]{2,1,0:T(8,128)}, f32[4,384,128]{2,1,0:T...) custom-call(bf16[384,512]{1,0:T(8,128)(2,1)} %x_ref.1, ...), custom_call_target="tpu_custom_call" | custom-call | flops 393216000 | bytes 8388608 | tf_op jit(solution)/shard_map/recur_pre/pallas_call | solution.py:234
  95.4 0.7 slice.102
  96.1 0.7 broadcast_in_dim.54
  96.8 4.3 %all-to-all-start.4 = ((f32[64,4,128]{2,1,0:T(4,128)}), f32[64,4,128]{2,1,0:T(4,128)S(1)}, u32[]{:S(2)}, u32[]{:S(2)}) async-start(f32[64,4,128]{2,1,0:T(4,128)} %broadcast_in_dim.54), calls=%async_computation.4 | async-start | bytes 262144 | tf_op jit(solution)/shard_map/all_to_all | solution.py:662
  101.0 6.4 %back_own.1 = bf16[64,16,1152]{2,1,0:T(8,128)(2,1)} custom-call(s32[1]{0:T(128)} %bitcast.3.core_ref, bf16[1152,512]{1,0:T(8,128)(2,1)} %get-tuple-element.37.gate_adj_ref, bf16[1152,512]{1,0:T(8,128)(2,1)} %get-tuple-element.38.up_adj_ref, bf16[2048,512]{1,0:T(8,128)(2,1)} %bitcast.21, bf16[2048,512]{1,0:T(8,128)(2,1)} %bitcast.24), custom_call_target="tpu_custom_call" | custom-call | flops 2415919104 | bytes 7340032 | tf_op jit(solution)/shard_map/back_own/pallas_call | solution.py:383
  107.4 3.7 %add_convert_fusion = bf16[64,16,1152]{2,1,0:T(8,128)(2,1)} fusion(bf16[64,16,1152]{2,1,0:T(8,128)(2,1)S(1)} %collective-permute-done.1, bf16[64,16,1152]{2,1,0:T(8,128)(2,1)} %back_own.1), kind=kLoop, calls=%fused_computation | loop fusion | flops 4718592 | bytes 7077888 | tf_op jit(solution)/shard_map/convert_element_type | solution.py:733
  111.1 10.5 %all-to-all-start.1 = ((bf16[64,16,1152]{2,1,0:T(8,128)(2,1)}), bf16[64,16,1152]{2,1,0:T(8,128)(2,1)S(1)}, u32[]{:S(2)}, u32[]{:S(2)}) async-start(bf16[64,16,1152]{2,1,0:T(8,128)(2,1)} %add_convert_fusion), calls=%async_computation.1 | async-start | bytes 4718592 | tf_op jit(solution)/shard_map/all_to_all | solution.py:662
  121.6 0.8 copy.23
  122.4 0.1 broadcast_select_fusion
  122.6 29.3 %all-to-all-done.1.block_ref = bf16[64,16,1152]{2,1,0:T(8,128)(2,1)S(1)} async-done(((bf16[64,16,1152]{2,1,0:T(8,128)(2,1)}), bf16[64,16,1152]{2,1,0:T(8,128)(2,1)S(1)}, u32[]{:S(2)}, u32[]{:S(2)}) %all-to-all-start.1) | async-done | bytes 2359328 | tf_op jit(solution)/shard_map/all_to_all | solution.py:662
  151.9 1.4 copy-done
  153.3 5.9 %combine.1.own_ref = bf16[384,1024]{1,0:T(8,128)(2,1)} custom-call(s32[1]{0:T(128)} %bitcast.3.core_ref, bf16[64,16,1152]{2,1,0:T(8,128)(2,1)} %copy-done, s32[384,8]{1,0:T(8,128)} %bitcast.25, bf16[384,2048]{1,0:T(8,128)(2,1)} %cot_ref.3), custom_call_target="tpu_custom_call" | custom-call | tf_op jit(solution)/shard_map/combine/pallas_call | solution.py:490
  159.3 2.4 %collective-permute-done.2.peer_ref = bf16[384,1024]{1,0:T(8,128)(2,1)S(1)} collective-permute-done((bf16[384,1024]{1,0:T(8,128)(2,1)}, bf16[384,1024]{1,0:T(8,128)(2,1)S(1)}, u32[]{:S(2)}, u32[]{:S(2)}) %collective-permute-start.2) | collective-permute-done | bytes 786464 | tf_op jit(solution)/shard_map/ppermute | solution.py:666
  161.7 0.9 copy-done.1
  162.6 5.6 %scan.1 = (f32[384,512]{1,0:T(8,128)}, f32[4,384,128]{2,1,0:T(8,128)}, f32[1,512]{1,0:T(1,128)}) custom-call(s32[1]{0:T(128)} %bitcast.3.core_ref, bf16[384,1024]{1,0:T(8,128)(2,1)} %combine.1.own_ref, bf16[384,1024]{1,0:T(8,128)(2,1)} %copy-done.1, bf16[2048,512]{1,0:T(8,128)(2,1)} %weight_ref.1, f32[384,512]{1,0:T(8,128)} %get-tuple-element.47.slope_ref, ...), custom_call_target="tpu_custom_call" | custom-call | tf_op jit(solution)/shard_map/scan/pallas_call | solution.py:544
  168.2 1.4 broadcast_in_dim.51
  169.5 7.2 %all-to-all-start.3 = ((f32[64,4,128]{2,1,0:T(4,128)}), f32[64,4,128]{2,1,0:T(4,128)S(1)}, u32[]{:S(2)}, u32[]{:S(2)}) async-start(f32[64,4,128]{2,1,0:T(4,128)} %broadcast_in_dim.51), calls=%async_computation.3 | async-start | bytes 262144 | tf_op jit(solution)/shard_map/all_to_all | solution.py:662
  176.7 4.1 %project.1 = bf16[2048,512]{1,0:T(8,128)(2,1)} custom-call(s32[1]{0:T(128)} %bitcast.3.core_ref, bf16[384,1024]{1,0:T(8,128)(2,1)} %combine.1.own_ref, bf16[384,1024]{1,0:T(8,128)(2,1)} %copy-done.1, bf16[384,512]{1,0:T(8,128)(2,1)} %get-tuple-element.46.mixed_ref), custom_call_target="tpu_custom_call" | custom-call | tf_op jit(solution)/shard_map/project/pallas_call | solution.py:585
  180.8 4.8 %all-to-all-done.3 = f32[64,4,128]{2,1,0:T(4,128)S(1)} async-done(((f32[64,4,128]{2,1,0:T(4,128)}), f32[64,4,128]{2,1,0:T(4,128)S(1)}, u32[]{:S(2)}, u32[]{:S(2)}) %all-to-all-start.3) | async-done | bytes 131104 | tf_op jit(solution)/shard_map/all_to_all | solution.py:662
  185.6 5.9 %all-to-all-start.2 = ((bf16[64,32,512]{2,1,0:T(8,128)(2,1)}), bf16[64,32,512]{2,1,0:T(8,128)(2,1)S(1)}, u32[]{:S(2)}, u32[]{:S(2)}) async-start(bf16[64,32,512]{2,1,0:T(8,128)(2,1)} %bitcast.16), calls=%async_computation.2 | async-start | bytes 4194304 | tf_op jit(solution)/shard_map/all_to_all | solution.py:662
  191.6 0.1 pad.43
  191.7 0.1 pad.42
  191.8 0.1 pad.44
  191.9 0.1 pad.45
  192.0 0.2 pad.47
  192.2 0.2 pad.46
  192.5 0.4 pad.63
  192.9 0.4 pad.87
  193.4 9.1 %grad_in.1 = (bf16[2048,512]{1,0:T(8,128)(2,1)}, bf16[2048,512]{1,0:T(8,128)(2,1)}) custom-call(bf16[1152,2048]{1,0:T(8,128)(2,1)} %get-tuple-element.32.packed_ref, bf16[1152,512]{1,0:T(8,128)(2,1)} %get-tuple-element.37.gate_adj_ref, bf16[1152,512]{1,0:T(8,128)(2,1)} %get-tuple-element.38.up_adj_ref), custom_call_target="tpu_custom_call" | custom-call | flops 4831838208 | bytes 11534336 | tf_op jit(solution)/shard_map/grad_in/pallas_call | solution.py:412
  202.5 0.7 multiply_reduce_fusion
  203.2 4.4 %adjoint.1.grad_ref = f32[384,512]{1,0:T(8,128)} custom-call(f32[1,512]{1,0:T(1,128)} %bitcast.26, f32[4,384,128]{2,1,0:T(8,128)} %get-tuple-element.53.local_ref, f32[4,384,128]{2,1,0:T(8,128)} %get-tuple-element.50.product_ref, f32[384,512]{1,0:T(8,128)} %get-tuple-element.54.keep_ref, f32[384,512]{1,0:T(8,128)} %get-tuple-element.55.input_ref, ...), custom_call_target="tpu_custom_call" | custom-call | tf_op jit(solution)/shard_map/adjoint/pallas_call | solution.py:624
  207.6 0.7 slice.150
  208.3 6.7 %collective-permute-start.4 = (f32[3,512]{1,0:T(4,128)S(1)}, f32[3,512]{1,0:T(4,128)S(1)}, u32[]{:S(2)}, u32[]{:S(2)}) collective-permute-start(f32[3,512]{1,0:T(4,128)S(1)} %slice.150), channel_id=1, source_target_pairs={{2,0},{4,2},{6,4},{8,6},{10,8},{12,10},{14,12},{16,14},{18,16},{20... | collective-permute-start | bytes 18440 | tf_op jit(solution)/shard_map/ppermute | solution.py:672
  215.0 7.0 %grad_down.1 = bf16[512,2048]{1,0:T(8,128)(2,1)} custom-call(s32[1]{0:T(128)} %bitcast.3.core_ref, bf16[1152,512]{1,0:T(8,128)(2,1)} %get-tuple-element.41.active_ref, bf16[1152,1024]{1,0:T(8,128)(2,1)} %get-tuple-element.42.near_ref, bf16[1152,1024]{1,0:T(8,128)(2,1)} %get-tuple-element.43.far_ref), custom_call_target="tpu_custom_call" | custom-call | flops 2415919104 | bytes 9437184 | tf_op jit(solution)/shard_map/grad_down/pallas_call | solution.py:445
  222.0 0.6 copy-done.6
  222.6 3.5 %grad_x.1 = f32[384,512]{1,0:T(8,128)} custom-call(f32[384,512]{1,0:T(8,128)} %adjoint.1.grad_ref, f32[3,512]{1,0:T(4,128)} %copy-done.6, f32[4,512]{1,0:T(4,128)} %taps_ref.3), custom_call_target="tpu_custom_call" | custom-call | tf_op jit(solution)/shard_map/grad_x/pallas_call | solution.py:649
  226.1 0.9 convert_reduce_fusion
  (50 shorter events, 0.4 us)
Async XLA Ops:
  50.0 11.8 %copy-start.3 = (bf16[64,16,1152]{2,1,0:T(8,128)(2,1)}, bf16[64,16,1152]{2,1,0:T(8,128)(2,1)S(1)}, u32[]{:S(2)}) copy-start(bf16[64,16,1152]{2,1,0:T(8,128)(2,1)S(1)} %all_to_all.25.block_ref) | copy-start | bytes 7077892
  50.0 17.1 %collective-permute-start = (bf16[64,16,1152]{2,1,0:T(8,128)(2,1)S(1)}, bf16[64,16,1152]{2,1,0:T(8,128)(2,1)S(1)}, u32[]{:S(2)}, u32[]{:S(2)}) collective-permute-start(bf16[64,16,1152]{2,1,0:T(8,128)(2,1)S(1)} %all_to_all.25.block_ref), channel_id=1, source_target_pairs={{0,1},{1,0},{2,3},{3,2},{4,5},{5,4},{6,7},{7,6},{8,9},{9,8},{10,11... | collective-permute-start | bytes 7077896 | tf_op jit(solution)/shard_map/ppermute | solution.py:666
  67.1 1.4 copy-start.2
  78.3 29.1 %collective-permute-start.1 = (bf16[64,16,1152]{2,1,0:T(8,128)(2,1)}, bf16[64,16,1152]{2,1,0:T(8,128)(2,1)S(1)}, u32[]{:S(2)}, u32[]{:S(2)}) collective-permute-start(bf16[64,16,1152]{2,1,0:T(8,128)(2,1)} %get-tuple-element.44), channel_id=1, source_target_pairs={{0,1},{1,0},{2,3},{3,2},{4,5},{5,4},{6,7},{7,6},{8,9},{9,8},{10,11... | collective-permute-start | bytes 7077896 | tf_op jit(solution)/shard_map/ppermute | solution.py:666
  79.7 9.7 %collective-permute-start.3 = (bf16[4,512]{1,0:T(4,128)(2,1)S(1)}, bf16[4,512]{1,0:T(4,128)(2,1)S(1)}, u32[]{:S(2)}, u32[]{:S(2)}) collective-permute-start(bf16[4,512]{1,0:T(4,128)(2,1)S(1)} %pad_maximum_fusion.4), channel_id=1, source_target_pairs={{0,2},{2,4},{4,6},{6,8},{8,10},{10,12},{12,14},{14,16},{16,18},{18... | collective-permute-start | bytes 12296 | tf_op jit(solution)/shard_map/ppermute | solution.py:672
  89.4 0.6 copy-start.7
  96.8 14.3 %all-to-all-start.4 = ((f32[64,4,128]{2,1,0:T(4,128)}), f32[64,4,128]{2,1,0:T(4,128)S(1)}, u32[]{:S(2)}, u32[]{:S(2)}) async-start(f32[64,4,128]{2,1,0:T(4,128)} %broadcast_in_dim.54), calls=%async_computation.4 | async-start | bytes 262144 | tf_op jit(solution)/shard_map/all_to_all | solution.py:662
  111.1 10.5 %copy-start.5 = (s32[8,384]{1,0:T(8,128)S(1)}, s32[8,384]{1,0:T(8,128)}, u32[]{:S(2)}) copy-start(s32[8,384]{1,0:T(8,128)} %get-tuple-element.45) | copy-start | bytes 36868
  111.1 40.8 %all-to-all-start.1 = ((bf16[64,16,1152]{2,1,0:T(8,128)(2,1)}), bf16[64,16,1152]{2,1,0:T(8,128)(2,1)S(1)}, u32[]{:S(2)}, u32[]{:S(2)}) async-start(bf16[64,16,1152]{2,1,0:T(8,128)(2,1)} %add_convert_fusion), calls=%async_computation.1 | async-start | bytes 4718592 | tf_op jit(solution)/shard_map/all_to_all | solution.py:662
  122.6 54.1 %copy-start.4 = (f32[8,4,128]{2,1,0:T(4,128)}, f32[8,4,128]{2,1,0:T(4,128)S(1)}, u32[]{:S(2)}) copy-start(f32[8,4,128]{2,1,0:T(4,128)S(1)} %slice_multiply_fusion.2) | copy-start | bytes 49156
  151.9 1.4 copy-start
  159.2 2.5 %collective-permute-start.2 = (bf16[384,1024]{1,0:T(8,128)(2,1)}, bf16[384,1024]{1,0:T(8,128)(2,1)S(1)}, u32[]{:S(2)}, u32[]{:S(2)}) collective-permute-start(bf16[384,1024]{1,0:T(8,128)(2,1)} %combine.1.own_ref), channel_id=1, source_target_pairs={{0,1},{1,0},{2,3},{3,2},{4,5},{5,4},{6,7},{7,6},{8,9},{9,8},{10,11... | collective-permute-start | bytes 2359304 | tf_op jit(solution)/shard_map/ppermute | solution.py:666
  161.7 0.9 copy-start.1
  169.5 16.1 %all-to-all-start.3 = ((f32[64,4,128]{2,1,0:T(4,128)}), f32[64,4,128]{2,1,0:T(4,128)S(1)}, u32[]{:S(2)}, u32[]{:S(2)}) async-start(f32[64,4,128]{2,1,0:T(4,128)} %broadcast_in_dim.51), calls=%async_computation.3 | async-start | bytes 262144 | tf_op jit(solution)/shard_map/all_to_all | solution.py:662
  180.8 10.8 %slice-start = ((f32[8,4,128]{2,1,0:T(4,128)}), f32[1,4,128]{2,1,0:T(4,128)S(1)}, s32[]{:S(2)}) async-start(f32[8,4,128]{2,1,0:T(4,128)} %copy-done.4), calls=%async_computation.5 | async-start | bytes 4096 | tf_op jit(solution)/shard_map/slice | solution.py:684
  185.6 40.5 %all-to-all-start.2 = ((bf16[64,32,512]{2,1,0:T(8,128)(2,1)}), bf16[64,32,512]{2,1,0:T(8,128)(2,1)S(1)}, u32[]{:S(2)}, u32[]{:S(2)}) async-start(bf16[64,32,512]{2,1,0:T(8,128)(2,1)} %bitcast.16), calls=%async_computation.2 | async-start | bytes 4194304 | tf_op jit(solution)/shard_map/all_to_all | solution.py:662
  208.3 13.7 %collective-permute-start.4 = (f32[3,512]{1,0:T(4,128)S(1)}, f32[3,512]{1,0:T(4,128)S(1)}, u32[]{:S(2)}, u32[]{:S(2)}) collective-permute-start(f32[3,512]{1,0:T(4,128)S(1)} %slice.150), channel_id=1, source_target_pairs={{2,0},{4,2},{6,4},{8,6},{10,8},{12,10},{14,12},{16,14},{18,16},{20... | collective-permute-start | bytes 18440 | tf_op jit(solution)/shard_map/ppermute | solution.py:672
  222.0 0.6 copy-start.6
where the time goes:
time: 229 us; the launch traced here: 227 us
  Pallas kernels  84.3 us (37%)
  waiting for transfers between devices  43.8 us (19%)
  blocking collectives  43.1 us (19%)
  starting transfers between devices  36.9 us (16%)
  local copies, waits for them, and re-layouts  12.2 us (5%)
  other arithmetic  5.75 us (3%)
    all_to_all x1, blocking collectives, exchange(): return lax.all_to_all(value, axis, split_axis=0, concat_axis=0, tiled=True)  43.1 us
    all_to_all x4, waiting for transfers between devices, exchange(): return lax.all_to_all(value, axis, split_axis=0, concat_axis=0, tiled=True)  34.1 us
    all_to_all x4, starting transfers between devices, exchange(): return lax.all_to_all(value, axis, split_axis=0, concat_axis=0, tiled=True)  27.8 us
    pallas_call x1, Pallas kernels, expert_pre(): pl.pallas_call(expert_pre_kernel, grid=(count // size,), in_specs=[by_row...  11.8 us
    pallas_call x1, Pallas kernels, far(): pl.pallas_call(far_kernel, grid_spec=pltpu.PrefetchScalarGridSpec(num_sca...  9.75 us
    ppermute x2, starting transfers between devices, shifted(): return lax.ppermute(value, axis, pairs)  9.08 us
    pallas_call x1, Pallas kernels, grad_in(): pl.pallas_call(grad_in_kernel, grid=(model // size,), in_specs=[pl.BlockS...  9.08 us
    ppermute x2, waiting for transfers between devices, shifted(): return lax.ppermute(value, axis, pairs)  7.31 us
  transfers between devices with their start and end apart: 9, of which 4 were waited for; matrix products, arithmetic and copies ran while one was open for 5% of the time, Pallas kernels for 25%

commit v1 on v0

--- a/solution.py
+++ b/solution.py
@@ -32,7 +32,7 @@
     return pltpu.CompilerParams(dimension_semantics=("arbitrary",) * n, vmem_limit_bytes=mb << 20)
 
 
-def whole(shape, memory_space=None):
+def whole(shape):
     return pl.BlockSpec(shape, lambda *_: (0,) * len(shape))
 
 
@@ -218,10 +218,23 @@
         step = scratch[pl.ds(j + 1, segments, stride=length), :]
         product = step if product is None else step * product
         product_ref[0, pl.ds(j, segments, stride=length), :] = product
-    total = decay[0:1]
-    for s in range(segments):
-        total = total * product[s : s + 1]
-    first_ref[...] = jnp.concatenate([decay[0:1], total, jnp.zeros_like(decay[0:6])], axis=0)
+    rest = product[1:2]
+    for s in range(2, segments):
+        rest = rest * product[s : s + 1]
+    total = decay[0:1] * product[0:1] * rest
+    first_ref[...] = jnp.concatenate(
+        [
+            decay[0:1],
+            total,
+            jnp.zeros_like(total),
+            product_ref[0, 0:3, :] * rest,
+            keep_ref[0:3, :],
+            input_ref[0:3, :],
+            direct_ref[0:3, :],
+            jnp.zeros_like(total),
+        ],
+        axis=0,
+    )
 
 
 def recur_pre(in_x, in_y, state, edge, taps, gate_a, gate_x, rate):
@@ -235,12 +248,12 @@
         recur_pre_kernel,
         grid=(blocks,),
         in_specs=[col(tokens), col(tokens), col(tokens), col(4), col(4), block, block, col(1)],
-        out_specs=[col(tokens)] * 3 + [cube] * 2 + [col(tokens)] * 3 + [col(8)],
+        out_specs=[col(tokens)] * 3 + [cube] * 2 + [col(tokens)] * 3 + [col(16)],
         out_shape=[jax.ShapeDtypeStruct((tokens, channels), bf16)]
         + [big] * 2
         + [jax.ShapeDtypeStruct((blocks, tokens, span), f32)] * 2
         + [big] * 3
-        + [jax.ShapeDtypeStruct((8, channels), f32)],
+        + [jax.ShapeDtypeStruct((16, channels), f32)],
         scratch_shapes=[pltpu.VMEM((tokens + 16, span), f32)],
         compiler_params=params(),
         cost_estimate=pl.CostEstimate(
@@ -374,7 +387,7 @@
 
 
 def back_own(core, gate_adj, up_adj, gate, up, shape):
-    experts, _, wide = shape
+    _, _, wide = shape
     half = wide - 128
     count, hidden = gate_adj.shape
     size = pair * group_rows
@@ -506,11 +519,17 @@
     )(core, returned, target, cotangent)
 
 
+def two_terms(value):
+    high = value.astype(bf16)
+    return high, (value - high.astype(f32)).astype(bf16)
+
+
 def scan_kernel(
     core_ref, own_ref, peer_ref, weight_ref, slope_ref, gelu_ref, ahead_ref, product_ref, first_ref,
-    grad_y_ref, local_ref, total_ref, scratch,
+    share_ref, grad_y_ref, local_ref, out_ref, head_ref, scratch,
 ):
     tokens, half = own_ref.shape
+    channels = weight_ref.shape[1]
     core = core_ref[0]
     near_weight = weight_ref[pl.ds(pl.multiple_of(core * half, half), half), :]
     far_weight = weight_ref[pl.ds(pl.multiple_of((1 - core) * half, half), half), :]
@@ -518,10 +537,11 @@
     grad_y_ref[...] = grad * slope_ref[...]
     state_grad = grad * gelu_ref[...]
     length = tokens // segments
-    for b in range(scratch.shape[0]):
-        at = slice(128 * b, 128 * (b + 1))
-        scratch[b] = state_grad[:, at]
-    for b in range(scratch.shape[0]):
+    blocks = scratch.shape[0]
+    for b in range(blocks):
+        scratch[b] = state_grad[:, 128 * b : 128 * (b + 1)]
+    carries = []
+    for b in range(blocks):
         at = slice(128 * b, 128 * (b + 1))
         value = None
         for j in reversed(range(length)):
@@ -533,14 +553,24 @@
             local_ref[b, pl.ds(j, segments, stride=length), :] = value
         product = product_ref[b, pl.ds(0, segments, stride=length), :]
         carry = value[segments - 1 : segments]
-        for s in reversed(range(segments - 1)):
+        for s in reversed(range(1, segments - 1)):
             carry = value[s : s + 1] + product[s : s + 1] * carry
-        total_ref[:, at] = first_ref[0:1, at] * carry
-
-
-def scan(core, own, peer, weight, slope, gelu, ahead, product, first):
+        ends = local_ref[b, 0:3, :] + product_ref[b, 0:3, :] * carry
+        carries.append(first_ref[0:1, at] * ends[0:1])
+        head_ref[:, at] = jnp.concatenate(
+            [ends, first_ref[3:15, at], jnp.zeros((1, 128), f32)], axis=0
+        )
+    decay = jnp.concatenate([first_ref[1:2, 128 * b : 128 * (b + 1)] for b in range(blocks)], axis=0)
+    terms = two_terms(decay) + two_terms(jnp.concatenate(carries, axis=0))
+    line = jnp.concatenate([term.astype(f32) for term in terms], axis=0).astype(bf16)
+    out_ref[:, :, 0:channels] = share_ref[...]
+    out_ref[:, :, channels:] = jnp.broadcast_to(line[None], (out_ref.shape[0], *line.shape))
+
+
+def scan(core, own, peer, weight, slope, gelu, ahead, product, first, share):
     tokens, half = own.shape
     channels = weight.shape[1]
+    experts, rows, _ = share.shape
     return pl.pallas_call(
         scan_kernel,
         grid_spec=pltpu.PrefetchScalarGridSpec(
@@ -554,108 +584,131 @@
                 whole((tokens, channels)),
                 whole(ahead.shape),
                 whole(ahead.shape),
-                whole((8, channels)),
+                whole((16, channels)),
+                whole(share.shape),
             ],
-            out_specs=[whole((tokens, channels)), whole(ahead.shape), whole((1, channels))],
+            out_specs=[
+                whole((tokens, channels)),
+                whole(ahead.shape),
+                whole((experts, rows, channels + 128)),
+                whole((16, channels)),
+            ],
             scratch_shapes=[pltpu.VMEM(ahead.shape, f32)],
         ),
         out_shape=[
             jax.ShapeDtypeStruct((tokens, channels), f32),
             jax.ShapeDtypeStruct(ahead.shape, f32),
-            jax.ShapeDtypeStruct((1, channels), f32),
+            jax.ShapeDtypeStruct((experts, rows, channels + 128), bf16),
+            jax.ShapeDtypeStruct((16, channels), f32),
         ],
         compiler_params=params(),
+        cost_estimate=pl.CostEstimate(
+            flops=4 * tokens * half * channels, transcendentals=0, bytes_accessed=9 << 20
+        ),
         name="scan",
-    )(core, own, peer, weight, slope, gelu, ahead, product, first)
-
-
-def project_kernel(core_ref, own_ref, peer_ref, mixed_ref, out_ref):
-    half = own_ref.shape[1]
+    )(core, own, peer, weight, slope, gelu, ahead, product, first, share)
+
+
+def project_kernel(core_ref, own_ref, peer_ref, mixed_ref, early_ref, late_ref):
     core = core_ref[0]
     mixed = mixed_ref[...]
-    near_rows = dot(own_ref[...], mixed, outer).astype(bf16)
-    far_rows = dot(peer_ref[...], mixed, outer).astype(bf16)
-    out_ref[pl.ds(pl.multiple_of(core * half, half), half), :] = near_rows
-    out_ref[pl.ds(pl.multiple_of((1 - core) * half, half), half), :] = far_rows
-
-
-def project(core, own, peer, mixed):
+    owners, rows, channels = early_ref.shape
+    share = owners // 2
+    for ref, place in ((own_ref, core), (peer_ref, 1 - core)):
+        value = dot(ref[...], mixed, outer).astype(bf16).reshape(share, 2 * rows, channels)
+        at = pl.ds(pl.multiple_of(place * share, share), share)
+        early_ref[at] = value[:, 0:rows]
+        late_ref[at] = value[:, rows:]
+
+
+def project(core, own, peer, mixed, owners):
     tokens, half = own.shape
     channels = mixed.shape[1]
+    shape = (owners, half // owners, channels)
     return pl.pallas_call(
         project_kernel,
         grid_spec=pltpu.PrefetchScalarGridSpec(
             num_scalar_prefetch=1,
             grid=(1,),
             in_specs=[whole((tokens, half)), whole((tokens, half)), whole((tokens, channels))],
-            out_specs=whole((2 * half, channels)),
-        ),
-        out_shape=jax.ShapeDtypeStruct((2 * half, channels), bf16),
+            out_specs=[whole(shape), whole(shape)],
+        ),
+        out_shape=[jax.ShapeDtypeStruct(shape, bf16)] * 2,
         compiler_params=params(),
         name="project",
     )(core, own, peer, mixed)
 
 
-def adjoint_kernel(
-    carry_ref, local_ref, product_ref, keep_ref, input_ref, direct_ref, a_ref, i_ref,
-    out_ref, scratch,
+def tail_kernel(
+    place_ref, line_ref, head_ref, local_ref, product_ref, keep_ref, input_ref, direct_ref,
+    a_ref, i_ref, taps_ref, out_ref, carries, adjoint, grads,
 ):
+    step = pl.program_id(0)
     tokens = local_ref.shape[1]
     length = tokens // segments
-    carry = carry_ref[...]
+    place = place_ref[0]
+
+    @pl.when(step == 0)
+    def _():
+        own = jnp.zeros((4, 128), f32)
+        beyond = jnp.zeros((4, 128), f32)
+        for j in reversed(range(line_ref.shape[0])):
+            line = line_ref[j].astype(f32)
+            decay = line[0:4] + line[4:8]
+            total = line[8:12] + line[12:16]
+            own = jnp.where(j > place, total + decay * own, own)
+            beyond = jnp.where(j > place + 1, total + decay * beyond, beyond)
+        carries[0:4, :] = own
+        carries[4:8, :] = beyond
+
+    def conv_grad(value, keep, gate, direct):
+        keep = (value * keep).astype(bf16)
+        gate = (value * gate).astype(bf16)
+        return value * direct + dot(keep, a_ref[0], inner) + dot(gate, i_ref[0], inner)
+
+    carry = carries[pl.ds(step, 1), :]
     for s in reversed(range(segments)):
         lo = s * length
         piece = local_ref[0, lo : lo + length, :] + product_ref[0, lo : lo + length, :] * carry
-        scratch[lo : lo + length, :] = piece
+        adjoint[lo : lo + length, :] = piece
         carry = piece[0:1]
-    adjoint = scratch[...]
-    keep = (adjoint * keep_ref[...]).astype(bf16)
-    gate = (adjoint * input_ref[...]).astype(bf16)
-    out_ref[...] = adjoint * direct_ref[...] + dot(keep, a_ref[0], inner) + dot(gate, i_ref[0], inner)
-
-
-def conv_grad_of(carry, local, product, keep, gate, direct, gate_a, gate_x):
-    tokens = local.shape[1]
-    blocks, span = gate_a.shape[:2]
+    grads[0:tokens, :] = conv_grad(adjoint[...], keep_ref[...], input_ref[...], direct_ref[...])
+    head = head_ref[...]
+    spare = jnp.zeros((5, 128), f32)
+    three = lambda k: jnp.concatenate([head[3 * k : 3 * k + 3], spare], axis=0)
+    later = three(0) + three(1) * carries[pl.ds(step + 4, 1), :]
+    grads[tokens : tokens + 8, :] = conv_grad(later, three(2), three(3), three(4))
+    total = taps_ref[0:1, :] * grads[3 : 3 + tokens, :]
+    for j in range(1, 4):
+        total = total + taps_ref[j : j + 1, :] * grads[3 - j : 3 - j + tokens, :]
+    out_ref[...] = total
+
+
+def tail(place, shares, head, local, product, keep, gate, direct, gate_a, gate_x, taps):
+    blocks, tokens, span = local.shape
     channels = blocks * span
-    cube = pl.BlockSpec((1, tokens, span), lambda i: (i, 0, 0))
-    col = lambda rows: pl.BlockSpec((rows, span), lambda i: (0, i))
-    block = pl.BlockSpec((1, span, span), lambda i: (i, 0, 0))
-    return pl.pallas_call(
-        adjoint_kernel,
-        grid=(blocks,),
-        in_specs=[col(1), cube, cube] + [col(tokens)] * 3 + [block, block],
-        out_specs=col(tokens),
+    owners, rows, _ = shares.shape
+    cube = pl.BlockSpec((1, tokens, span), lambda i, c: (i, 0, 0))
+    col = lambda rows: pl.BlockSpec((rows, span), lambda i, c: (0, i))
+    block = pl.BlockSpec((1, span, span), lambda i, c: (i, 0, 0))
+    line = pl.BlockSpec((owners, rows, 128), lambda i, c: (0, 0, channels // 128))
+    return pl.pallas_call(
+        tail_kernel,
+        grid_spec=pltpu.PrefetchScalarGridSpec(
+            num_scalar_prefetch=1,
+            grid=(blocks,),
+            in_specs=[line, col(16), cube, cube] + [col(tokens)] * 3 + [block, block, col(4)],
+            out_specs=col(tokens),
+            scratch_shapes=[
+                pltpu.VMEM((8, span), f32),
+                pltpu.VMEM((tokens, span), f32),
+                pltpu.VMEM((tokens + 8, span), f32),
+            ],
+        ),
         out_shape=jax.ShapeDtypeStruct((tokens, channels), f32),
-        scratch_shapes=[pltpu.VMEM((tokens, span), f32)],
-        compiler_params=params(),
-        name="adjoint",
-    )(carry, local, product, keep, gate, direct, gate_a, gate_x)
-
-
-def grad_x_kernel(grad_ref, later_ref, taps_ref, out_ref, scratch):
-    tokens = grad_ref.shape[0]
-    scratch[0:tokens, :] = grad_ref[...]
-    scratch[tokens : tokens + 3, :] = later_ref[...]
-    total = taps_ref[0:1, :] * scratch[3 : 3 + tokens, :]
-    for j in range(1, 4):
-        total = total + taps_ref[j : j + 1, :] * scratch[3 - j : 3 - j + tokens, :]
-    out_ref[...] = total
-
-
-def grad_x_of(grad, later, taps):
-    tokens, channels = grad.shape
-    col = lambda rows: pl.BlockSpec((rows, 128), lambda i: (0, i))
-    return pl.pallas_call(
-        grad_x_kernel,
-        grid=(channels // 128,),
-        in_specs=[col(tokens), col(3), col(4)],
-        out_specs=col(tokens),
-        out_shape=jax.ShapeDtypeStruct((tokens, channels), f32),
-        scratch_shapes=[pltpu.VMEM((tokens + 8, 128), f32)],
-        compiler_params=params(),
-        name="grad_x",
-    )(grad, later, taps)
+        compiler_params=params(),
+        name="tail",
+    )(place, shares, head, local, product, keep, gate, direct, gate_a, gate_x, taps)
 
 
 def exchange(value, axis):
@@ -670,20 +723,6 @@
     devices = lax.axis_size(axis)
     pairs = [(i, i + by) for i in range(devices) if 0 <= i + by < devices]
     return lax.ppermute(value, axis, pairs)
-
-
-def sent_to_all(value, axis):
-    copies = jnp.broadcast_to(value[None], (lax.axis_size(axis), *value.shape))
-    return exchange(copies, axis)
-
-
-def carry_weights(total_decay):
-    devices, place = lax.axis_size("sp"), lax.axis_index("sp")
-    number = jnp.arange(devices)[:, None, None]
-    factors = jnp.where(number > place, total_decay, 1.0)
-    upto = lax.associative_scan(jnp.multiply, factors, axis=0)
-    between = jnp.concatenate([jnp.ones_like(upto[:1]), upto[:-1]], axis=0)
-    return jnp.where(number > place, between, 0.0)
 
 
 def body(
@@ -709,19 +748,20 @@
     taps = conv_taps.shape[0]
     channels = in_x.shape[1]
 
+    place = lax.axis_index("sp").astype(jnp.int32).reshape(1)
+
+    edge = shifted(
+        jnp.concatenate([in_x[tokens - taps + 1 :], state[tokens - 1 :]], axis=0), "sp", 1
+    )
     outgoing, target = send(core, routes.T, route_weight.T, cotangent, experts)
+    outgoing, edge = lax.optimization_barrier((outgoing, edge))
     arrived = exchange(outgoing, "sp")
     target = target.T
 
-    edge = shifted(
-        jnp.concatenate([in_x[tokens - taps + 1 :], state[tokens - 1 :]], axis=0), "sp", 1
-    )
     packed, silu, slope, active = expert_pre(expert_rows[0], gate_w[0], up_w[0])
     mixed, y_slope, gelu, ahead, product, keep_part, input_part, direct, first = recur_pre(
         in_x, in_y, state, edge, conv_taps, gate_a, gate_x, decay_rate[None]
     )
-    decays = sent_to_all(first[1:2].reshape(channels // 128, 128), "sp")
-    weights = carry_weights(decays)
 
     arrived_far = swapped(arrived)
     near_rows, part = near(core, arrived, down_w[0])
@@ -738,20 +778,24 @@
 
     stream_own = combine(core, returned, target, cotangent)
     stream_peer = swapped(stream_own)
-    grad_y, local, total = scan(
-        core, stream_own, stream_peer, out_weight, y_slope, gelu, ahead, product, first
-    )
-    totals = sent_to_all(total.reshape(channels // 128, 128), "sp")
-    partial = project(core, stream_own, stream_peer, mixed)
-    shares = exchange(partial.reshape(experts, -1, channels), "sp")
-
-    carry = jnp.sum(totals * weights, axis=0).reshape(1, channels)
-    conv_grad = conv_grad_of(
-        carry, local, product, keep_part, input_part, direct, gate_a, gate_x
-    )
-    later = shifted(conv_grad[: taps - 1], "sp", -1)
-    grad_x = grad_x_of(conv_grad, later, conv_taps)
-    grad_proj = jnp.sum(shares.astype(f32), axis=0)
+    early, late = project(core, stream_own, stream_peer, mixed, experts)
+    early_shares = exchange(early, "sp")
+    grad_y, local, late, head = scan(
+        core, stream_own, stream_peer, out_weight, y_slope, gelu, ahead, product, first, late
+    )
+    head = shifted(head, "sp", -1)
+    late_shares = exchange(late, "sp")
+    grad_x = tail(
+        place, late_shares, head, local, product, keep_part, input_part, direct,
+        gate_a, gate_x, conv_taps,
+    )
+    grad_proj = jnp.concatenate(
+        [
+            jnp.sum(early_shares.astype(f32), axis=0),
+            jnp.sum(late_shares[:, :, :channels].astype(f32), axis=0),
+        ],
+        axis=0,
+    )
     return (grad_gate[None], grad_up[None], grad_down[None], grad_proj, grad_x, grad_y)
 
 

time: 229 us -> 214 us (0.934)
  starting transfers between devices: 36.9 us -> 29.4 us
  local copies, waits for them, and re-layouts: 12.2 us -> 6.52 us
    all_to_all x4 -> x3, waiting for transfers between devices: 34.1 us -> 43.7 us  [exchange(): return lax.all_to_all(value, axis, split_axis=0, concat_axis=0, tiled=True)]
    all_to_all x4 -> x3, starting transfers between devices: 27.8 us -> 19.4 us  [exchange(): return lax.all_to_all(value, axis, split_axis=0, concat_axis=0, tiled=True)]
    ppermute x2, waiting for transfers between devices: 7.31 us -> 0.46 us  [shifted(): return lax.ppermute(value, axis, pairs)]
    pallas_call x2 -> x1, Pallas kernels: 7.86 us -> 5.1 us  [tail(): pl.pallas_call(tail_kernel, grid_spec=pltpu.PrefetchScalarGridSpec(num_sc...]
    ppermute x3, waiting for transfers between devices: 2.39 us -> 0.01 us  [swapped(): return lax.ppermute(value, 'tp', [(0, 1), (1, 0)])]
    unnamed x17 -> x18, local copies, waits for them, and re-layouts: 5.29 us -> 4.3 us
  transfers between devices with their start and end apart: 9 -> 8, of which waited for: 4 -> 4; matrix products, arithmetic and copies ran while one was open for 5% -> 1% of each run, Pallas kernels for 25% -> 24%
where the time goes in v1:
time: 214 us; the launch traced here: 210 us
  Pallas kernels  82.2 us (38%)
  waiting for transfers between devices  44.1 us (21%)
  blocking collectives  42.5 us (20%)
  starting transfers between devices  29.4 us (14%)
  local copies, waits for them, and re-layouts  6.52 us (3%)
  other arithmetic  4.84 us (2%)
    all_to_all x3, waiting for transfers between devices, exchange(): return lax.all_to_all(value, axis, split_axis=0, concat_axis=0, tiled=True)  43.7 us
    all_to_all x1, blocking collectives, exchange(): return lax.all_to_all(value, axis, split_axis=0, concat_axis=0, tiled=True)  42.5 us
    all_to_all x3, starting transfers between devices, exchange(): return lax.all_to_all(value, axis, split_axis=0, concat_axis=0, tiled=True)  19.4 us
    pallas_call x1, Pallas kernels, expert_pre(): pl.pallas_call(expert_pre_kernel, grid=(count // size,), in_specs=[by_row...  11.9 us
    ppermute x2, starting transfers between devices, shifted(): return lax.ppermute(value, axis, pairs)  10.1 us
    pallas_call x1, Pallas kernels, far(): pl.pallas_call(far_kernel, grid_spec=pltpu.PrefetchScalarGridSpec(num_sca...  9.76 us
    pallas_call x1, Pallas kernels, grad_in(): pl.pallas_call(grad_in_kernel, grid=(model // size,), in_specs=[pl.BlockS...  9.08 us
    pallas_call x1, Pallas kernels, grad_down_of(): pl.pallas_call(grad_down_kernel, grid_spec=pltpu.PrefetchScalarGridSpec(n...  7.02 us
  transfers between devices with their start and end apart: 8, of which 4 were waited for; matrix products, arithmetic and copies ran while one was open for 1% of the time, Pallas kernels for 24%

profile of v1, /device:TPU:32, one launch (start us, length us, event | category | flops | bytes accessed | tf_op | source)
XLA Modules:
  0.0 210.4 jit_solution(6270941322465749095)
XLA Ops:
  0.6 0.7 slice.10
  1.3 0.7 slice.9
  2.1 3.4 %collective-permute-start = (bf16[4,512]{1,0:T(4,128)(2,1)S(1)}, bf16[4,512]{1,0:T(4,128)(2,1)S(1)}, u32[]{:S(2)}, u32[]{:S(2)}) collective-permute-start(bf16[4,512]{1,0:T(4,128)(2,1)S(1)} %pad_maximum_fusion.1), channel_id=1, source_target_pairs={{0,2},{2,4},{4,6},{6,8},{8,10},{10,12},{12,14},{14,16},{16,18},{18... | collective-permute-start | bytes 12296 | tf_op jit(solution)/shard_map/ppermute | solution.py:725
  5.5 6.2 %send.1 = (bf16[64,16,1152]{2,1,0:T(8,128)(2,1)}, s32[8,384]{1,0:T(8,128)}) custom-call(s32[1]{0:T(128)} %bitcast.3.core_ref, s32[2,384]{1,0:T(2,128)} %bitcast.22, f32[2,384]{1,0:T(2,128)} %bitcast.23, bf16[384,2048]{1,0:T(8,128)(2,1)} %cot_ref.3), custom_call_target="tpu_custom_call" | custom-call | tf_op jit(solution)/shard_map/send/pallas_call | solution.py:102
  11.7 0.1 collective-permute-done.edge_ref
  11.8 0.0 copy-start.7
  11.8 42.5 %all_to_all.20.block_ref = bf16[64,16,1152]{2,1,0:T(8,128)(2,1)S(1)} all-to-all(bf16[64,16,1152]{2,1,0:T(8,128)(2,1)} %get-tuple-element.39), channel_id=1, replica_groups=mesh['sp'=64,'tp'=2] {'sp'}, dimensions={0} | all-to-all | bytes 4718592 | tf_op jit(solution)/shard_map/all_to_all | solution.py:715
  54.3 0.0 copy-done.7
  54.3 0.0 collective-permute-start.1
  54.3 11.9 %expert_pre.1 = (bf16[1152,2048]{1,0:T(8,128)(2,1)}, f32[1152,512]{1,0:T(8,128)}, f32[1152,512]{1,0:T(8,128)}, bf16[1152,512]{1,0:T(8,128)(2,1)}) custom-call(bf16[1152,2048]{1,0:T(8,128)(2,1)} %bitcast.25, bf16[2048,512]{1,0:T(8,128)(2,1)} %bitcast.15, bf16[2048,512]{1,0:T(8,128)(2,1)} %bitcast.18), custom_call_target="tpu_custom_call" | custom-call | flops 4831838208 | bytes 20971520 | tf_op jit(solution)/shard_map/expert_pre/pallas_call | solution.py:160
  66.1 0.0 copy-done.4
  66.1 5.3 %near.1 = (bf16[1152,1024]{1,0:T(8,128)(2,1)}, f32[1152,512]{1,0:T(8,128)}) custom-call(s32[1]{0:T(128)} %bitcast.3.core_ref, bf16[64,16,1152]{2,1,0:T(8,128)(2,1)} %copy-done.4, bf16[512,2048]{1,0:T(8,128)(2,1)} %bitcast.13), custom_call_target="tpu_custom_call" | custom-call | flops 1207959552 | bytes 9437184 | tf_op jit(solution)/shard_map/near/pallas_call | solution.py:302
  71.4 0.0 collective-permute-done.1.block_ref
  71.5 1.4 copy-done.3
  72.9 9.8 %far.1 = (bf16[1152,1024]{1,0:T(8,128)(2,1)}, bf16[1152,512]{1,0:T(8,128)(2,1)}, bf16[1152,512]{1,0:T(8,128)(2,1)}, bf16[64,16,1152]{2,1,0:T(8,128)(2,1)}) custom-call(s32[1]{0:T(128)} %bitcast.3.core_ref, bf16[64,16,1152]{2,1,0:T(8,128)(2,1)} %copy-done.3, bf16[512,2048]{1,0:T(8,128)(2,1)} %bitcast.14, f32[1152,512]{1,0:T(8,128)} %get-tuple-element.40.part_ref, ...), custom_call_target="tpu_custom_call" | custom-call | flops 3623878656 | bytes 16777216 | tf_op jit(solution)/shard_map/far/pallas_call | solution.py:353
  82.6 0.0 collective-permute-start.2
  82.6 6.4 %back_own.1 = bf16[64,16,1152]{2,1,0:T(8,128)(2,1)} custom-call(s32[1]{0:T(128)} %bitcast.3.core_ref, bf16[1152,512]{1,0:T(8,128)(2,1)} %get-tuple-element.43.gate_adj_ref, bf16[1152,512]{1,0:T(8,128)(2,1)} %get-tuple-element.44.up_adj_ref, bf16[2048,512]{1,0:T(8,128)(2,1)} %bitcast.17, bf16[2048,512]{1,0:T(8,128)(2,1)} %bitcast.20), custom_call_target="tpu_custom_call" | custom-call | flops 2415919104 | bytes 7340032 | tf_op jit(solution)/shard_map/back_own/pallas_call | solution.py:396
  89.0 0.0 collective-permute-done.2
  89.0 3.6 %add_convert_fusion = bf16[64,16,1152]{2,1,0:T(8,128)(2,1)} fusion(bf16[64,16,1152]{2,1,0:T(8,128)(2,1)S(1)} %collective-permute-done.2, bf16[64,16,1152]{2,1,0:T(8,128)(2,1)} %back_own.1), kind=kLoop, calls=%fused_computation | loop fusion | flops 4718592 | bytes 7077888 | tf_op jit(solution)/shard_map/convert_element_type | solution.py:773
  92.6 6.5 %all-to-all-start.1 = ((bf16[64,16,1152]{2,1,0:T(8,128)(2,1)}), bf16[64,16,1152]{2,1,0:T(8,128)(2,1)S(1)}, u32[]{:S(2)}, u32[]{:S(2)}) async-start(bf16[64,16,1152]{2,1,0:T(8,128)(2,1)} %add_convert_fusion), calls=%async_computation.1 | async-start | bytes 4718592 | tf_op jit(solution)/shard_map/all_to_all | solution.py:715
  99.1 0.0 copy-done.6
  99.1 0.8 copy.21
  100.0 31.5 %all-to-all-done.1.block_ref = bf16[64,16,1152]{2,1,0:T(8,128)(2,1)S(1)} async-done(((bf16[64,16,1152]{2,1,0:T(8,128)(2,1)}), bf16[64,16,1152]{2,1,0:T(8,128)(2,1)S(1)}, u32[]{:S(2)}, u32[]{:S(2)}) %all-to-all-start.1) | async-done | bytes 2359328 | tf_op jit(solution)/shard_map/all_to_all | solution.py:715
  131.5 1.4 copy-done.1
  132.9 5.9 %combine.1.own_ref = bf16[384,1024]{1,0:T(8,128)(2,1)} custom-call(s32[1]{0:T(128)} %bitcast.3.core_ref, bf16[64,16,1152]{2,1,0:T(8,128)(2,1)} %copy-done.1, s32[384,8]{1,0:T(8,128)} %bitcast.21, bf16[384,2048]{1,0:T(8,128)(2,1)} %cot_ref.3), custom_call_target="tpu_custom_call" | custom-call | tf_op jit(solution)/shard_map/combine/pallas_call | solution.py:503
  138.8 0.0 collective-permute-start.3
  138.8 5.3 %recur_pre.1 = (bf16[384,512]{1,0:T(8,128)(2,1)}, f32[384,512]{1,0:T(8,128)}, f32[384,512]{1,0:T(8,128)}, f32[4,384,128]{2,1,0:T(8,128)}, f32[4,384,128]{2,1,0:T...) custom-call(bf16[384,512]{1,0:T(8,128)(2,1)} %x_ref.1, ...), custom_call_target="tpu_custom_call" | custom-call | flops 393216000 | bytes 8388608 | tf_op jit(solution)/shard_map/recur_pre/pallas_call | solution.py:247
  144.1 0.0 collective-permute-done.3.peer_ref
  144.1 0.0 copy-start.2
  144.1 0.9 copy-done.2
  145.0 4.1 %project.1 = (bf16[64,16,512]{2,1,0:T(8,128)(2,1)}, bf16[64,16,512]{2,1,0:T(8,128)(2,1)}) custom-call(s32[1]{0:T(128)} %bitcast.3.core_ref, bf16[384,1024]{1,0:T(8,128)(2,1)} %combine.1.own_ref, bf16[384,1024]{1,0:T(8,128)(2,1)} %copy-done.2, bf16[384,512]{1,0:T(8,128)(2,1)} %get-tuple-element.53.mixed_ref), custom_call_target="tpu_custom_call" | custom-call | tf_op jit(solution)/shard_map/project/pallas_call | solution.py:628
  149.0 6.9 %all-to-all-start.2 = ((bf16[64,16,512]{2,1,0:T(8,128)(2,1)}), bf16[64,16,512]{2,1,0:T(8,128)(2,1)S(1)}, u32[]{:S(2)}, u32[]{:S(2)}) async-start(bf16[64,16,512]{2,1,0:T(8,128)(2,1)} %get-tuple-element.54), calls=%async_computation.2 | async-start | bytes 2097152 | tf_op jit(solution)/shard_map/all_to_all | solution.py:715
  156.0 6.3 %scan.1 = (f32[384,512]{1,0:T(8,128)}, f32[4,384,128]{2,1,0:T(8,128)}, bf16[64,16,640]{2,1,0:T(8,128)(2,1)}, f32[16,512]{1,0:T(8,128)}) custom-call(s32[1]{0:T(128)} %bitcast.3.core_ref, bf16[384,1024]{1,0:T(8,128)(2,1)} %combine.1.own_ref, bf16[384,1024]{1,0:T(8,128)(2,1)} %copy-done.2, bf16[2048,512]{1,0:T(8,128)(2,1)} %weight_ref.1, ...), custom_call_target="tpu_custom_call" | custom-call | flops 805306368 | bytes 9437184 | tf_op jit(solution)/shard_map/scan/pallas_call | solution.py:574
  162.3 12.1 %all-to-all-done.2 = bf16[64,16,512]{2,1,0:T(8,128)(2,1)S(1)} async-done(((bf16[64,16,512]{2,1,0:T(8,128)(2,1)}), bf16[64,16,512]{2,1,0:T(8,128)(2,1)S(1)}, u32[]{:S(2)}, u32[]{:S(2)}) %all-to-all-start.2) | async-done | bytes 1048608 | tf_op jit(solution)/shard_map/all_to_all | solution.py:715
  174.4 5.9 %all-to-all-start.3 = ((bf16[64,16,640]{2,1,0:T(8,128)(2,1)}), bf16[64,16,640]{2,1,0:T(8,128)(2,1)S(1)}, u32[]{:S(2)}, u32[]{:S(2)}) async-start(bf16[64,16,640]{2,1,0:T(8,128)(2,1)} %get-tuple-element.61), calls=%async_computation.3 | async-start | bytes 2621440 | tf_op jit(solution)/shard_map/all_to_all | solution.py:715
  180.3 7.0 %grad_down.1 = bf16[512,2048]{1,0:T(8,128)(2,1)} custom-call(s32[1]{0:T(128)} %bitcast.3.core_ref, bf16[1152,512]{1,0:T(8,128)(2,1)} %get-tuple-element.47.active_ref, bf16[1152,1024]{1,0:T(8,128)(2,1)} %get-tuple-element.48.near_ref, bf16[1152,1024]{1,0:T(8,128)(2,1)} %get-tuple-element.49.far_ref), custom_call_target="tpu_custom_call" | custom-call | flops 2415919104 | bytes 9437184 | tf_op jit(solution)/shard_map/grad_down/pallas_call | solution.py:458
  187.4 9.1 %grad_in.1 = (bf16[2048,512]{1,0:T(8,128)(2,1)}, bf16[2048,512]{1,0:T(8,128)(2,1)}) custom-call(bf16[1152,2048]{1,0:T(8,128)(2,1)} %get-tuple-element.37.packed_ref, bf16[1152,512]{1,0:T(8,128)(2,1)} %get-tuple-element.43.gate_adj_ref, bf16[1152,512]{1,0:T(8,128)(2,1)} %get-tuple-element.44.up_adj_ref), custom_call_target="tpu_custom_call" | custom-call | flops 4831838208 | bytes 11534336 | tf_op jit(solution)/shard_map/grad_in/pallas_call | solution.py:425
  196.4 0.0 copy-done.8
  196.4 6.7 %collective-permute-start.4 = (f32[16,512]{1,0:T(8,128)S(1)}, f32[16,512]{1,0:T(8,128)S(1)}, u32[]{:S(2)}, u32[]{:S(2)}) collective-permute-start(f32[16,512]{1,0:T(8,128)S(1)} %copy-done.8), channel_id=1, source_target_pairs={{2,0},{4,2},{6,4},{8,6},{10,8},{12,10},{14,12},{16,14},{18,16},{20... | collective-permute-start | bytes 98312 | tf_op jit(solution)/shard_map/ppermute | solution.py:725
  203.1 0.2 convert_reduce_fusion.1
  203.3 0.0 all-to-all-done.3.line_ref
  203.3 0.0 copy-start
  203.3 0.2 convert_reduce_fusion
  203.5 0.8 pad_maximum_fusion
  204.3 0.4 collective-permute-done.4.head_ref
  204.7 0.0 copy-done
  204.7 0.6 copy-done.5
  205.3 5.1 %tail.1 = f32[384,512]{1,0:T(8,128)} custom-call(s32[1]{0:T(128)} %bitcast.12.place_ref, bf16[64,16,640]{2,1,0:T(8,128)(2,1)} %copy-done, f32[16,512]{1,0:T(8,128)} %copy-done.5, f32[4,384,128]{2,1,0:T(8,128)} %get-tuple-element.63.local_ref, f32[4,384,128]{2,1,0:T(8,128)} %get-tuple-element.58.product_ref, f32[384,512]{1,0:T(8,128)} %get-tuple-element.64.keep_ref, ...), custom_call_target="tpu_custom_call" | custom-call | tf_op jit(solution)/shard_map/tail/pallas_call | solution.py:695
  (7 shorter events, 0.0 us)
Async XLA Ops:
  2.1 9.7 %collective-permute-start = (bf16[4,512]{1,0:T(4,128)(2,1)S(1)}, bf16[4,512]{1,0:T(4,128)(2,1)S(1)}, u32[]{:S(2)}, u32[]{:S(2)}) collective-permute-start(bf16[4,512]{1,0:T(4,128)(2,1)S(1)} %pad_maximum_fusion.1), channel_id=1, source_target_pairs={{0,2},{2,4},{4,6},{6,8},{8,10},{10,12},{12,14},{14,16},{16,18},{18... | collective-permute-start | bytes 12296 | tf_op jit(solution)/shard_map/ppermute | solution.py:725
  11.8 42.5 %copy-start.7 = (bf16[4,512]{1,0:T(4,128)(2,1)}, bf16[4,512]{1,0:T(4,128)(2,1)S(1)}, u32[]{:S(2)}) copy-start(bf16[4,512]{1,0:T(4,128)(2,1)S(1)} %collective-permute-done.edge_ref) | copy-start | bytes 12292
  54.3 11.9 %copy-start.4 = (bf16[64,16,1152]{2,1,0:T(8,128)(2,1)}, bf16[64,16,1152]{2,1,0:T(8,128)(2,1)S(1)}, u32[]{:S(2)}) copy-start(bf16[64,16,1152]{2,1,0:T(8,128)(2,1)S(1)} %all_to_all.20.block_ref) | copy-start | bytes 7077892
  54.3 17.2 %collective-permute-start.1 = (bf16[64,16,1152]{2,1,0:T(8,128)(2,1)S(1)}, bf16[64,16,1152]{2,1,0:T(8,128)(2,1)S(1)}, u32[]{:S(2)}, u32[]{:S(2)}) collective-permute-start(bf16[64,16,1152]{2,1,0:T(8,128)(2,1)S(1)} %all_to_all.20.block_ref), channel_id=1, source_target_pairs={{0,1},{1,0},{2,3},{3,2},{4,5},{5,4},{6,7},{7,6},{8,9},{9,8},{10,11... | collective-permute-start | bytes 7077896 | tf_op jit(solution)/shard_map/ppermute | solution.py:719
  71.4 1.4 copy-start.3
  82.6 6.4 %collective-permute-start.2 = (bf16[64,16,1152]{2,1,0:T(8,128)(2,1)}, bf16[64,16,1152]{2,1,0:T(8,128)(2,1)S(1)}, u32[]{:S(2)}, u32[]{:S(2)}) collective-permute-start(bf16[64,16,1152]{2,1,0:T(8,128)(2,1)} %get-tuple-element.50), channel_id=1, source_target_pairs={{0,1},{1,0},{2,3},{3,2},{4,5},{5,4},{6,7},{7,6},{8,9},{9,8},{10,11... | collective-permute-start | bytes 7077896 | tf_op jit(solution)/shard_map/ppermute | solution.py:719
  92.6 6.5 %copy-start.6 = (s32[8,384]{1,0:T(8,128)S(1)}, s32[8,384]{1,0:T(8,128)}, u32[]{:S(2)}) copy-start(s32[8,384]{1,0:T(8,128)} %get-tuple-element.51) | copy-start | bytes 36868
  92.6 38.9 %all-to-all-start.1 = ((bf16[64,16,1152]{2,1,0:T(8,128)(2,1)}), bf16[64,16,1152]{2,1,0:T(8,128)(2,1)S(1)}, u32[]{:S(2)}, u32[]{:S(2)}) async-start(bf16[64,16,1152]{2,1,0:T(8,128)(2,1)} %add_convert_fusion), calls=%async_computation.1 | async-start | bytes 4718592 | tf_op jit(solution)/shard_map/all_to_all | solution.py:715
  131.5 1.4 copy-start.1
  138.8 5.3 %collective-permute-start.3 = (bf16[384,1024]{1,0:T(8,128)(2,1)}, bf16[384,1024]{1,0:T(8,128)(2,1)S(1)}, u32[]{:S(2)}, u32[]{:S(2)}) collective-permute-start(bf16[384,1024]{1,0:T(8,128)(2,1)} %combine.1.own_ref), channel_id=1, source_target_pairs={{0,1},{1,0},{2,3},{3,2},{4,5},{5,4},{6,7},{7,6},{8,9},{9,8},{10,11... | collective-permute-start | bytes 2359304 | tf_op jit(solution)/shard_map/ppermute | solution.py:719
  144.1 0.9 copy-start.2
  149.0 25.3 %all-to-all-start.2 = ((bf16[64,16,512]{2,1,0:T(8,128)(2,1)}), bf16[64,16,512]{2,1,0:T(8,128)(2,1)S(1)}, u32[]{:S(2)}, u32[]{:S(2)}) async-start(bf16[64,16,512]{2,1,0:T(8,128)(2,1)} %get-tuple-element.54), calls=%async_computation.2 | async-start | bytes 2097152 | tf_op jit(solution)/shard_map/all_to_all | solution.py:715
  174.4 28.9 %all-to-all-start.3 = ((bf16[64,16,640]{2,1,0:T(8,128)(2,1)}), bf16[64,16,640]{2,1,0:T(8,128)(2,1)S(1)}, u32[]{:S(2)}, u32[]{:S(2)}) async-start(bf16[64,16,640]{2,1,0:T(8,128)(2,1)} %get-tuple-element.61), calls=%async_computation.3 | async-start | bytes 2621440 | tf_op jit(solution)/shard_map/all_to_all | solution.py:715
  187.4 9.1 %copy-start.8 = (f32[16,512]{1,0:T(8,128)S(1)}, f32[16,512]{1,0:T(8,128)}, u32[]{:S(2)}) copy-start(f32[16,512]{1,0:T(8,128)} %get-tuple-element.62) | copy-start | bytes 98308
  196.4 8.3 %collective-permute-start.4 = (f32[16,512]{1,0:T(8,128)S(1)}, f32[16,512]{1,0:T(8,128)S(1)}, u32[]{:S(2)}, u32[]{:S(2)}) collective-permute-start(f32[16,512]{1,0:T(8,128)S(1)} %copy-done.8), channel_id=1, source_target_pairs={{2,0},{4,2},{6,4},{8,6},{10,8},{12,10},{14,12},{16,14},{18,16},{20... | collective-permute-start | bytes 98312 | tf_op jit(solution)/shard_map/ppermute | solution.py:725
  203.3 1.4 copy-start
  204.7 0.6 copy-start.5

commit v2 on v1

--- a/solution.py
+++ b/solution.py
@@ -28,7 +28,7 @@
     return lax.dot_general(a, b, dims, preferred_element_type=f32)
 
 
-def params(n=1, mb=58):
+def params(n=1, mb=32):
     return pltpu.CompilerParams(dimension_semantics=("arbitrary",) * n, vmem_limit_bytes=mb << 20)
 
 
@@ -524,22 +524,70 @@
     return high, (value - high.astype(f32)).astype(bf16)
 
 
+def share_rows(values, owners):
+    value = values.astype(bf16).reshape(owners, 2 * main, values.shape[1])
+    return value[:, 0:main], value[:, main:]
+
+
+def own_kernel(core_ref, own_ref, weight_ref, mixed_ref, grad_ref, share_ref):
+    own = own_ref[...]
+    grad_ref[...] = dot(own, weight_ref[...], plain)
+    left, right = share_rows(dot(own, mixed_ref[...], outer), share_ref.shape[0])
+    channels = left.shape[2]
+    share_ref[:, :, 0:channels] = left
+    share_ref[:, :, channels:] = right
+
+
+def own_part(core, own, weight, mixed, owners):
+    tokens, half = own.shape
+    channels = mixed.shape[1]
+    return pl.pallas_call(
+        own_kernel,
+        grid_spec=pltpu.PrefetchScalarGridSpec(
+            num_scalar_prefetch=1,
+            grid=(1,),
+            in_specs=[
+                whole((tokens, half)),
+                pl.BlockSpec((half, channels), lambda i, c: (c[0], 0)),
+                whole((tokens, channels)),
+            ],
+            out_specs=[whole((tokens, channels)), whole((owners // 2, main, 2 * channels))],
+        ),
+        out_shape=[
+            jax.ShapeDtypeStruct((tokens, channels), f32),
+            jax.ShapeDtypeStruct((owners // 2, main, 2 * channels), bf16),
+        ],
+        compiler_params=params(),
+        cost_estimate=pl.CostEstimate(
+            flops=4 * tokens * half * channels, transcendentals=0, bytes_accessed=4 << 20
+        ),
+        name="own_part",
+    )(core, own, weight, mixed)
+
+
 def scan_kernel(
-    core_ref, own_ref, peer_ref, weight_ref, slope_ref, gelu_ref, ahead_ref, product_ref, first_ref,
-    share_ref, grad_y_ref, local_ref, out_ref, head_ref, scratch,
+    core_ref, peer_ref, weight_ref, mixed_ref, part_ref, share_ref, slope_ref, gelu_ref, ahead_ref,
+    product_ref, first_ref,
+    grad_y_ref, local_ref, out_ref, head_ref, scratch,
 ):
-    tokens, half = own_ref.shape
+    tokens, _ = peer_ref.shape
     channels = weight_ref.shape[1]
     core = core_ref[0]
-    near_weight = weight_ref[pl.ds(pl.multiple_of(core * half, half), half), :]
-    far_weight = weight_ref[pl.ds(pl.multiple_of((1 - core) * half, half), half), :]
-    grad = dot(own_ref[...], near_weight, plain) + dot(peer_ref[...], far_weight, plain)
+    peer = peer_ref[...]
+    grad = part_ref[...] + dot(peer, weight_ref[...], plain)
     grad_y_ref[...] = grad * slope_ref[...]
     state_grad = grad * gelu_ref[...]
     length = tokens // segments
     blocks = scratch.shape[0]
     for b in range(blocks):
         scratch[b] = state_grad[:, 128 * b : 128 * (b + 1)]
+    owners = share_ref.shape[0]
+    left, right = share_rows(dot(peer, mixed_ref[...], outer), owners)
+    own_at = pl.ds(pl.multiple_of(core * owners, owners), owners)
+    peer_at = pl.ds(pl.multiple_of((1 - core) * owners, owners), owners)
+    out_ref[own_at, :, 0 : 2 * channels] = share_ref[...]
+    out_ref[peer_at, :, 0:channels] = left
+    out_ref[peer_at, :, channels : 2 * channels] = right
     carries = []
     for b in range(blocks):
         at = slice(128 * b, 128 * (b + 1))
@@ -563,14 +611,14 @@
     decay = jnp.concatenate([first_ref[1:2, 128 * b : 128 * (b + 1)] for b in range(blocks)], axis=0)
     terms = two_terms(decay) + two_terms(jnp.concatenate(carries, axis=0))
     line = jnp.concatenate([term.astype(f32) for term in terms], axis=0).astype(bf16)
-    out_ref[:, :, 0:channels] = share_ref[...]
-    out_ref[:, :, channels:] = jnp.broadcast_to(line[None], (out_ref.shape[0], *line.shape))
-
-
-def scan(core, own, peer, weight, slope, gelu, ahead, product, first, share):
-    tokens, half = own.shape
+    out_ref[:, :, 2 * channels :] = jnp.broadcast_to(line[None], (out_ref.shape[0], *line.shape))
+
+
+def scan(core, peer, weight, mixed, part, share, slope, gelu, ahead, product, first):
+    tokens, half = peer.shape
     channels = weight.shape[1]
-    experts, rows, _ = share.shape
+    owners, rows, _ = share.shape
+    out_shape = (2 * owners, rows, 2 * channels + 128)
     return pl.pallas_call(
         scan_kernel,
         grid_spec=pltpu.PrefetchScalarGridSpec(
@@ -578,19 +626,20 @@
             grid=(1,),
             in_specs=[
                 whole((tokens, half)),
-                whole((tokens, half)),
-                whole(weight.shape),
+                pl.BlockSpec((half, channels), lambda i, c: (1 - c[0], 0)),
+                whole((tokens, channels)),
+                whole((tokens, channels)),
+                whole(share.shape),
                 whole((tokens, channels)),
                 whole((tokens, channels)),
                 whole(ahead.shape),
                 whole(ahead.shape),
                 whole((16, channels)),
-                whole(share.shape),
             ],
             out_specs=[
                 whole((tokens, channels)),
                 whole(ahead.shape),
-                whole((experts, rows, channels + 128)),
+                whole(out_shape),
                 whole((16, channels)),
             ],
             scratch_shapes=[pltpu.VMEM(ahead.shape, f32)],
@@ -598,7 +647,7 @@
         out_shape=[
             jax.ShapeDtypeStruct((tokens, channels), f32),
             jax.ShapeDtypeStruct(ahead.shape, f32),
-            jax.ShapeDtypeStruct((experts, rows, channels + 128), bf16),
+            jax.ShapeDtypeStruct(out_shape, bf16),
             jax.ShapeDtypeStruct((16, channels), f32),
         ],
         compiler_params=params(),
@@ -606,37 +655,7 @@
             flops=4 * tokens * half * channels, transcendentals=0, bytes_accessed=9 << 20
         ),
         name="scan",
-    )(core, own, peer, weight, slope, gelu, ahead, product, first, share)
-
-
-def project_kernel(core_ref, own_ref, peer_ref, mixed_ref, early_ref, late_ref):
-    core = core_ref[0]
-    mixed = mixed_ref[...]
-    owners, rows, channels = early_ref.shape
-    share = owners // 2
-    for ref, place in ((own_ref, core), (peer_ref, 1 - core)):
-        value = dot(ref[...], mixed, outer).astype(bf16).reshape(share, 2 * rows, channels)
-        at = pl.ds(pl.multiple_of(place * share, share), share)
-        early_ref[at] = value[:, 0:rows]
-        late_ref[at] = value[:, rows:]
-
-
-def project(core, own, peer, mixed, owners):
-    tokens, half = own.shape
-    channels = mixed.shape[1]
-    shape = (owners, half // owners, channels)
-    return pl.pallas_call(
-        project_kernel,
-        grid_spec=pltpu.PrefetchScalarGridSpec(
-            num_scalar_prefetch=1,
-            grid=(1,),
-            in_specs=[whole((tokens, half)), whole((tokens, half)), whole((tokens, channels))],
-            out_specs=[whole(shape), whole(shape)],
-        ),
-        out_shape=[jax.ShapeDtypeStruct(shape, bf16)] * 2,
-        compiler_params=params(),
-        name="project",
-    )(core, own, peer, mixed)
+    )(core, peer, weight, mixed, part, share, slope, gelu, ahead, product, first)
 
 
 def tail_kernel(
@@ -691,7 +710,7 @@
     cube = pl.BlockSpec((1, tokens, span), lambda i, c: (i, 0, 0))
     col = lambda rows: pl.BlockSpec((rows, span), lambda i, c: (0, i))
     block = pl.BlockSpec((1, span, span), lambda i, c: (i, 0, 0))
-    line = pl.BlockSpec((owners, rows, 128), lambda i, c: (0, 0, channels // 128))
+    line = pl.BlockSpec((owners, rows, 128), lambda i, c: (0, 0, 2 * channels // 128))
     return pl.pallas_call(
         tail_kernel,
         grid_spec=pltpu.PrefetchScalarGridSpec(
@@ -754,7 +773,6 @@
         jnp.concatenate([in_x[tokens - taps + 1 :], state[tokens - 1 :]], axis=0), "sp", 1
     )
     outgoing, target = send(core, routes.T, route_weight.T, cotangent, experts)
-    outgoing, edge = lax.optimization_barrier((outgoing, edge))
     arrived = exchange(outgoing, "sp")
     target = target.T
 
@@ -778,24 +796,18 @@
 
     stream_own = combine(core, returned, target, cotangent)
     stream_peer = swapped(stream_own)
-    early, late = project(core, stream_own, stream_peer, mixed, experts)
-    early_shares = exchange(early, "sp")
-    grad_y, local, late, head = scan(
-        core, stream_own, stream_peer, out_weight, y_slope, gelu, ahead, product, first, late
+    part, share = own_part(core, stream_own, out_weight, mixed, experts)
+    grad_y, local, outgoing, head = scan(
+        core, stream_peer, out_weight, mixed, part, share, y_slope, gelu, ahead, product, first
     )
     head = shifted(head, "sp", -1)
-    late_shares = exchange(late, "sp")
+    shares = exchange(outgoing, "sp")
     grad_x = tail(
-        place, late_shares, head, local, product, keep_part, input_part, direct,
+        place, shares, head, local, product, keep_part, input_part, direct,
         gate_a, gate_x, conv_taps,
     )
-    grad_proj = jnp.concatenate(
-        [
-            jnp.sum(early_shares.astype(f32), axis=0),
-            jnp.sum(late_shares[:, :, :channels].astype(f32), axis=0),
-        ],
-        axis=0,
-    )
+    summed = jnp.sum(shares[:, :, : 2 * channels].astype(f32), axis=0)
+    grad_proj = jnp.concatenate([summed[:, :channels], summed[:, channels:]], axis=0)
     return (grad_gate[None], grad_up[None], grad_down[None], grad_proj, grad_x, grad_y)
 
 

time: 214 us -> 183 us (0.86)
  Pallas kernels: 82.2 us -> 45 us
  local copies, waits for them, and re-layouts: 6.52 us -> 21.5 us
  starting transfers between devices: 29.4 us -> 20.4 us
    unnamed x18 -> x74, local copies, waits for them, and re-layouts: 4.3 us -> 21.4 us
    all_to_all x3 -> x2, starting transfers between devices: 19.4 us -> 10.8 us  [exchange(): return lax.all_to_all(value, axis, split_axis=0, concat_axis=0, tiled=True)]
    ppermute x2, waiting for transfers between devices: 0.46 us -> 7.46 us  [shifted(): return lax.ppermute(value, axis, pairs)]
    all_to_all x3 -> x2, waiting for transfers between devices: 43.7 us -> 37.8 us  [exchange(): return lax.all_to_all(value, axis, split_axis=0, concat_axis=0, tiled=True)]
    pallas_call x1, Pallas kernels: 11.9 us -> 6.91 us  [expert_pre(): pl.pallas_call(expert_pre_kernel, grid=(count // size,), in_specs=[by_row...]
    pallas_call x1, Pallas kernels: 9.76 us -> 5.03 us  [far(): pl.pallas_call(far_kernel, grid_spec=pltpu.PrefetchScalarGridSpec(num_sca...]
    pallas_call x1, Pallas kernels: 6.28 us -> 1.9 us  [scan(): pl.pallas_call(scan_kernel, grid_spec=pltpu.PrefetchScalarGridSpec(num_sc...]
    pallas_call x1, Pallas kernels: 5.3 us -> 2.16 us  [near(): pl.pallas_call(near_kernel, grid_spec=pltpu.PrefetchScalarGridSpec(num_sc...]
  transfers between devices with their start and end apart: 8 -> 7, of which waited for: 4 -> 4; matrix products, arithmetic and copies ran while one was open for 1% -> 1% of each run, Pallas kernels for 24% -> 16%
where the time goes in v2:
time: 183 us; the launch traced here: 180 us
  waiting for transfers between devices  46.1 us (25%)
  Pallas kernels  45 us (25%)
  blocking collectives  43.2 us (24%)
  local copies, waits for them, and re-layouts  21.5 us (12%)
  starting transfers between devices  20.4 us (11%)
  other arithmetic  2.92 us (2%)
    all_to_all x1, blocking collectives, exchange(): return lax.all_to_all(value, axis, split_axis=0, concat_axis=0, tiled=True)  43.2 us
    all_to_all x2, waiting for transfers between devices, exchange(): return lax.all_to_all(value, axis, split_axis=0, concat_axis=0, tiled=True)  37.8 us
    unnamed x74, local copies, waits for them, and re-layouts  21.4 us
    all_to_all x2, starting transfers between devices, exchange(): return lax.all_to_all(value, axis, split_axis=0, concat_axis=0, tiled=True)  10.8 us
    ppermute x2, starting transfers between devices, shifted(): return lax.ppermute(value, axis, pairs)  8.94 us
    ppermute x2, waiting for transfers between devices, shifted(): return lax.ppermute(value, axis, pairs)  7.46 us
    pallas_call x1, Pallas kernels, grad_in(): pl.pallas_call(grad_in_kernel, grid=(model // size,), in_specs=[pl.BlockS...  7.42 us
    pallas_call x1, Pallas kernels, expert_pre(): pl.pallas_call(expert_pre_kernel, grid=(count // size,), in_specs=[by_row...  6.91 us
  transfers between devices with their start and end apart: 7, of which 4 were waited for; matrix products, arithmetic and copies ran while one was open for 1% of the time, Pallas kernels for 16%

profile of v2, /device:TPU:32, one launch (start us, length us, event | category | flops | bytes accessed | tf_op | source)
XLA Modules:
  0.0 180.3 jit_solution(17872326089952521740)
XLA Ops:
  0.6 0.0 copy-start.1
  0.6 1.4 copy-done.1
  2.1 0.7 copy-done.21
  2.7 0.7 copy-done.22
  3.4 3.4 %send.1 = (bf16[64,16,1152]{2,1,0:T(8,128)(2,1)S(1)}, s32[8,384]{1,0:T(8,128)S(1)}) custom-call(s32[1]{0:T(128)} %bitcast.3.core_ref, s32[2,384]{1,0:T(2,128)S(1)} %bitcast.22, f32[2,384]{1,0:T(2,128)S(1)} %bitcast.23, bf16[384,2048]{1,0:T(8,128)(2,1)S(1)} %copy-done.1), custom_call_target="tpu_custom_call" | custom-call | tf_op jit(solution)/shard_map/send/pallas_call | solution.py:102
  6.8 0.0 copy-start.5
  6.9 43.2 %all_to_all.15.block_ref = bf16[64,16,1152]{2,1,0:T(8,128)(2,1)S(1)} all-to-all(bf16[64,16,1152]{2,1,0:T(8,128)(2,1)S(1)} %get-tuple-element.36), channel_id=1, replica_groups=mesh['sp'=64,'tp'=2] {'sp'}, dimensions={0} | all-to-all | bytes 4718592 | tf_op jit(solution)/shard_map/all_to_all | solution.py:734
  50.1 2.3 %copy-done.24 = bf16[1,1152,2048]{2,1,0:T(8,128)(2,1)S(1)} copy-done((bf16[1,1152,2048]{2,1,0:T(8,128)(2,1)S(1)}, bf16[1,1152,2048]{2,1,0:T(8,128)(2,1)}, u32[]{:S(2)}) %copy-start.24) | copy-done | bytes 4718616
  52.4 6.9 %expert_pre.1 = (bf16[1152,2048]{1,0:T(8,128)(2,1)S(1)}, f32[1152,512]{1,0:T(8,128)S(1)}, f32[1152,512]{1,0:T(8,128)S(1)}, bf16[1152,512]{1,0:T(8,128)(2,1)S(1)}) custom-call(bf16[1152,2048]{1,0:T(8,128)(2,1)S(1)} %bitcast.25, bf16[2048,512]{1,0:T(8,128)(2,1)S(1)} %bitcast.15, bf16[2048,512]{1,0:T(8,128)(2,1)S(1)} %bitcast.18), custom_call_target="tpu_custom_call" | custom-call | flops 4831838208 | bytes 20971520 | tf_op jit(solution)/shard_map/expert_pre/pallas_call | solution.py:160
  59.4 2.2 %copy-done.35 = bf16[1152,2048]{1,0:T(8,128)(2,1)} copy-done((bf16[1152,2048]{1,0:T(8,128)(2,1)}, bf16[1152,2048]{1,0:T(8,128)(2,1)S(1)}, u32[]{:S(2)}) %copy-start.35) | copy-done | bytes 4718616
  61.5 2.2 %near.1 = (bf16[1152,1024]{1,0:T(8,128)(2,1)S(1)}, f32[1152,512]{1,0:T(8,128)S(1)}) custom-call(s32[1]{0:T(128)} %bitcast.3.core_ref, bf16[64,16,1152]{2,1,0:T(8,128)(2,1)S(1)} %all_to_all.15.block_ref, bf16[512,2048]{1,0:T(8,128)(2,1)S(1)} %bitcast.13), custom_call_target="tpu_custom_call" | custom-call | flops 1207959552 | bytes 9437184 | tf_op jit(solution)/shard_map/near/pallas_call | solution.py:302
  63.7 1.4 copy-done.31
  65.1 5.0 %far.1 = (bf16[1152,1024]{1,0:T(8,128)(2,1)S(1)}, bf16[1152,512]{1,0:T(8,128)(2,1)S(1)}, bf16[1152,512]{1,0:T(8,128)(2,1)S(1)}, bf16[64,16,1152]{2,1,0:T(8,128)(2,1)S(1)}) custom-call(s32[1]{0:T(128)} %bitcast.3.core_ref, bf16[64,16,1152]{2,1,0:T(8,128)(2,1)S(1)} %collective-permute-done.block_ref, bf16[512,2048]{1,0:T(8,128)(2,1)S(1)} %bitcast.14, ...), custom_call_target="tpu_custom_call" | custom-call | flops 3623878656 | bytes 16777216 | tf_op jit(solution)/shard_map/far/pallas_call | solution.py:353
  70.2 0.6 collective-permute-start.1
  70.8 3.3 %back_own.1 = bf16[64,16,1152]{2,1,0:T(8,128)(2,1)S(1)} custom-call(s32[1]{0:T(128)} %bitcast.3.core_ref, bf16[1152,512]{1,0:T(8,128)(2,1)S(1)} %get-tuple-element.40.gate_adj_ref, bf16[1152,512]{1,0:T(8,128)(2,1)S(1)} %get-tuple-element.41.up_adj_ref, bf16[2048,512]{1,0:T(8,128)(2,1)S(1)} %bitcast.17, bf16[2048,512]{1,0:T(8,128)(2,1)S(1)} %bitcast.20), custom_call_target="tpu_custom_call" | custom-call | flops 2415919104 | bytes 7340032 | tf_op jit(solution)/shard_map/back_own/pallas_call | solution.py:396
  74.1 0.8 collective-permute-done.1
  74.9 2.0 %add_convert_fusion = bf16[64,16,1152]{2,1,0:T(8,128)(2,1)} fusion(bf16[64,16,1152]{2,1,0:T(8,128)(2,1)S(1)} %collective-permute-done.1, bf16[64,16,1152]{2,1,0:T(8,128)(2,1)S(1)} %back_own.1), kind=kLoop, calls=%fused_computation | loop fusion | flops 4718592 | bytes 7077888 | tf_op jit(solution)/shard_map/convert_element_type | solution.py:791
  76.9 6.4 %all-to-all-start.1 = ((bf16[64,16,1152]{2,1,0:T(8,128)(2,1)}), bf16[64,16,1152]{2,1,0:T(8,128)(2,1)S(1)}, u32[]{:S(2)}, u32[]{:S(2)}) async-start(bf16[64,16,1152]{2,1,0:T(8,128)(2,1)} %add_convert_fusion), calls=%async_computation.1 | async-start | bytes 4718592 | tf_op jit(solution)/shard_map/all_to_all | solution.py:734
  83.2 0.1 copy.21
  83.4 32.2 %all-to-all-done.1.block_ref = bf16[64,16,1152]{2,1,0:T(8,128)(2,1)S(1)} async-done(((bf16[64,16,1152]{2,1,0:T(8,128)(2,1)}), bf16[64,16,1152]{2,1,0:T(8,128)(2,1)S(1)}, u32[]{:S(2)}, u32[]{:S(2)}) %all-to-all-start.1) | async-done | bytes 2359328 | tf_op jit(solution)/shard_map/all_to_all | solution.py:734
  115.6 1.4 copy-done.2
  117.1 3.4 %combine.1.own_ref = bf16[384,1024]{1,0:T(8,128)(2,1)S(1)} custom-call(s32[1]{0:T(128)} %bitcast.3.core_ref, bf16[64,16,1152]{2,1,0:T(8,128)(2,1)S(1)} %all-to-all-done.1.block_ref, s32[384,8]{1,0:T(8,128)S(1)} %bitcast.21, bf16[384,2048]{1,0:T(8,128)(2,1)S(1)} %copy-done.2), custom_call_target="tpu_custom_call" | custom-call | tf_op jit(solution)/shard_map/combine/pallas_call | solution.py:503
  120.5 0.1 collective-permute-start.2
  120.6 2.3 %collective-permute-start.3 = (bf16[4,512]{1,0:T(4,128)(2,1)S(1)}, bf16[4,512]{1,0:T(4,128)(2,1)S(1)}, u32[]{:S(2)}, u32[]{:S(2)}) collective-permute-start(bf16[4,512]{1,0:T(4,128)(2,1)S(1)} %pad_maximum_fusion.1), channel_id=1, source_target_pairs={{0,2},{2,4},{4,6},{6,8},{8,10},{10,12},{12,14},{14,16},{16,18},{18... | collective-permute-start | bytes 12296 | tf_op jit(solution)/shard_map/ppermute | solution.py:744
  122.9 7.5 %collective-permute-done.3.edge_ref = bf16[4,512]{1,0:T(4,128)(2,1)S(1)} collective-permute-done((bf16[4,512]{1,0:T(4,128)(2,1)S(1)}, bf16[4,512]{1,0:T(4,128)(2,1)S(1)}, u32[]{:S(2)}, u32[]{:S(2)}) %collective-permute-start.3) | collective-permute-done | bytes 4128 | tf_op jit(solution)/shard_map/ppermute | solution.py:744
  130.4 3.2 %recur_pre.1 = (bf16[384,512]{1,0:T(8,128)(2,1)S(1)}, f32[384,512]{1,0:T(8,128)S(1)}, f32[384,512]{1,0:T(8,128)S(1)}, f32[4,384,128]{2,1,0:T(8,128)S(1)}, f32[4,...) custom-call(bf16[384,512]{1,0:T(8,128)(2,1)S(1)} %copy-done.17, ...), custom_call_target="tpu_custom_call" | custom-call | flops 393216000 | bytes 8388608 | tf_op jit(solution)/shard_map/recur_pre/pallas_call | solution.py:247
  133.7 1.1 own_part.1
  134.8 0.0 copy-done.9
  134.8 0.2 copy-done.11
  135.1 1.9 %scan.1 = (f32[384,512]{1,0:T(8,128)}, f32[4,384,128]{2,1,0:T(8,128)S(1)}, bf16[64,16,1152]{2,1,0:T(8,128)(2,1)S(1)}, f32[16,512]{1,0:T(8,128)S(1)}) custom-call(s32[1]{0:T(128)} %bitcast.3.core_ref, bf16[384,1024]{1,0:T(8,128)(2,1)S(1)} %collective-permute-done.2.peer_ref, bf16[2048,512]{1,0:T(8,128)(2,1)S(1)} %copy-done, ...), custom_call_target="tpu_custom_call" | custom-call | flops 805306368 | bytes 9437184 | tf_op jit(solution)/shard_map/scan/pallas_call | solution.py:622
  137.0 1.4 copy-done.3
  138.3 0.9 copy-done.13
  139.2 4.5 %all-to-all-start.2 = ((bf16[64,16,1152]{2,1,0:T(8,128)(2,1)}), bf16[64,16,1152]{2,1,0:T(8,128)(2,1)S(1)}, u32[]{:S(2)}, u32[]{:S(2)}) async-start(bf16[64,16,1152]{2,1,0:T(8,128)(2,1)} %copy-done.3), calls=%async_computation.2 | async-start | bytes 4718592 | tf_op jit(solution)/shard_map/all_to_all | solution.py:734
  143.7 1.7 copy-done.26
  145.4 1.7 copy-done.32
  147.1 1.3 copy-done.34
  148.3 4.2 %grad_down.1 = bf16[512,2048]{1,0:T(8,128)(2,1)} custom-call(s32[1]{0:T(128)} %bitcast.3.core_ref, bf16[1152,512]{1,0:T(8,128)(2,1)S(1)} %copy-done.34, bf16[1152,1024]{1,0:T(8,128)(2,1)S(1)} %copy-done.32, bf16[1152,1024]{1,0:T(8,128)(2,1)S(1)} %copy-done.26), custom_call_target="tpu_custom_call" | custom-call | flops 2415919104 | bytes 9437184 | tf_op jit(solution)/shard_map/grad_down/pallas_call | solution.py:458
  152.6 2.3 %copy-done.36 = bf16[1152,2048]{1,0:T(8,128)(2,1)S(1)} copy-done((bf16[1152,2048]{1,0:T(8,128)(2,1)S(1)}, bf16[1152,2048]{1,0:T(8,128)(2,1)}, u32[]{:S(2)}) %copy-start.36) | copy-done | bytes 4718616
  154.9 7.4 %grad_in.1 = (bf16[2048,512]{1,0:T(8,128)(2,1)}, bf16[2048,512]{1,0:T(8,128)(2,1)}) custom-call(bf16[1152,2048]{1,0:T(8,128)(2,1)S(1)} %copy-done.36, bf16[1152,512]{1,0:T(8,128)(2,1)S(1)} %copy-done.28, bf16[1152,512]{1,0:T(8,128)(2,1)S(1)} %copy-done.30), custom_call_target="tpu_custom_call" | custom-call | flops 4831838208 | bytes 11534336 | tf_op jit(solution)/shard_map/grad_in/pallas_call | solution.py:425
  162.3 6.7 %collective-permute-start.4 = (f32[16,512]{1,0:T(8,128)S(1)}, f32[16,512]{1,0:T(8,128)S(1)}, u32[]{:S(2)}, u32[]{:S(2)}) collective-permute-start(f32[16,512]{1,0:T(8,128)S(1)} %get-tuple-element.58), channel_id=1, source_target_pairs={{2,0},{4,2},{6,4},{8,6},{10,8},{12,10},{14,12},{16,14},{18,16},{20... | collective-permute-start | bytes 98312 | tf_op jit(solution)/shard_map/ppermute | solution.py:744
  169.0 5.6 %all-to-all-done.2.line_ref = bf16[64,16,1152]{2,1,0:T(8,128)(2,1)S(1)} async-done(((bf16[64,16,1152]{2,1,0:T(8,128)(2,1)}), bf16[64,16,1152]{2,1,0:T(8,128)(2,1)S(1)}, u32[]{:S(2)}, u32[]{:S(2)}) %all-to-all-start.2) | async-done | bytes 2359328 | tf_op jit(solution)/shard_map/all_to_all | solution.py:734
  174.7 0.3 convert_reduce_fusion
  175.0 0.6 pad_maximum_fusion
  175.6 0.2 copy-done.8
  175.8 0.3 copy-done.10
  176.1 0.2 copy-done.12
  176.3 1.1 copy-done.14
  177.4 2.8 %tail.1 = f32[384,512]{1,0:T(8,128)} custom-call(s32[1]{0:T(128)} %bitcast.12.place_ref, bf16[64,16,1152]{2,1,0:T(8,128)(2,1)S(1)} %all-to-all-done.2.line_ref, f32[16,512]{1,0:T(8,128)S(1)} %collective-permute-done.4.head_ref, f32[4,384,128]{2,1,0:T(8,128)S(1)} %copy-done.14, f32[4,384,128]{2,1,0:T(8,128)S(1)} %get-tuple-element.55.product_ref, ...), custom_call_target="tpu_custom_call" | custom-call | tf_op jit(solution)/shard_map/tail/pallas_call | solution.py:714
  (61 shorter events, 0.2 us)
Async XLA Ops:
  0.6 1.4 copy-start.1
  2.0 0.7 copy-start.21
  2.7 0.7 copy-start.22
  6.8 43.2 %copy-start.5 = (bf16[1,2048,512]{2,1,0:T(8,128)(2,1)S(1)}, bf16[1,2048,512]{2,1,0:T(8,128)(2,1)}, u32[]{:S(2)}) copy-start(bf16[1,2048,512]{2,1,0:T(8,128)(2,1)} %param.19) | copy-start | bytes 6291460
  6.9 43.2 %copy-start.6 = (bf16[1,2048,512]{2,1,0:T(8,128)(2,1)S(1)}, bf16[1,2048,512]{2,1,0:T(8,128)(2,1)}, u32[]{:S(2)}) copy-start(bf16[1,2048,512]{2,1,0:T(8,128)(2,1)} %param.20) | copy-start | bytes 6291460
  50.1 15.0 %collective-permute-start = (bf16[64,16,1152]{2,1,0:T(8,128)(2,1)S(1)}, bf16[64,16,1152]{2,1,0:T(8,128)(2,1)S(1)}, u32[]{:S(2)}, u32[]{:S(2)}) collective-permute-start(bf16[64,16,1152]{2,1,0:T(8,128)(2,1)S(1)} %all_to_all.15.block_ref), channel_id=1, source_target_pairs={{0,1},{1,0},{2,3},{3,2},{4,5},{5,4},{6,7},{7,6},{8,9},{9,8},{10,11... | collective-permute-start | bytes 7077896 | tf_op jit(solution)/shard_map/ppermute | solution.py:738
  50.1 2.3 %copy-start.24 = (bf16[1,1152,2048]{2,1,0:T(8,128)(2,1)S(1)}, bf16[1,1152,2048]{2,1,0:T(8,128)(2,1)}, u32[]{:S(2)}) copy-start(bf16[1,1152,2048]{2,1,0:T(8,128)(2,1)} %param.18) | copy-start | bytes 14155780
  52.4 9.1 %copy-start.4 = (bf16[1,512,2048]{2,1,0:T(8,128)(2,1)S(1)}, bf16[1,512,2048]{2,1,0:T(8,128)(2,1)}, u32[]{:S(2)}) copy-start(bf16[1,512,2048]{2,1,0:T(8,128)(2,1)} %param.21) | copy-start | bytes 6291460
  59.4 2.2 %copy-start.35 = (bf16[1152,2048]{1,0:T(8,128)(2,1)}, bf16[1152,2048]{1,0:T(8,128)(2,1)S(1)}, u32[]{:S(2)}) copy-start(bf16[1152,2048]{1,0:T(8,128)(2,1)S(1)} %get-tuple-element.35.packed_ref) | copy-start | bytes 14155780
  61.5 3.6 %copy-start.33 = (bf16[1152,512]{1,0:T(8,128)(2,1)}, bf16[1152,512]{1,0:T(8,128)(2,1)S(1)}, u32[]{:S(2)}) copy-start(bf16[1152,512]{1,0:T(8,128)(2,1)S(1)} %get-tuple-element.44.active_ref) | copy-start | bytes 3538948
  63.7 1.4 copy-start.31
  70.1 3.9 %copy-start.25 = (bf16[1152,1024]{1,0:T(8,128)(2,1)}, bf16[1152,1024]{1,0:T(8,128)(2,1)S(1)}, u32[]{:S(2)}) copy-start(bf16[1152,1024]{1,0:T(8,128)(2,1)S(1)} %get-tuple-element.46.far_ref) | copy-start | bytes 7077892
  70.2 3.9 %copy-start.27 = (bf16[1152,512]{1,0:T(8,128)(2,1)}, bf16[1152,512]{1,0:T(8,128)(2,1)S(1)}, u32[]{:S(2)}) copy-start(bf16[1152,512]{1,0:T(8,128)(2,1)S(1)} %get-tuple-element.40.gate_adj_ref) | copy-start | bytes 3538948
  70.2 3.9 %copy-start.29 = (bf16[1152,512]{1,0:T(8,128)(2,1)}, bf16[1152,512]{1,0:T(8,128)(2,1)S(1)}, u32[]{:S(2)}) copy-start(bf16[1152,512]{1,0:T(8,128)(2,1)S(1)} %get-tuple-element.41.up_adj_ref) | copy-start | bytes 3538948
  70.2 4.7 %collective-permute-start.1 = (bf16[64,16,1152]{2,1,0:T(8,128)(2,1)S(1)}, bf16[64,16,1152]{2,1,0:T(8,128)(2,1)S(1)}, u32[]{:S(2)}, u32[]{:S(2)}) collective-permute-start(bf16[64,16,1152]{2,1,0:T(8,128)(2,1)S(1)} %get-tuple-element.47), channel_id=1, source_target_pairs={{0,1},{1,0},{2,3},{3,2},{4,5},{5,4},{6,7},{7,6},{8,9},{9,8},{10,11... | collective-permute-start | bytes 7077896 | tf_op jit(solution)/shard_map/ppermute | solution.py:738
  76.9 38.7 %all-to-all-start.1 = ((bf16[64,16,1152]{2,1,0:T(8,128)(2,1)}), bf16[64,16,1152]{2,1,0:T(8,128)(2,1)S(1)}, u32[]{:S(2)}, u32[]{:S(2)}) async-start(bf16[64,16,1152]{2,1,0:T(8,128)(2,1)} %add_convert_fusion), calls=%async_computation.1 | async-start | bytes 4718592 | tf_op jit(solution)/shard_map/all_to_all | solution.py:734
  115.6 1.4 copy-start.2
  117.0 3.6 %copy-start.18 = (bf16[384,512]{1,0:T(8,128)(2,1)S(1)}, bf16[384,512]{1,0:T(8,128)(2,1)}, u32[]{:S(2)}) copy-start(bf16[384,512]{1,0:T(8,128)(2,1)} %state_ref.1) | copy-start | bytes 1179652
  117.0 3.6 %copy-start.17 = (bf16[384,512]{1,0:T(8,128)(2,1)S(1)}, bf16[384,512]{1,0:T(8,128)(2,1)}, u32[]{:S(2)}) copy-start(bf16[384,512]{1,0:T(8,128)(2,1)} %x_ref.1) | copy-start | bytes 1179652
  117.0 13.3 %copy-start.15 = (bf16[4,128,128]{2,1,0:T(8,128)(2,1)S(1)}, bf16[4,128,128]{2,1,0:T(8,128)(2,1)}, u32[]{:S(2)}) copy-start(bf16[4,128,128]{2,1,0:T(8,128)(2,1)} %a_ref.3) | copy-start | bytes 393220
  117.0 13.3 %copy-start.16 = (bf16[4,128,128]{2,1,0:T(8,128)(2,1)S(1)}, bf16[4,128,128]{2,1,0:T(8,128)(2,1)}, u32[]{:S(2)}) copy-start(bf16[4,128,128]{2,1,0:T(8,128)(2,1)} %i_ref.3) | copy-start | bytes 393220
  117.0 13.3 %copy-start.19 = (bf16[384,512]{1,0:T(8,128)(2,1)S(1)}, bf16[384,512]{1,0:T(8,128)(2,1)}, u32[]{:S(2)}) copy-start(bf16[384,512]{1,0:T(8,128)(2,1)} %y_ref.1) | copy-start | bytes 1179652
  117.0 13.3 %copy-start.20 = (f32[4,512]{1,0:T(4,128)S(1)}, f32[4,512]{1,0:T(4,128)}, u32[]{:S(2)}) copy-start(f32[4,512]{1,0:T(4,128)} %taps_ref.3) | copy-start | bytes 24580
  117.0 13.3 %copy-start.23 = (f32[512]{0:T(512)S(1)}, f32[512]{0:T(512)}, u32[]{:S(2)}) copy-start(f32[512]{0:T(512)} %param.28) | copy-start | bytes 6148
  117.0 16.6 %copy-start = (bf16[2048,512]{1,0:T(8,128)(2,1)S(1)}, bf16[2048,512]{1,0:T(8,128)(2,1)}, u32[]{:S(2)}) copy-start(bf16[2048,512]{1,0:T(8,128)(2,1)} %weight_ref.3) | copy-start | bytes 6291460
  120.5 14.3 %collective-permute-start.2 = (bf16[384,1024]{1,0:T(8,128)(2,1)S(1)}, bf16[384,1024]{1,0:T(8,128)(2,1)S(1)}, u32[]{:S(2)}, u32[]{:S(2)}) collective-permute-start(bf16[384,1024]{1,0:T(8,128)(2,1)S(1)} %combine.1.own_ref), channel_id=1, source_target_pairs={{0,1},{1,0},{2,3},{3,2},{4,5},{5,4},{6,7},{7,6},{8,9},{9,8},{10,11... | collective-permute-start | bytes 2359304 | tf_op jit(solution)/shard_map/ppermute | solution.py:738
  120.6 9.7 %collective-permute-start.3 = (bf16[4,512]{1,0:T(4,128)(2,1)S(1)}, bf16[4,512]{1,0:T(4,128)(2,1)S(1)}, u32[]{:S(2)}, u32[]{:S(2)}) collective-permute-start(bf16[4,512]{1,0:T(4,128)(2,1)S(1)} %pad_maximum_fusion.1), channel_id=1, source_target_pairs={{0,2},{2,4},{4,6},{6,8},{8,10},{10,12},{12,14},{14,16},{16,18},{18... | collective-permute-start | bytes 12296 | tf_op jit(solution)/shard_map/ppermute | solution.py:744
  133.6 1.2 copy-start.7
  133.6 1.2 copy-start.9
  133.6 1.4 copy-start.11
  137.0 1.4 copy-start.3
  138.3 0.9 copy-start.13
  139.2 35.5 %all-to-all-start.2 = ((bf16[64,16,1152]{2,1,0:T(8,128)(2,1)}), bf16[64,16,1152]{2,1,0:T(8,128)(2,1)S(1)}, u32[]{:S(2)}, u32[]{:S(2)}) async-start(bf16[64,16,1152]{2,1,0:T(8,128)(2,1)} %copy-done.3), calls=%async_computation.2 | async-start | bytes 4718592 | tf_op jit(solution)/shard_map/all_to_all | solution.py:734
  143.7 1.7 copy-start.26
  145.4 1.7 copy-start.32
  147.1 1.3 copy-start.34
  148.3 4.2 %copy-start.28 = (bf16[1152,512]{1,0:T(8,128)(2,1)S(1)}, bf16[1152,512]{1,0:T(8,128)(2,1)}, u32[]{:S(2)}) copy-start(bf16[1152,512]{1,0:T(8,128)(2,1)} %copy-done.27) | copy-start | bytes 3538948
  148.3 4.3 %copy-start.30 = (bf16[1152,512]{1,0:T(8,128)(2,1)S(1)}, bf16[1152,512]{1,0:T(8,128)(2,1)}, u32[]{:S(2)}) copy-start(bf16[1152,512]{1,0:T(8,128)(2,1)} %copy-done.29) | copy-start | bytes 3538948
  152.6 2.3 %copy-start.36 = (bf16[1152,2048]{1,0:T(8,128)(2,1)S(1)}, bf16[1152,2048]{1,0:T(8,128)(2,1)}, u32[]{:S(2)}) copy-start(bf16[1152,2048]{1,0:T(8,128)(2,1)} %copy-done.35) | copy-start | bytes 14155780
  162.3 13.3 %collective-permute-start.4 = (f32[16,512]{1,0:T(8,128)S(1)}, f32[16,512]{1,0:T(8,128)S(1)}, u32[]{:S(2)}, u32[]{:S(2)}) collective-permute-start(f32[16,512]{1,0:T(8,128)S(1)} %get-tuple-element.58), channel_id=1, source_target_pairs={{2,0},{4,2},{6,4},{8,6},{10,8},{12,10},{14,12},{16,14},{18,16},{20... | collective-permute-start | bytes 98312 | tf_op jit(solution)/shard_map/ppermute | solution.py:744
  174.7 1.1 copy-start.8
  174.7 1.4 copy-start.10
  174.7 1.6 copy-start.12
  176.3 1.1 copy-start.14

commit v3 on v2

--- a/solution.py
+++ b/solution.py
@@ -30,6 +30,10 @@
 
 def params(n=1, mb=32):
     return pltpu.CompilerParams(dimension_semantics=("arbitrary",) * n, vmem_limit_bytes=mb << 20)
+
+
+def held(value):
+    return pltpu.with_memory_space_constraint(value, pltpu.HBM)
 
 
 def whole(shape):
@@ -116,12 +120,12 @@
             scratch_shapes=[pltpu.VMEM((8, tokens), jnp.int32), pltpu.VMEM((128, 128), f32)],
         ),
         out_shape=[
-            jax.ShapeDtypeStruct((experts, main, half + 128), bf16),
+            pltpu.HBM((experts, main, half + 128), bf16),
             jax.ShapeDtypeStruct((8, tokens), jnp.int32),
         ],
         compiler_params=params(),
         name="send",
-    )(core, routes, weight, cotangent)
+    )(core, held(routes), held(weight), held(cotangent))
 
 
 pair = 2
@@ -163,17 +167,17 @@
         in_specs=[by_row(model), whole((model, hidden)), whole((model, hidden))],
         out_specs=[by_row(model), by_row(hidden), by_row(hidden), by_row(hidden)],
         out_shape=[
-            jax.ShapeDtypeStruct((count, model), bf16),
-            jax.ShapeDtypeStruct((count, hidden), f32),
-            jax.ShapeDtypeStruct((count, hidden), f32),
-            jax.ShapeDtypeStruct((count, hidden), bf16),
+            pltpu.HBM((count, model), bf16),
+            pltpu.HBM((count, hidden), f32),
+            pltpu.HBM((count, hidden), f32),
+            pltpu.HBM((count, hidden), bf16),
         ],
         compiler_params=params(),
         cost_estimate=pl.CostEstimate(
             flops=4 * count * model * hidden, transcendentals=0, bytes_accessed=20 << 20
         ),
         name="expert_pre",
-    )(rows, gate, up)
+    )(held(rows), held(gate), held(up))
 
 
 def recur_pre_kernel(
@@ -243,24 +247,24 @@
     col = lambda rows: pl.BlockSpec((rows, span), lambda i: (0, i))
     block = pl.BlockSpec((1, span, span), lambda i: (i, 0, 0))
     cube = pl.BlockSpec((1, tokens, span), lambda i: (i, 0, 0))
-    big = jax.ShapeDtypeStruct((tokens, channels), f32)
+    big = pltpu.HBM((tokens, channels), f32)
     return pl.pallas_call(
         recur_pre_kernel,
         grid=(blocks,),
         in_specs=[col(tokens), col(tokens), col(tokens), col(4), col(4), block, block, col(1)],
         out_specs=[col(tokens)] * 3 + [cube] * 2 + [col(tokens)] * 3 + [col(16)],
-        out_shape=[jax.ShapeDtypeStruct((tokens, channels), bf16)]
+        out_shape=[pltpu.HBM((tokens, channels), bf16)]
         + [big] * 2
-        + [jax.ShapeDtypeStruct((blocks, tokens, span), f32)] * 2
+        + [pltpu.HBM((blocks, tokens, span), f32)] * 2
         + [big] * 3
-        + [jax.ShapeDtypeStruct((16, channels), f32)],
+        + [pltpu.HBM((16, channels), f32)],
         scratch_shapes=[pltpu.VMEM((tokens + 16, span), f32)],
         compiler_params=params(),
         cost_estimate=pl.CostEstimate(
             flops=2000 * tokens * channels, transcendentals=0, bytes_accessed=8 << 20
         ),
         name="recur_pre",
-    )(in_x, in_y, state, edge, taps, gate_a, gate_x, rate)
+    )(held(in_x), held(in_y), held(state), held(edge), held(taps), held(gate_a), held(gate_x), held(rate))
 
 
 def unpack(block, scratch):
@@ -287,9 +291,8 @@
         )
 
 
-def near_kernel(core_ref, block_ref, down_ref, rows_ref, part_ref, scratch):
+def near_kernel(core_ref, block_ref, down_ref, part_ref, scratch):
     rows = unpack(block_ref[...], scratch)
-    rows_ref[...] = rows
     part_ref[...] = dot(rows, down_ref[...], inner)
 
 
@@ -308,30 +311,23 @@
                 pl.BlockSpec((pair * group, main, wide), lambda i, c: (i, 0, 0)),
                 pl.BlockSpec((hidden, half), lambda i, c: (0, c[0])),
             ],
-            out_specs=[
-                pl.BlockSpec((size, half), lambda i, c: (i, 0)),
-                pl.BlockSpec((size, hidden), lambda i, c: (i, 0)),
-            ],
+            out_specs=pl.BlockSpec((size, hidden), lambda i, c: (i, 0)),
             scratch_shapes=[pltpu.VMEM((128, 128), f32)],
         ),
-        out_shape=[
-            jax.ShapeDtypeStruct((count, half), bf16),
-            jax.ShapeDtypeStruct((count, hidden), f32),
-        ],
+        out_shape=jax.ShapeDtypeStruct((count, hidden), f32),
         compiler_params=params(),
         cost_estimate=pl.CostEstimate(
             flops=2 * count * half * hidden, transcendentals=0, bytes_accessed=9 << 20
         ),
         name="near",
-    )(core, arrived, down)
+    )(core, arrived, held(down))
 
 
 def far_kernel(
     core_ref, block_ref, down_ref, part_ref, silu_ref, slope_ref, gate_ref, up_ref,
-    rows_ref, gate_adj_ref, up_adj_ref, back_ref, scratch,
+    gate_adj_ref, up_adj_ref, back_ref, scratch,
 ):
     rows = unpack(block_ref[...], scratch)
-    rows_ref[...] = rows
     grad = part_ref[...] + dot(rows, down_ref[...], inner)
     gate_adj = (grad * slope_ref[...]).astype(bf16)
     up_adj = (grad * silu_ref[...]).astype(bf16)
@@ -364,11 +360,10 @@
                 weight,
                 weight,
             ],
-            out_specs=[by_row(half), by_row(hidden), by_row(hidden), block],
+            out_specs=[by_row(hidden), by_row(hidden), block],
             scratch_shapes=[pltpu.VMEM((128, 128), f32)],
         ),
         out_shape=[
-            jax.ShapeDtypeStruct((count, half), bf16),
             jax.ShapeDtypeStruct((count, hidden), bf16),
             jax.ShapeDtypeStruct((count, hidden), bf16),
             jax.ShapeDtypeStruct(arrived.shape, bf16),
@@ -378,7 +373,7 @@
             flops=6 * count * half * hidden, transcendentals=0, bytes_accessed=16 << 20
         ),
         name="far",
-    )(core, arrived, down, part, silu, slope, gate, up)
+    )(core, arrived, held(down), part, silu, slope, held(gate), held(up))
 
 
 def back_kernel(core_ref, gate_adj_ref, up_adj_ref, gate_ref, up_ref, back_ref, scratch):
@@ -408,7 +403,7 @@
             flops=4 * count * half * hidden, transcendentals=0, bytes_accessed=7 << 20
         ),
         name="back_own",
-    )(core, gate_adj, up_adj, gate, up)
+    )(core, gate_adj, up_adj, held(gate), held(up))
 
 
 def grad_in_kernel(packed_ref, gate_adj_ref, up_adj_ref, gate_ref, up_ref):
@@ -437,31 +432,32 @@
             flops=4 * count * model * hidden, transcendentals=0, bytes_accessed=11 << 20
         ),
         name="grad_in",
-    )(packed, gate_adj, up_adj)
-
-
-def grad_down_kernel(core_ref, active_ref, near_ref, far_ref, out_ref):
+    )(held(packed), held(gate_adj), held(up_adj))
+
+
+def grad_down_kernel(core_ref, active_ref, near_ref, far_ref, out_ref, scratch):
     active = active_ref[...]
 
     @pl.when(pl.program_id(0) == 0)
     def _():
-        out_ref[...] = dot(active, near_ref[...], outer).astype(bf16)
+        out_ref[...] = dot(active, unpack(near_ref[...], scratch), outer).astype(bf16)
 
     @pl.when(pl.program_id(0) == 1)
     def _():
-        out_ref[...] = dot(active, far_ref[...], outer).astype(bf16)
-
-
-def grad_down_of(core, active, near_rows, far_rows):
+        out_ref[...] = dot(active, unpack(far_ref[...], scratch), outer).astype(bf16)
+
+
+def grad_down_of(core, active, arrived, arrived_far):
     count, hidden = active.shape
-    half = near_rows.shape[1]
+    half = arrived.shape[2] - 128
     return pl.pallas_call(
         grad_down_kernel,
         grid_spec=pltpu.PrefetchScalarGridSpec(
             num_scalar_prefetch=1,
             grid=(2,),
-            in_specs=[whole((count, hidden)), whole((count, half)), whole((count, half))],
+            in_specs=[whole((count, hidden)), whole(arrived.shape), whole(arrived.shape)],
             out_specs=pl.BlockSpec((hidden, half), lambda i, c: (0, i + c[0] - 2 * i * c[0])),
+            scratch_shapes=[pltpu.VMEM((128, 128), f32)],
         ),
         out_shape=jax.ShapeDtypeStruct((hidden, 2 * half), bf16),
         compiler_params=params(),
@@ -469,7 +465,7 @@
             flops=4 * count * half * hidden, transcendentals=0, bytes_accessed=9 << 20
         ),
         name="grad_down",
-    )(core, active, near_rows, far_rows)
+    )(core, held(active), held(arrived), held(arrived_far))
 
 
 def combine_kernel(core_ref, block_ref, target_ref, cot_ref, out_ref, total, scratch):
@@ -516,7 +512,7 @@
         out_shape=jax.ShapeDtypeStruct((tokens, half), bf16),
         compiler_params=params(),
         name="combine",
-    )(core, returned, target, cotangent)
+    )(core, returned, held(target), held(cotangent))
 
 
 def two_terms(value):
@@ -568,50 +564,63 @@
 def scan_kernel(
     core_ref, peer_ref, weight_ref, mixed_ref, part_ref, share_ref, slope_ref, gelu_ref, ahead_ref,
     product_ref, first_ref,
-    grad_y_ref, local_ref, out_ref, head_ref, scratch,
+    grad_y_out, local_out, share_out, head_out,
+    state_grad, grad_y, local, peer_share, lines, head, sems,
 ):
     tokens, _ = peer_ref.shape
     channels = weight_ref.shape[1]
     core = core_ref[0]
+    owners = share_ref.shape[0]
+    own_at = pl.ds(pl.multiple_of(core * owners, owners), owners)
+    peer_at = pl.ds(pl.multiple_of((1 - core) * owners, owners), owners)
+    waits = []
+
+    def copy_out(source, target):
+        copy = pltpu.make_async_copy(source, target, sems.at[len(waits)])
+        copy.start()
+        waits.append(copy)
+
+    copy_out(share_ref, share_out.at[own_at, :, pl.ds(0, 2 * channels)])
     peer = peer_ref[...]
     grad = part_ref[...] + dot(peer, weight_ref[...], plain)
-    grad_y_ref[...] = grad * slope_ref[...]
-    state_grad = grad * gelu_ref[...]
+    grad_y[...] = grad * slope_ref[...]
+    copy_out(grad_y, grad_y_out)
+    values = grad * gelu_ref[...]
     length = tokens // segments
-    blocks = scratch.shape[0]
+    blocks = state_grad.shape[0]
     for b in range(blocks):
-        scratch[b] = state_grad[:, 128 * b : 128 * (b + 1)]
-    owners = share_ref.shape[0]
-    left, right = share_rows(dot(peer, mixed_ref[...], outer), owners)
-    own_at = pl.ds(pl.multiple_of(core * owners, owners), owners)
-    peer_at = pl.ds(pl.multiple_of((1 - core) * owners, owners), owners)
-    out_ref[own_at, :, 0 : 2 * channels] = share_ref[...]
-    out_ref[peer_at, :, 0:channels] = left
-    out_ref[peer_at, :, channels : 2 * channels] = right
+        state_grad[b] = values[:, 128 * b : 128 * (b + 1)]
     carries = []
     for b in range(blocks):
         at = slice(128 * b, 128 * (b + 1))
         value = None
         for j in reversed(range(length)):
-            here = scratch[b, pl.ds(j, segments, stride=length), :]
+            here = state_grad[b, pl.ds(j, segments, stride=length), :]
             if value is None:
                 value = here
             else:
                 value = here + ahead_ref[b, pl.ds(j, segments, stride=length), :] * value
-            local_ref[b, pl.ds(j, segments, stride=length), :] = value
+            local[b, pl.ds(j, segments, stride=length), :] = value
         product = product_ref[b, pl.ds(0, segments, stride=length), :]
         carry = value[segments - 1 : segments]
         for s in reversed(range(1, segments - 1)):
             carry = value[s : s + 1] + product[s : s + 1] * carry
-        ends = local_ref[b, 0:3, :] + product_ref[b, 0:3, :] * carry
+        ends = local[b, 0:3, :] + product_ref[b, 0:3, :] * carry
         carries.append(first_ref[0:1, at] * ends[0:1])
-        head_ref[:, at] = jnp.concatenate(
-            [ends, first_ref[3:15, at], jnp.zeros((1, 128), f32)], axis=0
-        )
+        head[:, at] = jnp.concatenate([ends, first_ref[3:15, at], jnp.zeros((1, 128), f32)], axis=0)
     decay = jnp.concatenate([first_ref[1:2, 128 * b : 128 * (b + 1)] for b in range(blocks)], axis=0)
     terms = two_terms(decay) + two_terms(jnp.concatenate(carries, axis=0))
     line = jnp.concatenate([term.astype(f32) for term in terms], axis=0).astype(bf16)
-    out_ref[:, :, 2 * channels :] = jnp.broadcast_to(line[None], (out_ref.shape[0], *line.shape))
+    lines[...] = jnp.broadcast_to(line[None], lines.shape)
+    copy_out(lines, share_out.at[:, :, pl.ds(2 * channels, 128)])
+    copy_out(local, local_out)
+    copy_out(head, head_out)
+    left, right = share_rows(dot(peer, mixed_ref[...], outer), owners)
+    peer_share[:, :, 0:channels] = left
+    peer_share[:, :, channels : 2 * channels] = right
+    copy_out(peer_share, share_out.at[peer_at, :, pl.ds(0, 2 * channels)])
+    for copy in waits:
+        copy.wait()
 
 
 def scan(core, peer, weight, mixed, part, share, slope, gelu, ahead, product, first):
@@ -619,6 +628,7 @@
     channels = weight.shape[1]
     owners, rows, _ = share.shape
     out_shape = (2 * owners, rows, 2 * channels + 128)
+    anywhere = pl.BlockSpec(memory_space=pl.ANY)
     return pl.pallas_call(
         scan_kernel,
         grid_spec=pltpu.PrefetchScalarGridSpec(
@@ -636,19 +646,22 @@
                 whole(ahead.shape),
                 whole((16, channels)),
             ],
-            out_specs=[
-                whole((tokens, channels)),
-                whole(ahead.shape),
-                whole(out_shape),
-                whole((16, channels)),
+            out_specs=[anywhere] * 4,
+            scratch_shapes=[
+                pltpu.VMEM(ahead.shape, f32),
+                pltpu.VMEM((tokens, channels), f32),
+                pltpu.VMEM(ahead.shape, f32),
+                pltpu.VMEM(share.shape, bf16),
+                pltpu.VMEM((2 * owners, rows, 128), bf16),
+                pltpu.VMEM((16, channels), f32),
+                pltpu.SemaphoreType.DMA((6,)),
             ],
-            scratch_shapes=[pltpu.VMEM(ahead.shape, f32)],
         ),
         out_shape=[
-            jax.ShapeDtypeStruct((tokens, channels), f32),
-            jax.ShapeDtypeStruct(ahead.shape, f32),
-            jax.ShapeDtypeStruct(out_shape, bf16),
-            jax.ShapeDtypeStruct((16, channels), f32),
+            pltpu.HBM((tokens, channels), f32),
+            pltpu.HBM(ahead.shape, f32),
+            pltpu.HBM(out_shape, bf16),
+            pltpu.HBM((16, channels), f32),
         ],
         compiler_params=params(),
         cost_estimate=pl.CostEstimate(
@@ -727,7 +740,7 @@
         out_shape=jax.ShapeDtypeStruct((tokens, channels), f32),
         compiler_params=params(),
         name="tail",
-    )(place, shares, head, local, product, keep, gate, direct, gate_a, gate_x, taps)
+    )(place, shares, head, held(local), product, keep, gate, direct, held(gate_a), held(gate_x), held(taps))
 
 
 def exchange(value, axis):
@@ -782,8 +795,8 @@
     )
 
     arrived_far = swapped(arrived)
-    near_rows, part = near(core, arrived, down_w[0])
-    far_rows, gate_adj, up_adj, back_far = far(
+    part = near(core, arrived, down_w[0])
+    gate_adj, up_adj, back_far = far(
         core, arrived_far, down_w[0], part, silu, slope, gate_w[0], up_w[0]
     )
     back_in = swapped(back_far)
@@ -792,7 +805,7 @@
     returned = exchange(returning, "sp")
 
     grad_gate, grad_up = grad_in(packed, gate_adj, up_adj)
-    grad_down = grad_down_of(core, active, near_rows, far_rows)
+    grad_down = grad_down_of(core, active, arrived, arrived_far)
 
     stream_own = combine(core, returned, target, cotangent)
     stream_peer = swapped(stream_own)

time: 183 us -> 190 us (1.038)
  Pallas kernels: 45 us -> 69 us
  local copies, waits for them, and re-layouts: 21.5 us -> 5.07 us
    unnamed x74 -> x36, local copies, waits for them, and re-layouts: 21.4 us -> 2.85 us
    pallas_call x1, Pallas kernels: 6.91 us -> 11.9 us  [expert_pre(): pl.pallas_call(expert_pre_kernel, grid=(count // size,), in_specs=[by_row...]
    pallas_call x1, Pallas kernels: 4.24 us -> 7.19 us  [grad_down_of(): pl.pallas_call(grad_down_kernel, grid_spec=pltpu.PrefetchScalarGridSpec(n...]
    pallas_call x1, Pallas kernels: 3.42 us -> 6.23 us  [send(): pl.pallas_call(send_kernel, grid_spec=pltpu.PrefetchScalarGridSpec(num_sc...]
    pallas_call x1, Pallas kernels: 5.03 us -> 7.62 us  [far(): pl.pallas_call(far_kernel, grid_spec=pltpu.PrefetchScalarGridSpec(num_sca...]
    pallas_call x1, Pallas kernels: 3.31 us -> 5.6 us  [back_own(): pl.pallas_call(back_kernel, grid_spec=pltpu.PrefetchScalarGridSpec(num_sc...]
    pallas_call x1, Pallas kernels: 3.24 us -> 5.27 us  [recur_pre(): pl.pallas_call(recur_pre_kernel, grid=(blocks,), in_specs=[col(tokens), c...]
  transfers between devices with their start and end apart: 7 -> 7, of which waited for: 4 -> 3; matrix products, arithmetic and copies ran while one was open for 1% -> 2% of each run, Pallas kernels for 16% -> 23%
where the time goes in v3:
time: 190 us; the launch traced here: 187 us
  Pallas kernels  69 us (36%)
  waiting for transfers between devices  45.8 us (24%)
  blocking collectives  43.1 us (23%)
  starting transfers between devices  20 us (11%)
  local copies, waits for them, and re-layouts  5.07 us (3%)
  other arithmetic  2.92 us (2%)
    all_to_all x1, blocking collectives, exchange(): return lax.all_to_all(value, axis, split_axis=0, concat_axis=0, tiled=True)  43.1 us
    all_to_all x2, waiting for transfers between devices, exchange(): return lax.all_to_all(value, axis, split_axis=0, concat_axis=0, tiled=True)  38.6 us
    pallas_call x1, Pallas kernels, expert_pre(): pl.pallas_call(expert_pre_kernel, grid=(count // size,), in_specs=[by_row...  11.9 us
    all_to_all x2, starting transfers between devices, exchange(): return lax.all_to_all(value, axis, split_axis=0, concat_axis=0, tiled=True)  10.8 us
    pallas_call x1, Pallas kernels, grad_in(): pl.pallas_call(grad_in_kernel, grid=(model // size,), in_specs=[pl.BlockS...  9.08 us
    ppermute x2, starting transfers between devices, shifted(): return lax.ppermute(value, axis, pairs)  9.04 us
    pallas_call x1, Pallas kernels, far(): pl.pallas_call(far_kernel, grid_spec=pltpu.PrefetchScalarGridSpec(num_sca...  7.62 us
    ppermute x2, waiting for transfers between devices, shifted(): return lax.ppermute(value, axis, pairs)  7.2 us
  transfers between devices with their start and end apart: 7, of which 3 were waited for; matrix products, arithmetic and copies ran while one was open for 2% of the time, Pallas kernels for 23%

profile of v3, /device:TPU:32, one launch (start us, length us, event | category | flops | bytes accessed | tf_op | source)
XLA Modules:
  0.0 186.8 jit_solution(4663975979482978880)
XLA Ops:
  0.6 6.2 %send.1 = (bf16[64,16,1152]{2,1,0:T(8,128)(2,1)}, s32[8,384]{1,0:T(8,128)S(1)}) custom-call(s32[1]{0:T(128)} %bitcast.3.core_ref, s32[2,384]{1,0:T(2,128)} %bitcast.22, f32[2,384]{1,0:T(2,128)} %bitcast.23, bf16[384,2048]{1,0:T(8,128)(2,1)} %cot_ref.3), custom_call_target="tpu_custom_call" | custom-call | tf_op jit(solution)/shard_map/send/pallas_call | solution.py:106
  6.9 43.1 %all_to_all.15.block_ref.near_ref = bf16[64,16,1152]{2,1,0:T(8,128)(2,1)S(1)} all-to-all(bf16[64,16,1152]{2,1,0:T(8,128)(2,1)} %get-tuple-element.33), channel_id=1, replica_groups=mesh['sp'=64,'tp'=2] {'sp'}, dimensions={0} | all-to-all | bytes 4718592 | tf_op jit(solution)/shard_map/all_to_all | solution.py:747
  50.0 0.0 collective-permute-start
  50.0 11.9 %expert_pre.1 = (bf16[1152,2048]{1,0:T(8,128)(2,1)}, f32[1152,512]{1,0:T(8,128)}, f32[1152,512]{1,0:T(8,128)}, bf16[1152,512]{1,0:T(8,128)(2,1)}) custom-call(bf16[1152,2048]{1,0:T(8,128)(2,1)} %bitcast.25, bf16[2048,512]{1,0:T(8,128)(2,1)} %bitcast.15, bf16[2048,512]{1,0:T(8,128)(2,1)} %bitcast.18), custom_call_target="tpu_custom_call" | custom-call | flops 4831838208 | bytes 20971520 | tf_op jit(solution)/shard_map/expert_pre/pallas_call | solution.py:164
  61.9 0.0 copy-done
  61.9 0.0 copy-start.5
  61.9 3.5 %near.1.part_ref = f32[1152,512]{1,0:T(8,128)S(1)} custom-call(s32[1]{0:T(128)} %bitcast.3.core_ref, bf16[64,16,1152]{2,1,0:T(8,128)(2,1)S(1)} %all_to_all.15.block_ref.near_ref, bf16[512,2048]{1,0:T(8,128)(2,1)} %bitcast.13), custom_call_target="tpu_custom_call" | custom-call | flops 1207959552 | bytes 9437184 | tf_op jit(solution)/shard_map/near/pallas_call | solution.py:305
  65.4 0.0 collective-permute-done.block_ref.far_ref
  65.4 0.0 copy-start.3
  65.4 0.0 copy-done.4
  65.4 0.0 copy-done.5
  65.4 7.6 %far.1 = (bf16[1152,512]{1,0:T(8,128)(2,1)S(1)}, bf16[1152,512]{1,0:T(8,128)(2,1)S(1)}, bf16[64,16,1152]{2,1,0:T(8,128)(2,1)S(1)}) custom-call(s32[1]{0:T(128)} %bitcast.3.core_ref, bf16[64,16,1152]{2,1,0:T(8,128)(2,1)S(1)} %collective-permute-done.block_ref.far_ref, bf16[512,2048]{1,0:T(8,128)(2,1)} %bitcast.14, f32[1152,512]{1,0:T(8,128)S(1)} %near.1.part_ref, ...), custom_call_target="tpu_custom_call" | custom-call | flops 3623878656 | bytes 16777216 | tf_op jit(solution)/shard_map/far/pallas_call | solution.py:349
  73.1 0.1 collective-permute-start.1
  73.2 5.6 %back_own.1 = bf16[64,16,1152]{2,1,0:T(8,128)(2,1)S(1)} custom-call(s32[1]{0:T(128)} %bitcast.3.core_ref, bf16[1152,512]{1,0:T(8,128)(2,1)S(1)} %get-tuple-element.36.gate_adj_ref, bf16[1152,512]{1,0:T(8,128)(2,1)S(1)} %get-tuple-element.37.up_adj_ref, bf16[2048,512]{1,0:T(8,128)(2,1)} %bitcast.17, bf16[2048,512]{1,0:T(8,128)(2,1)} %bitcast.20), custom_call_target="tpu_custom_call" | custom-call | flops 2415919104 | bytes 7340032 | tf_op jit(solution)/shard_map/back_own/pallas_call | solution.py:391
  78.8 0.0 collective-permute-done.1
  78.8 2.0 %add_convert_fusion = bf16[64,16,1152]{2,1,0:T(8,128)(2,1)} fusion(bf16[64,16,1152]{2,1,0:T(8,128)(2,1)S(1)} %collective-permute-done.1, bf16[64,16,1152]{2,1,0:T(8,128)(2,1)S(1)} %back_own.1), kind=kLoop, calls=%fused_computation | loop fusion | flops 4718592 | bytes 7077888 | tf_op jit(solution)/shard_map/convert_element_type | solution.py:804
  80.8 6.4 %all-to-all-start.1 = ((bf16[64,16,1152]{2,1,0:T(8,128)(2,1)}), bf16[64,16,1152]{2,1,0:T(8,128)(2,1)S(1)}, u32[]{:S(2)}, u32[]{:S(2)}) async-start(bf16[64,16,1152]{2,1,0:T(8,128)(2,1)} %add_convert_fusion), calls=%async_computation.1 | async-start | bytes 4718592 | tf_op jit(solution)/shard_map/all_to_all | solution.py:747
  87.1 0.8 copy.21
  87.9 30.6 %all-to-all-done.1.block_ref = bf16[64,16,1152]{2,1,0:T(8,128)(2,1)S(1)} async-done(((bf16[64,16,1152]{2,1,0:T(8,128)(2,1)}), bf16[64,16,1152]{2,1,0:T(8,128)(2,1)S(1)}, u32[]{:S(2)}, u32[]{:S(2)}) %all-to-all-start.1) | async-done | bytes 2359328 | tf_op jit(solution)/shard_map/all_to_all | solution.py:747
  118.5 4.7 %combine.1.own_ref = bf16[384,1024]{1,0:T(8,128)(2,1)S(1)} custom-call(s32[1]{0:T(128)} %bitcast.3.core_ref, bf16[64,16,1152]{2,1,0:T(8,128)(2,1)S(1)} %all-to-all-done.1.block_ref, s32[384,8]{1,0:T(8,128)} %bitcast.21, bf16[384,2048]{1,0:T(8,128)(2,1)} %cot_ref.3), custom_call_target="tpu_custom_call" | custom-call | tf_op jit(solution)/shard_map/combine/pallas_call | solution.py:499
  123.3 0.1 collective-permute-start.2
  123.4 0.7 slice.16
  124.1 0.7 slice.15
  124.8 2.5 %collective-permute-start.3 = (bf16[4,512]{1,0:T(4,128)(2,1)S(1)}, bf16[4,512]{1,0:T(4,128)(2,1)S(1)}, u32[]{:S(2)}, u32[]{:S(2)}) collective-permute-start(bf16[4,512]{1,0:T(4,128)(2,1)S(1)} %pad_maximum_fusion.1), channel_id=1, source_target_pairs={{0,2},{2,4},{4,6},{6,8},{8,10},{10,12},{12,14},{14,16},{16,18},{18... | collective-permute-start | bytes 12296 | tf_op jit(solution)/shard_map/ppermute | solution.py:757
  127.3 7.2 %collective-permute-done.3.edge_ref = bf16[4,512]{1,0:T(4,128)(2,1)S(1)} collective-permute-done((bf16[4,512]{1,0:T(4,128)(2,1)S(1)}, bf16[4,512]{1,0:T(4,128)(2,1)S(1)}, u32[]{:S(2)}, u32[]{:S(2)}) %collective-permute-start.3) | collective-permute-done | bytes 4128 | tf_op jit(solution)/shard_map/ppermute | solution.py:757
  134.5 0.6 copy-done.16
  135.1 5.3 %recur_pre.1 = (bf16[384,512]{1,0:T(8,128)(2,1)}, f32[384,512]{1,0:T(8,128)}, f32[384,512]{1,0:T(8,128)}, f32[4,384,128]{2,1,0:T(8,128)}, f32[4,384,128]{2,1,0:T...) custom-call(bf16[384,512]{1,0:T(8,128)(2,1)} %x_ref.1, ...), custom_call_target="tpu_custom_call" | custom-call | flops 393216000 | bytes 8388608 | tf_op jit(solution)/shard_map/recur_pre/pallas_call | solution.py:251
  140.4 0.0 copy-start.2
  140.4 1.1 copy-done.6
  141.5 1.1 own_part.1
  142.6 0.0 collective-permute-done.2.peer_ref
  142.6 0.0 copy-done.10
  142.6 0.2 copy-done.11
  142.9 0.2 copy-done.12
  143.1 2.8 %scan.1 = (f32[384,512]{1,0:T(8,128)}, f32[4,384,128]{2,1,0:T(8,128)}, bf16[64,16,1152]{2,1,0:T(8,128)(2,1)}, f32[16,512]{1,0:T(8,128)}) custom-call(s32[1]{0:T(128)} %bitcast.3.core_ref, bf16[384,1024]{1,0:T(8,128)(2,1)S(1)} %collective-permute-done.2.peer_ref, bf16[2048,512]{1,0:T(8,128)(2,1)S(1)} %copy-done.1, bf16[384,512]{1,0:T(8,128)(2,1)S(1)} %copy-done.6, ...), custom_call_target="tpu_custom_call" | custom-call | flops 805306368 | bytes 9437184 | tf_op jit(solution)/shard_map/scan/pallas_call | solution.py:632
  145.9 4.5 %all-to-all-start.2 = ((bf16[64,16,1152]{2,1,0:T(8,128)(2,1)}), bf16[64,16,1152]{2,1,0:T(8,128)(2,1)S(1)}, u32[]{:S(2)}, u32[]{:S(2)}) async-start(bf16[64,16,1152]{2,1,0:T(8,128)(2,1)} %get-tuple-element.51), calls=%async_computation.2 | async-start | bytes 4718592 | tf_op jit(solution)/shard_map/all_to_all | solution.py:747
  150.3 7.2 %grad_down.1 = bf16[512,2048]{1,0:T(8,128)(2,1)} custom-call(s32[1]{0:T(128)} %bitcast.3.core_ref, bf16[1152,512]{1,0:T(8,128)(2,1)} %get-tuple-element.40.active_ref, bf16[64,16,1152]{2,1,0:T(8,128)(2,1)} %copy-done, bf16[64,16,1152]{2,1,0:T(8,128)(2,1)} %copy-done.3), custom_call_target="tpu_custom_call" | custom-call | flops 2415919104 | bytes 9437184 | tf_op jit(solution)/shard_map/grad_down/pallas_call | solution.py:453
  157.5 9.1 %grad_in.1 = (bf16[2048,512]{1,0:T(8,128)(2,1)}, bf16[2048,512]{1,0:T(8,128)(2,1)}) custom-call(bf16[1152,2048]{1,0:T(8,128)(2,1)} %get-tuple-element.32.packed_ref, bf16[1152,512]{1,0:T(8,128)(2,1)} %copy-done.14, bf16[1152,512]{1,0:T(8,128)(2,1)} %copy-done.15), custom_call_target="tpu_custom_call" | custom-call | flops 4831838208 | bytes 11534336 | tf_op jit(solution)/shard_map/grad_in/pallas_call | solution.py:420
  166.6 0.0 copy-done.17
  166.6 6.5 %collective-permute-start.4 = (f32[16,512]{1,0:T(8,128)S(1)}, f32[16,512]{1,0:T(8,128)S(1)}, u32[]{:S(2)}, u32[]{:S(2)}) collective-permute-start(f32[16,512]{1,0:T(8,128)S(1)} %copy-done.17), channel_id=1, source_target_pairs={{2,0},{4,2},{6,4},{8,6},{10,8},{12,10},{14,12},{16,14},{18,16},{20... | collective-permute-start | bytes 98312 | tf_op jit(solution)/shard_map/ppermute | solution.py:757
  173.1 8.0 %all-to-all-done.2.line_ref = bf16[64,16,1152]{2,1,0:T(8,128)(2,1)S(1)} async-done(((bf16[64,16,1152]{2,1,0:T(8,128)(2,1)}), bf16[64,16,1152]{2,1,0:T(8,128)(2,1)S(1)}, u32[]{:S(2)}, u32[]{:S(2)}) %all-to-all-start.2) | async-done | bytes 2359328 | tf_op jit(solution)/shard_map/all_to_all | solution.py:747
  181.2 0.3 convert_reduce_fusion
  181.5 0.6 pad_maximum_fusion
  182.1 0.0 collective-permute-done.4.head_ref
  182.1 0.2 copy-done.7
  182.3 0.3 copy-done.8
  182.6 0.2 copy-done.9
  182.8 4.0 %tail.1 = f32[384,512]{1,0:T(8,128)} custom-call(s32[1]{0:T(128)} %bitcast.12.place_ref, bf16[64,16,1152]{2,1,0:T(8,128)(2,1)S(1)} %all-to-all-done.2.line_ref, f32[16,512]{1,0:T(8,128)S(1)} %collective-permute-done.4.head_ref, f32[4,384,128]{2,1,0:T(8,128)} %get-tuple-element.53.local_ref, f32[4,384,128]{2,1,0:T(8,128)S(1)} %copy-done.2, ...), custom_call_target="tpu_custom_call" | custom-call | tf_op jit(solution)/shard_map/tail/pallas_call | solution.py:727
  (23 shorter events, 0.1 us)
Async XLA Ops:
  50.0 11.9 %copy-start = (bf16[64,16,1152]{2,1,0:T(8,128)(2,1)}, bf16[64,16,1152]{2,1,0:T(8,128)(2,1)S(1)}, u32[]{:S(2)}) copy-start(bf16[64,16,1152]{2,1,0:T(8,128)(2,1)S(1)} %all_to_all.15.block_ref.near_ref) | copy-start | bytes 7077892
  50.0 15.4 %collective-permute-start = (bf16[64,16,1152]{2,1,0:T(8,128)(2,1)S(1)}, bf16[64,16,1152]{2,1,0:T(8,128)(2,1)S(1)}, u32[]{:S(2)}, u32[]{:S(2)}) collective-permute-start(bf16[64,16,1152]{2,1,0:T(8,128)(2,1)S(1)} %all_to_all.15.block_ref.near_ref), channel_id=1, source_target_pairs={{0,1},{1,0},{2,3},{3,2},{4,5},{5,4},{6,7},{7,6},{8,9},{9,8},{10,11... | collective-permute-start | bytes 7077896 | tf_op jit(solution)/shard_map/ppermute | solution.py:751
  61.9 3.5 %copy-start.4 = (f32[1152,512]{1,0:T(8,128)S(1)}, f32[1152,512]{1,0:T(8,128)}, u32[]{:S(2)}) copy-start(f32[1152,512]{1,0:T(8,128)} %get-tuple-element.34.silu_ref) | copy-start | bytes 7077892
  61.9 3.5 %copy-start.5 = (f32[1152,512]{1,0:T(8,128)S(1)}, f32[1152,512]{1,0:T(8,128)}, u32[]{:S(2)}) copy-start(f32[1152,512]{1,0:T(8,128)} %get-tuple-element.35.slope_ref) | copy-start | bytes 7077892
  65.4 7.7 %copy-start.3 = (bf16[64,16,1152]{2,1,0:T(8,128)(2,1)}, bf16[64,16,1152]{2,1,0:T(8,128)(2,1)S(1)}, u32[]{:S(2)}) copy-start(bf16[64,16,1152]{2,1,0:T(8,128)(2,1)S(1)} %collective-permute-done.block_ref.far_ref) | copy-start | bytes 7077892
  73.1 5.7 %copy-start.14 = (bf16[1152,512]{1,0:T(8,128)(2,1)}, bf16[1152,512]{1,0:T(8,128)(2,1)S(1)}, u32[]{:S(2)}) copy-start(bf16[1152,512]{1,0:T(8,128)(2,1)S(1)} %get-tuple-element.36.gate_adj_ref) | copy-start | bytes 3538948
  73.1 5.7 %copy-start.15 = (bf16[1152,512]{1,0:T(8,128)(2,1)}, bf16[1152,512]{1,0:T(8,128)(2,1)S(1)}, u32[]{:S(2)}) copy-start(bf16[1152,512]{1,0:T(8,128)(2,1)S(1)} %get-tuple-element.37.up_adj_ref) | copy-start | bytes 3538948
  73.1 5.7 %collective-permute-start.1 = (bf16[64,16,1152]{2,1,0:T(8,128)(2,1)S(1)}, bf16[64,16,1152]{2,1,0:T(8,128)(2,1)S(1)}, u32[]{:S(2)}, u32[]{:S(2)}) collective-permute-start(bf16[64,16,1152]{2,1,0:T(8,128)(2,1)S(1)} %get-tuple-element.41), channel_id=1, source_target_pairs={{0,1},{1,0},{2,3},{3,2},{4,5},{5,4},{6,7},{7,6},{8,9},{9,8},{10,11... | collective-permute-start | bytes 7077896 | tf_op jit(solution)/shard_map/ppermute | solution.py:751
  80.8 37.8 %all-to-all-start.1 = ((bf16[64,16,1152]{2,1,0:T(8,128)(2,1)}), bf16[64,16,1152]{2,1,0:T(8,128)(2,1)S(1)}, u32[]{:S(2)}, u32[]{:S(2)}) async-start(bf16[64,16,1152]{2,1,0:T(8,128)(2,1)} %add_convert_fusion), calls=%async_computation.1 | async-start | bytes 4718592 | tf_op jit(solution)/shard_map/all_to_all | solution.py:747
  118.5 21.9 %copy-start.1 = (bf16[2048,512]{1,0:T(8,128)(2,1)S(1)}, bf16[2048,512]{1,0:T(8,128)(2,1)}, u32[]{:S(2)}) copy-start(bf16[2048,512]{1,0:T(8,128)(2,1)} %weight_ref.3) | copy-start | bytes 6291460
  123.3 19.3 %collective-permute-start.2 = (bf16[384,1024]{1,0:T(8,128)(2,1)S(1)}, bf16[384,1024]{1,0:T(8,128)(2,1)S(1)}, u32[]{:S(2)}, u32[]{:S(2)}) collective-permute-start(bf16[384,1024]{1,0:T(8,128)(2,1)S(1)} %combine.1.own_ref), channel_id=1, source_target_pairs={{0,1},{1,0},{2,3},{3,2},{4,5},{5,4},{6,7},{7,6},{8,9},{9,8},{10,11... | collective-permute-start | bytes 2359304 | tf_op jit(solution)/shard_map/ppermute | solution.py:751
  124.8 9.7 %collective-permute-start.3 = (bf16[4,512]{1,0:T(4,128)(2,1)S(1)}, bf16[4,512]{1,0:T(4,128)(2,1)S(1)}, u32[]{:S(2)}, u32[]{:S(2)}) collective-permute-start(bf16[4,512]{1,0:T(4,128)(2,1)S(1)} %pad_maximum_fusion.1), channel_id=1, source_target_pairs={{0,2},{2,4},{4,6},{6,8},{8,10},{10,12},{12,14},{14,16},{16,18},{18... | collective-permute-start | bytes 12296 | tf_op jit(solution)/shard_map/ppermute | solution.py:757
  134.5 0.6 copy-start.16
  140.4 2.2 %copy-start.2 = (f32[4,384,128]{2,1,0:T(8,128)S(1)}, f32[4,384,128]{2,1,0:T(8,128)}, u32[]{:S(2)}) copy-start(f32[4,384,128]{2,1,0:T(8,128)} %get-tuple-element.49.product_ref) | copy-start | bytes 2359300
  140.4 1.1 copy-start.6
  141.5 1.2 copy-start.10
  141.5 1.4 copy-start.11
  141.5 1.6 copy-start.12
  141.5 1.6 copy-start.13
  145.9 35.3 %all-to-all-start.2 = ((bf16[64,16,1152]{2,1,0:T(8,128)(2,1)}), bf16[64,16,1152]{2,1,0:T(8,128)(2,1)S(1)}, u32[]{:S(2)}, u32[]{:S(2)}) async-start(bf16[64,16,1152]{2,1,0:T(8,128)(2,1)} %get-tuple-element.51), calls=%async_computation.2 | async-start | bytes 4718592 | tf_op jit(solution)/shard_map/all_to_all | solution.py:747
  157.5 9.1 %copy-start.17 = (f32[16,512]{1,0:T(8,128)S(1)}, f32[16,512]{1,0:T(8,128)}, u32[]{:S(2)}) copy-start(f32[16,512]{1,0:T(8,128)} %get-tuple-element.52) | copy-start | bytes 98308
  166.6 15.5 %collective-permute-start.4 = (f32[16,512]{1,0:T(8,128)S(1)}, f32[16,512]{1,0:T(8,128)S(1)}, u32[]{:S(2)}, u32[]{:S(2)}) collective-permute-start(f32[16,512]{1,0:T(8,128)S(1)} %copy-done.17), channel_id=1, source_target_pairs={{2,0},{4,2},{6,4},{8,6},{10,8},{12,10},{14,12},{16,14},{18,16},{20... | collective-permute-start | bytes 98312 | tf_op jit(solution)/shard_map/ppermute | solution.py:757
  181.2 1.1 copy-start.7
  181.2 1.4 copy-start.8
  181.2 1.6 copy-start.9

commit v4 on v3

--- a/solution.py
+++ b/solution.py
@@ -291,9 +291,38 @@
         )
 
 
-def near_kernel(core_ref, block_ref, down_ref, part_ref, scratch):
+def near_by(value):
+    return pltpu.with_memory_space_constraint(value, pltpu.VMEM)
+
+
+def load_beside(copies):
+    @pl.when(pl.program_id(0) == 0)
+    def _():
+        for copy in copies:
+            copy.start()
+
+    return copies
+
+
+def finish(copies):
+    @pl.when(pl.program_id(0) == pl.num_programs(0) - 1)
+    def _():
+        for copy in copies:
+            copy.wait()
+
+
+anywhere = pl.BlockSpec(memory_space=pl.ANY)
+
+
+def near_kernel(core_ref, block_ref, down_ref, down_all, part_ref, down_next, scratch, sems):
+    half = down_ref.shape[1]
+    other = pl.multiple_of((1 - core_ref[0]) * half, half)
+    copies = load_beside(
+        [pltpu.make_async_copy(down_all.at[:, pl.ds(other, half)], down_next, sems.at[0])]
+    )
     rows = unpack(block_ref[...], scratch)
     part_ref[...] = dot(rows, down_ref[...], inner)
+    finish(copies)
 
 
 def near(core, arrived, down):
@@ -310,121 +339,174 @@
             in_specs=[
                 pl.BlockSpec((pair * group, main, wide), lambda i, c: (i, 0, 0)),
                 pl.BlockSpec((hidden, half), lambda i, c: (0, c[0])),
+                anywhere,
             ],
-            out_specs=pl.BlockSpec((size, hidden), lambda i, c: (i, 0)),
-            scratch_shapes=[pltpu.VMEM((128, 128), f32)],
-        ),
-        out_shape=jax.ShapeDtypeStruct((count, hidden), f32),
+            out_specs=[pl.BlockSpec((size, hidden), lambda i, c: (i, 0)), anywhere],
+            scratch_shapes=[pltpu.VMEM((128, 128), f32), pltpu.SemaphoreType.DMA((1,))],
+        ),
+        out_shape=[
+            jax.ShapeDtypeStruct((count, hidden), f32),
+            pltpu.VMEM((hidden, half), bf16),
+        ],
         compiler_params=params(),
         cost_estimate=pl.CostEstimate(
             flops=2 * count * half * hidden, transcendentals=0, bytes_accessed=9 << 20
         ),
         name="near",
-    )(core, arrived, held(down))
+    )(core, arrived, held(down), held(down))
 
 
 def far_kernel(
-    core_ref, block_ref, down_ref, part_ref, silu_ref, slope_ref, gate_ref, up_ref,
-    gate_adj_ref, up_adj_ref, back_ref, scratch,
+    core_ref, block_ref, down_ref, part_ref, silu_ref, slope_ref, gate_all, up_all,
+    adj_ref, gate_next, up_next, scratch, sems,
 ):
+    half = gate_next.shape[0]
+    own = pl.multiple_of(core_ref[0] * half, half)
+    copies = load_beside(
+        [
+            pltpu.make_async_copy(gate_all.at[pl.ds(own, half)], gate_next, sems.at[0]),
+            pltpu.make_async_copy(up_all.at[pl.ds(own, half)], up_next, sems.at[1]),
+        ]
+    )
     rows = unpack(block_ref[...], scratch)
     grad = part_ref[...] + dot(rows, down_ref[...], inner)
-    gate_adj = (grad * slope_ref[...]).astype(bf16)
-    up_adj = (grad * silu_ref[...]).astype(bf16)
-    gate_adj_ref[...] = gate_adj
-    up_adj_ref[...] = up_adj
-    back = dot(gate_adj, gate_ref[...], inner) + dot(up_adj, up_ref[...], inner)
-    pack_into(back_ref, back, scratch)
-
-
-def far(core, arrived, down, part, silu, slope, gate, up):
+    hidden = grad.shape[1]
+    adj_ref[:, 0:hidden] = (grad * slope_ref[...]).astype(bf16)
+    adj_ref[:, hidden:] = (grad * silu_ref[...]).astype(bf16)
+    finish(copies)
+
+
+def far(core, arrived, down_half, part, silu, slope, gate, up):
     experts, _, wide = arrived.shape
-    half = wide - 128
-    hidden = down.shape[0]
+    hidden, half = down_half.shape
     count = experts * (main + extra)
     size = pair * group_rows
     by_row = lambda width: pl.BlockSpec((size, width), lambda i, c: (i, 0))
-    block = pl.BlockSpec((pair * group, main, wide), lambda i, c: (i, 0, 0))
-    weight = pl.BlockSpec((half, hidden), lambda i, c: (1 - c[0], 0))
     return pl.pallas_call(
         far_kernel,
         grid_spec=pltpu.PrefetchScalarGridSpec(
             num_scalar_prefetch=1,
             grid=(count // size,),
             in_specs=[
-                block,
-                pl.BlockSpec((hidden, half), lambda i, c: (0, 1 - c[0])),
+                pl.BlockSpec((pair * group, main, wide), lambda i, c: (i, 0, 0)),
+                whole((hidden, half)),
                 by_row(hidden),
                 by_row(hidden),
                 by_row(hidden),
-                weight,
-                weight,
+                anywhere,
+                anywhere,
             ],
-            out_specs=[by_row(hidden), by_row(hidden), block],
-            scratch_shapes=[pltpu.VMEM((128, 128), f32)],
+            out_specs=[by_row(2 * hidden), anywhere, anywhere],
+            scratch_shapes=[pltpu.VMEM((128, 128), f32), pltpu.SemaphoreType.DMA((2,))],
         ),
         out_shape=[
-            jax.ShapeDtypeStruct((count, hidden), bf16),
-            jax.ShapeDtypeStruct((count, hidden), bf16),
-            jax.ShapeDtypeStruct(arrived.shape, bf16),
+            jax.ShapeDtypeStruct((count, 2 * hidden), bf16),
+            pltpu.VMEM((half, hidden), bf16),
+            pltpu.VMEM((half, hidden), bf16),
         ],
         compiler_params=params(),
         cost_estimate=pl.CostEstimate(
-            flops=6 * count * half * hidden, transcendentals=0, bytes_accessed=16 << 20
+            flops=2 * count * half * hidden, transcendentals=0, bytes_accessed=16 << 20
         ),
         name="far",
-    )(core, arrived, held(down), part, silu, slope, held(gate), held(up))
-
-
-def back_kernel(core_ref, gate_adj_ref, up_adj_ref, gate_ref, up_ref, back_ref, scratch):
-    back = dot(gate_adj_ref[...], gate_ref[...], inner) + dot(up_adj_ref[...], up_ref[...], inner)
-    pack_into(back_ref, back, scratch)
-
-
-def back_own(core, gate_adj, up_adj, gate, up, shape):
-    _, _, wide = shape
-    half = wide - 128
-    count, hidden = gate_adj.shape
+    )(core, arrived, near_by(down_half), part, silu, slope, held(gate), held(up))
+
+
+def back_rows(adj, gate, up):
+    hidden = gate.shape[1]
+    back = dot(adj[:, 0:hidden], gate, inner) + dot(adj[:, hidden:], up, inner)
+    return back.astype(bf16)
+
+
+def back_own_kernel(
+    core_ref, adj_ref, gate_ref, up_ref, gate_all, up_all, back_ref, gate_next, up_next, sems
+):
+    half = gate_next.shape[0]
+    own = pl.multiple_of(core_ref[0] * half, half)
+    copies = load_beside(
+        [
+            pltpu.make_async_copy(gate_all.at[pl.ds(own, half)], gate_next, sems.at[0]),
+            pltpu.make_async_copy(up_all.at[pl.ds(own, half)], up_next, sems.at[1]),
+        ]
+    )
+    back_ref[...] = back_rows(adj_ref[...], gate_ref[...], up_ref[...])
+    finish(copies)
+
+
+def back_own(core, adj, gate_half, up_half, gate_peer, up_peer):
+    count = adj.shape[0]
+    half, hidden = gate_half.shape
     size = pair * group_rows
     by_row = lambda width: pl.BlockSpec((size, width), lambda i, c: (i, 0))
-    weight = pl.BlockSpec((half, hidden), lambda i, c: (c[0], 0))
-    return pl.pallas_call(
-        back_kernel,
+    return pl.pallas_call(
+        back_own_kernel,
         grid_spec=pltpu.PrefetchScalarGridSpec(
             num_scalar_prefetch=1,
             grid=(count // size,),
-            in_specs=[by_row(hidden), by_row(hidden), weight, weight],
-            out_specs=pl.BlockSpec((pair * group, main, wide), lambda i, c: (i, 0, 0)),
-            scratch_shapes=[pltpu.VMEM((128, 128), f32)],
-        ),
-        out_shape=jax.ShapeDtypeStruct(shape, bf16),
+            in_specs=[
+                by_row(2 * hidden),
+                whole((half, hidden)),
+                whole((half, hidden)),
+                anywhere,
+                anywhere,
+            ],
+            out_specs=[by_row(half), anywhere, anywhere],
+            scratch_shapes=[pltpu.SemaphoreType.DMA((2,))],
+        ),
+        out_shape=[
+            jax.ShapeDtypeStruct((count, half), bf16),
+            pltpu.VMEM((half, hidden), bf16),
+            pltpu.VMEM((half, hidden), bf16),
+        ],
         compiler_params=params(),
         cost_estimate=pl.CostEstimate(
             flops=4 * count * half * hidden, transcendentals=0, bytes_accessed=7 << 20
         ),
         name="back_own",
-    )(core, gate_adj, up_adj, held(gate), held(up))
-
-
-def grad_in_kernel(packed_ref, gate_adj_ref, up_adj_ref, gate_ref, up_ref):
-    packed = packed_ref[...]
-    gate_ref[...] = dot(packed, gate_adj_ref[...], outer).astype(bf16)
-    up_ref[...] = dot(packed, up_adj_ref[...], outer).astype(bf16)
-
-
-def grad_in(packed, gate_adj, up_adj):
+    )(core, adj, near_by(gate_half), near_by(up_half), held(gate_peer), held(up_peer))
+
+
+def back_sum_kernel(adj_ref, own_ref, gate_ref, up_ref, out_ref, scratch):
+    peer = back_rows(adj_ref[...], gate_ref[...], up_ref[...])
+    pack_into(out_ref, own_ref[...].astype(f32) + peer.astype(f32), scratch)
+
+
+def back_sum(adj, own, gate_half, up_half, shape):
+    count = adj.shape[0]
+    half, hidden = gate_half.shape
+    size = pair * group_rows
+    by_row = lambda width: pl.BlockSpec((size, width), lambda i: (i, 0))
+    return pl.pallas_call(
+        back_sum_kernel,
+        grid=(count // size,),
+        in_specs=[by_row(2 * hidden), by_row(half), whole((half, hidden)), whole((half, hidden))],
+        out_specs=pl.BlockSpec((pair * group, main, shape[2]), lambda i: (i, 0, 0)),
+        scratch_shapes=[pltpu.VMEM((128, 128), f32)],
+        out_shape=pltpu.HBM(shape, bf16),
+        compiler_params=params(),
+        cost_estimate=pl.CostEstimate(
+            flops=4 * count * half * hidden, transcendentals=0, bytes_accessed=7 << 20
+        ),
+        name="back_sum",
+    )(adj, own, near_by(gate_half), near_by(up_half))
+
+
+def grad_in_kernel(packed_ref, adj_ref, gate_ref, up_ref):
+    grad = dot(packed_ref[...], adj_ref[...], outer).astype(bf16)
+    hidden = gate_ref.shape[1]
+    gate_ref[...] = grad[:, 0:hidden]
+    up_ref[...] = grad[:, hidden:]
+
+
+def grad_in(packed, adj):
     count, model = packed.shape
-    hidden = gate_adj.shape[1]
+    hidden = adj.shape[1] // 2
     size = 512
     out = pl.BlockSpec((size, hidden), lambda i: (i, 0))
     return pl.pallas_call(
         grad_in_kernel,
         grid=(model // size,),
-        in_specs=[
-            pl.BlockSpec((count, size), lambda i: (0, i)),
-            whole((count, hidden)),
-            whole((count, hidden)),
-        ],
+        in_specs=[pl.BlockSpec((count, size), lambda i: (0, i)), whole((count, 2 * hidden))],
         out_specs=[out, out],
         out_shape=[jax.ShapeDtypeStruct((model, hidden), bf16)] * 2,
         compiler_params=params(),
@@ -432,7 +514,7 @@
             flops=4 * count * model * hidden, transcendentals=0, bytes_accessed=11 << 20
         ),
         name="grad_in",
-    )(held(packed), held(gate_adj), held(up_adj))
+    )(held(packed), held(adj))
 
 
 def grad_down_kernel(core_ref, active_ref, near_ref, far_ref, out_ref, scratch):
@@ -628,7 +710,6 @@
     channels = weight.shape[1]
     owners, rows, _ = share.shape
     out_shape = (2 * owners, rows, 2 * channels + 128)
-    anywhere = pl.BlockSpec(memory_space=pl.ANY)
     return pl.pallas_call(
         scan_kernel,
         grid_spec=pltpu.PrefetchScalarGridSpec(
@@ -789,22 +870,24 @@
     arrived = exchange(outgoing, "sp")
     target = target.T
 
+    gate_peer = swapped(gate_w[0])
+    up_peer = swapped(up_w[0])
     packed, silu, slope, active = expert_pre(expert_rows[0], gate_w[0], up_w[0])
     mixed, y_slope, gelu, ahead, product, keep_part, input_part, direct, first = recur_pre(
         in_x, in_y, state, edge, conv_taps, gate_a, gate_x, decay_rate[None]
     )
 
     arrived_far = swapped(arrived)
-    part = near(core, arrived, down_w[0])
-    gate_adj, up_adj, back_far = far(
-        core, arrived_far, down_w[0], part, silu, slope, gate_w[0], up_w[0]
-    )
-    back_in = swapped(back_far)
-    own = back_own(core, gate_adj, up_adj, gate_w[0], up_w[0], arrived.shape)
-    returning = (own.astype(f32) + back_in.astype(f32)).astype(bf16)
+    part, down_half = near(core, arrived, down_w[0])
+    adj, gate_half, up_half = far(
+        core, arrived_far, down_half, part, silu, slope, gate_w[0], up_w[0]
+    )
+    adj_peer = swapped(adj)
+    own, gate_half, up_half = back_own(core, adj, gate_half, up_half, gate_peer, up_peer)
+    returning = back_sum(adj_peer, own, gate_half, up_half, arrived.shape)
     returned = exchange(returning, "sp")
 
-    grad_gate, grad_up = grad_in(packed, gate_adj, up_adj)
+    grad_gate, grad_up = grad_in(packed, adj)
     grad_down = grad_down_of(core, active, arrived, arrived_far)
 
     stream_own = combine(core, returned, target, cotangent)

time: 190 us -> 197 us (1.037)
  waiting for transfers between devices: 45.8 us -> 55.7 us
  Pallas kernels: 69 us -> 65.7 us
  local copies, waits for them, and re-layouts: 5.07 us -> 8.04 us
    ppermute x3 -> x5, waiting for transfers between devices: 0.01 us -> 8.85 us  [swapped(): return lax.ppermute(value, 'tp', [(0, 1), (1, 0)])]
    pallas_call x1, Pallas kernels: 7.62 us -> 2.45 us  [far(): pl.pallas_call(far_kernel, grid_spec=pltpu.PrefetchScalarGridSpec(num_sca...]
    unnamed x36 -> x42, local copies, waits for them, and re-layouts: 2.85 us -> 5.82 us
    pallas_call x1 -> x2, Pallas kernels: 5.6 us -> 7.49 us  [the longest x1 4.21 us: back_sum(): pl.pallas_call(back_sum_kernel, grid=(count // size,), in_specs=[by_row(2...]
  transfers between devices with their start and end apart: 7 -> 9, of which waited for: 3 -> 5; matrix products, arithmetic and copies ran while one was open for 2% -> 2% of each run, Pallas kernels for 23% -> 21%
where the time goes in v4:
time: 197 us; the launch traced here: 194 us
  Pallas kernels  65.7 us (33%)
  waiting for transfers between devices  55.7 us (28%)
  blocking collectives  43.1 us (22%)
  starting transfers between devices  19.7 us (10%)
  local copies, waits for them, and re-layouts  8.04 us (4%)
    all_to_all x1, blocking collectives, exchange(): return lax.all_to_all(value, axis, split_axis=0, concat_axis=0, tiled=True)  43.1 us
    all_to_all x2, waiting for transfers between devices, exchange(): return lax.all_to_all(value, axis, split_axis=0, concat_axis=0, tiled=True)  39.3 us
    pallas_call x1, Pallas kernels, expert_pre(): pl.pallas_call(expert_pre_kernel, grid=(count // size,), in_specs=[by_row...  11.9 us
    all_to_all x2, starting transfers between devices, exchange(): return lax.all_to_all(value, axis, split_axis=0, concat_axis=0, tiled=True)  10.8 us
    pallas_call x1, Pallas kernels, grad_in(): pl.pallas_call(grad_in_kernel, grid=(model // size,), in_specs=[pl.BlockS...  9.1 us
    ppermute x5, waiting for transfers between devices, swapped(): return lax.ppermute(value, 'tp', [(0, 1), (1, 0)])  8.85 us
    ppermute x2, starting transfers between devices, shifted(): return lax.ppermute(value, axis, pairs)  8.65 us
    ppermute x2, waiting for transfers between devices, shifted(): return lax.ppermute(value, axis, pairs)  7.54 us
  transfers between devices with their start and end apart: 9, of which 5 were waited for; matrix products, arithmetic and copies ran while one was open for 2% of the time, Pallas kernels for 21%

profile of v4, /device:TPU:32, one launch (start us, length us, event | category | flops | bytes accessed | tf_op | source)
XLA Modules:
  0.0 194.2 jit_solution(2397163283510667808)
XLA Ops:
  0.6 6.2 %send.1 = (bf16[64,16,1152]{2,1,0:T(8,128)(2,1)}, s32[8,384]{1,0:T(8,128)S(1)}) custom-call(s32[1]{0:T(128)} %bitcast.3.core_ref, s32[2,384]{1,0:T(2,128)} %bitcast.22, f32[2,384]{1,0:T(2,128)} %bitcast.23, bf16[384,2048]{1,0:T(8,128)(2,1)} %cot_ref.3), custom_call_target="tpu_custom_call" | custom-call | tf_op jit(solution)/shard_map/send/pallas_call | solution.py:106
  6.9 43.1 %all_to_all.15.block_ref.near_ref = bf16[64,16,1152]{2,1,0:T(8,128)(2,1)S(1)} all-to-all(bf16[64,16,1152]{2,1,0:T(8,128)(2,1)} %get-tuple-element.38), channel_id=1, replica_groups=mesh['sp'=64,'tp'=2] {'sp'}, dimensions={0} | all-to-all | bytes 4718592 | tf_op jit(solution)/shard_map/all_to_all | solution.py:828
  50.0 0.0 collective-permute-start
  50.0 11.9 %expert_pre.1 = (bf16[1152,2048]{1,0:T(8,128)(2,1)}, f32[1152,512]{1,0:T(8,128)}, f32[1152,512]{1,0:T(8,128)}, bf16[1152,512]{1,0:T(8,128)(2,1)}) custom-call(bf16[1152,2048]{1,0:T(8,128)(2,1)} %bitcast.25, bf16[2048,512]{1,0:T(8,128)(2,1)} %bitcast.15, bf16[2048,512]{1,0:T(8,128)(2,1)} %bitcast.18), custom_call_target="tpu_custom_call" | custom-call | flops 4831838208 | bytes 20971520 | tf_op jit(solution)/shard_map/expert_pre/pallas_call | solution.py:164
  61.9 3.5 %near.1 = (f32[1152,512]{1,0:T(8,128)S(1)}, bf16[512,1024]{1,0:T(8,128)(2,1)S(1)}) custom-call(s32[1]{0:T(128)} %bitcast.3.core_ref, bf16[64,16,1152]{2,1,0:T(8,128)(2,1)S(1)} %all_to_all.15.block_ref.near_ref, bf16[512,2048]{1,0:T(8,128)(2,1)} %bitcast.13, bf16[512,2048]{1,0:T(8,128)(2,1)} %bitcast.14), custom_call_target="tpu_custom_call" | custom-call | flops 1207959552 | bytes 9437184 | tf_op jit(solution)/shard_map/near/pallas_call | solution.py:334
  65.5 0.0 copy-start.15
  65.5 0.0 copy-start.16
  65.5 2.4 %far.1 = (bf16[1152,1024]{1,0:T(8,128)(2,1)S(1)}, bf16[1024,512]{1,0:T(8,128)(2,1)S(1)}, bf16[1024,512]{1,0:T(8,128)(2,1)S(1)}) custom-call(s32[1]{0:T(128)} %bitcast.3.core_ref, bf16[64,16,1152]{2,1,0:T(8,128)(2,1)S(1)} %collective-permute-done.block_ref.far_ref, bf16[512,1024]{1,0:T(8,128)(2,1)S(1)} %get-tuple-element.39.down_ref, ...), custom_call_target="tpu_custom_call" | custom-call | flops 1207959552 | bytes 16777216 | tf_op jit(solution)/shard_map/far/pallas_call | solution.py:385
  68.0 0.1 collective-permute-start.1
  68.1 0.5 copy-done.15
  68.5 0.0 collective-permute-start.2
  68.6 1.2 copy-done.16
  69.7 0.0 collective-permute-start.3
  69.7 5.8 %collective-permute-done.2.gate_all = bf16[2048,512]{1,0:T(8,128)(2,1)S(1)} collective-permute-done((bf16[2048,512]{1,0:T(8,128)(2,1)S(1)}, bf16[2048,512]{1,0:T(8,128)(2,1)S(1)}, u32[]{:S(2)}, u32[]{:S(2)}) %collective-permute-start.2) | collective-permute-done | bytes 2097184 | tf_op jit(solution)/shard_map/ppermute | solution.py:832
  75.6 3.0 %collective-permute-done.3.up_all = bf16[2048,512]{1,0:T(8,128)(2,1)S(1)} collective-permute-done((bf16[2048,512]{1,0:T(8,128)(2,1)S(1)}, bf16[2048,512]{1,0:T(8,128)(2,1)S(1)}, u32[]{:S(2)}, u32[]{:S(2)}) %collective-permute-start.3) | collective-permute-done | bytes 2097184 | tf_op jit(solution)/shard_map/ppermute | solution.py:832
  78.6 1.3 copy-done.19
  79.9 3.3 %back_own.1 = (bf16[1152,1024]{1,0:T(8,128)(2,1)S(1)}, bf16[1024,512]{1,0:T(8,128)(2,1)S(1)}, bf16[1024,512]{1,0:T(8,128)(2,1)S(1)}) custom-call(s32[1]{0:T(128)} %bitcast.3.core_ref, bf16[1152,1024]{1,0:T(8,128)(2,1)S(1)} %get-tuple-element.43.adj_ref, bf16[1024,512]{1,0:T(8,128)(2,1)S(1)} %get-tuple-element.47.gate_ref, ...), custom_call_target="tpu_custom_call" | custom-call | flops 2415919104 | bytes 7340032 | tf_op jit(solution)/shard_map/back_own/pallas_call | solution.py:441
  83.2 4.2 %back_sum.1 = bf16[64,16,1152]{2,1,0:T(8,128)(2,1)} custom-call(bf16[1152,1024]{1,0:T(8,128)(2,1)S(1)} %collective-permute-done.1.adj_ref, bf16[1152,1024]{1,0:T(8,128)(2,1)S(1)} %get-tuple-element.49.own_ref, bf16[1024,512]{1,0:T(8,128)(2,1)S(1)} %get-tuple-element.50.gate_ref, bf16[1024,512]{1,0:T(8,128)(2,1)S(1)} %get-tuple-element.51.up_ref), custom_call_target="tpu_custom_call" | custom-call | flops 2415919104 | bytes 7340032 | tf_op jit(solution)/shard_map/back_sum/pallas_call | solution.py:479
  87.4 6.3 %all-to-all-start.1 = ((bf16[64,16,1152]{2,1,0:T(8,128)(2,1)}), bf16[64,16,1152]{2,1,0:T(8,128)(2,1)S(1)}, u32[]{:S(2)}, u32[]{:S(2)}) async-start(bf16[64,16,1152]{2,1,0:T(8,128)(2,1)} %back_sum.1), calls=%async_computation.1 | async-start | bytes 4718592 | tf_op jit(solution)/shard_map/all_to_all | solution.py:828
  93.8 0.8 copy.21
  94.6 31.3 %all-to-all-done.1.block_ref = bf16[64,16,1152]{2,1,0:T(8,128)(2,1)S(1)} async-done(((bf16[64,16,1152]{2,1,0:T(8,128)(2,1)}), bf16[64,16,1152]{2,1,0:T(8,128)(2,1)S(1)}, u32[]{:S(2)}, u32[]{:S(2)}) %all-to-all-start.1) | async-done | bytes 2359328 | tf_op jit(solution)/shard_map/all_to_all | solution.py:828
  125.9 4.7 %combine.1.own_ref = bf16[384,1024]{1,0:T(8,128)(2,1)S(1)} custom-call(s32[1]{0:T(128)} %bitcast.3.core_ref, bf16[64,16,1152]{2,1,0:T(8,128)(2,1)S(1)} %all-to-all-done.1.block_ref, s32[384,8]{1,0:T(8,128)} %bitcast.21, bf16[384,2048]{1,0:T(8,128)(2,1)} %cot_ref.3), custom_call_target="tpu_custom_call" | custom-call | tf_op jit(solution)/shard_map/combine/pallas_call | solution.py:581
  130.6 0.1 collective-permute-start.4
  130.7 0.7 slice.16
  131.4 0.7 slice.15
  132.1 2.2 %collective-permute-start.5 = (bf16[4,512]{1,0:T(4,128)(2,1)S(1)}, bf16[4,512]{1,0:T(4,128)(2,1)S(1)}, u32[]{:S(2)}, u32[]{:S(2)}) collective-permute-start(bf16[4,512]{1,0:T(4,128)(2,1)S(1)} %pad_maximum_fusion.1), channel_id=1, source_target_pairs={{0,2},{2,4},{4,6},{6,8},{8,10},{10,12},{12,14},{14,16},{16,18},{18... | collective-permute-start | bytes 12296 | tf_op jit(solution)/shard_map/ppermute | solution.py:838
  134.3 7.5 %collective-permute-done.5.edge_ref = bf16[4,512]{1,0:T(4,128)(2,1)S(1)} collective-permute-done((bf16[4,512]{1,0:T(4,128)(2,1)S(1)}, bf16[4,512]{1,0:T(4,128)(2,1)S(1)}, u32[]{:S(2)}, u32[]{:S(2)}) %collective-permute-start.5) | collective-permute-done | bytes 4128 | tf_op jit(solution)/shard_map/ppermute | solution.py:838
  141.8 0.6 copy-done.17
  142.4 5.3 %recur_pre.1 = (bf16[384,512]{1,0:T(8,128)(2,1)}, f32[384,512]{1,0:T(8,128)}, f32[384,512]{1,0:T(8,128)}, f32[4,384,128]{2,1,0:T(8,128)}, f32[4,384,128]{2,1,0:T...) custom-call(bf16[384,512]{1,0:T(8,128)(2,1)} %x_ref.1, ...), custom_call_target="tpu_custom_call" | custom-call | flops 393216000 | bytes 8388608 | tf_op jit(solution)/shard_map/recur_pre/pallas_call | solution.py:251
  147.7 0.0 copy-start.2
  147.7 1.1 copy-done.6
  148.8 1.1 own_part.1
  149.9 0.0 collective-permute-done.4.peer_ref
  149.9 0.0 copy-done.10
  150.0 0.2 copy-done.11
  150.2 0.2 copy-done.12
  150.4 2.8 %scan.1 = (f32[384,512]{1,0:T(8,128)}, f32[4,384,128]{2,1,0:T(8,128)}, bf16[64,16,1152]{2,1,0:T(8,128)(2,1)}, f32[16,512]{1,0:T(8,128)}) custom-call(s32[1]{0:T(128)} %bitcast.3.core_ref, bf16[384,1024]{1,0:T(8,128)(2,1)S(1)} %collective-permute-done.4.peer_ref, bf16[2048,512]{1,0:T(8,128)(2,1)S(1)} %copy-done.1, bf16[384,512]{1,0:T(8,128)(2,1)S(1)} %copy-done.6, ...), custom_call_target="tpu_custom_call" | custom-call | flops 805306368 | bytes 9437184 | tf_op jit(solution)/shard_map/scan/pallas_call | solution.py:713
  153.2 4.5 %all-to-all-start.2 = ((bf16[64,16,1152]{2,1,0:T(8,128)(2,1)}), bf16[64,16,1152]{2,1,0:T(8,128)(2,1)S(1)}, u32[]{:S(2)}, u32[]{:S(2)}) async-start(bf16[64,16,1152]{2,1,0:T(8,128)(2,1)} %get-tuple-element.61), calls=%async_computation.2 | async-start | bytes 4718592 | tf_op jit(solution)/shard_map/all_to_all | solution.py:828
  157.7 7.2 %grad_down.1 = bf16[512,2048]{1,0:T(8,128)(2,1)} custom-call(s32[1]{0:T(128)} %bitcast.3.core_ref, bf16[1152,512]{1,0:T(8,128)(2,1)} %get-tuple-element.46.active_ref, bf16[64,16,1152]{2,1,0:T(8,128)(2,1)} %copy-done, bf16[64,16,1152]{2,1,0:T(8,128)(2,1)} %copy-done.3), custom_call_target="tpu_custom_call" | custom-call | flops 2415919104 | bytes 9437184 | tf_op jit(solution)/shard_map/grad_down/pallas_call | solution.py:535
  164.9 9.1 %grad_in.1 = (bf16[2048,512]{1,0:T(8,128)(2,1)}, bf16[2048,512]{1,0:T(8,128)(2,1)}) custom-call(bf16[1152,2048]{1,0:T(8,128)(2,1)} %get-tuple-element.37.packed_ref, bf16[1152,1024]{1,0:T(8,128)(2,1)} %copy-done.14), custom_call_target="tpu_custom_call" | custom-call | flops 4831838208 | bytes 11534336 | tf_op jit(solution)/shard_map/grad_in/pallas_call | solution.py:506
  174.0 6.5 %collective-permute-start.6 = (f32[16,512]{1,0:T(8,128)S(1)}, f32[16,512]{1,0:T(8,128)S(1)}, u32[]{:S(2)}, u32[]{:S(2)}) collective-permute-start(f32[16,512]{1,0:T(8,128)S(1)} %copy-done.20), channel_id=1, source_target_pairs={{2,0},{4,2},{6,4},{8,6},{10,8},{12,10},{14,12},{16,14},{18,16},{20... | collective-permute-start | bytes 98312 | tf_op jit(solution)/shard_map/ppermute | solution.py:838
  180.5 8.1 %all-to-all-done.2.line_ref = bf16[64,16,1152]{2,1,0:T(8,128)(2,1)S(1)} async-done(((bf16[64,16,1152]{2,1,0:T(8,128)(2,1)}), bf16[64,16,1152]{2,1,0:T(8,128)(2,1)S(1)}, u32[]{:S(2)}, u32[]{:S(2)}) %all-to-all-start.2) | async-done | bytes 2359328 | tf_op jit(solution)/shard_map/all_to_all | solution.py:828
  188.5 0.3 convert_reduce_fusion
  188.8 0.6 pad_maximum_fusion
  189.5 0.2 copy-done.7
  189.7 0.3 copy-done.8
  189.9 0.2 copy-done.9
  190.1 4.0 %tail.1 = f32[384,512]{1,0:T(8,128)} custom-call(s32[1]{0:T(128)} %bitcast.12.place_ref, bf16[64,16,1152]{2,1,0:T(8,128)(2,1)S(1)} %all-to-all-done.2.line_ref, f32[16,512]{1,0:T(8,128)S(1)} %collective-permute-done.6.head_ref, f32[4,384,128]{2,1,0:T(8,128)} %get-tuple-element.63.local_ref, f32[4,384,128]{2,1,0:T(8,128)S(1)} %copy-done.2, ...), custom_call_target="tpu_custom_call" | custom-call | tf_op jit(solution)/shard_map/tail/pallas_call | solution.py:808
  (33 shorter events, 0.1 us)
Async XLA Ops:
  50.0 11.9 %copy-start = (bf16[64,16,1152]{2,1,0:T(8,128)(2,1)}, bf16[64,16,1152]{2,1,0:T(8,128)(2,1)S(1)}, u32[]{:S(2)}) copy-start(bf16[64,16,1152]{2,1,0:T(8,128)(2,1)S(1)} %all_to_all.15.block_ref.near_ref) | copy-start | bytes 7077892
  50.0 15.4 %collective-permute-start = (bf16[64,16,1152]{2,1,0:T(8,128)(2,1)S(1)}, bf16[64,16,1152]{2,1,0:T(8,128)(2,1)S(1)}, u32[]{:S(2)}, u32[]{:S(2)}) collective-permute-start(bf16[64,16,1152]{2,1,0:T(8,128)(2,1)S(1)} %all_to_all.15.block_ref.near_ref), channel_id=1, source_target_pairs={{0,1},{1,0},{2,3},{3,2},{4,5},{5,4},{6,7},{7,6},{8,9},{9,8},{10,11... | collective-permute-start | bytes 7077896 | tf_op jit(solution)/shard_map/ppermute | solution.py:832
  61.9 3.5 %copy-start.4 = (f32[1152,512]{1,0:T(8,128)S(1)}, f32[1152,512]{1,0:T(8,128)}, u32[]{:S(2)}) copy-start(f32[1152,512]{1,0:T(8,128)} %get-tuple-element.41.silu_ref) | copy-start | bytes 7077892
  61.9 3.6 %copy-start.5 = (f32[1152,512]{1,0:T(8,128)S(1)}, f32[1152,512]{1,0:T(8,128)}, u32[]{:S(2)}) copy-start(f32[1152,512]{1,0:T(8,128)} %get-tuple-element.42.slope_ref) | copy-start | bytes 7077892
  65.4 2.5 %copy-start.3 = (bf16[64,16,1152]{2,1,0:T(8,128)(2,1)}, bf16[64,16,1152]{2,1,0:T(8,128)(2,1)S(1)}, u32[]{:S(2)}) copy-start(bf16[64,16,1152]{2,1,0:T(8,128)(2,1)S(1)} %collective-permute-done.block_ref.far_ref) | copy-start | bytes 7077892
  65.5 3.1 %copy-start.15 = (bf16[1,2048,512]{2,1,0:T(8,128)(2,1)S(1)}, bf16[1,2048,512]{2,1,0:T(8,128)(2,1)}, u32[]{:S(2)}) copy-start(bf16[1,2048,512]{2,1,0:T(8,128)(2,1)} %param.19) | copy-start | bytes 6291460
  65.5 4.3 %copy-start.16 = (bf16[1,2048,512]{2,1,0:T(8,128)(2,1)S(1)}, bf16[1,2048,512]{2,1,0:T(8,128)(2,1)}, u32[]{:S(2)}) copy-start(bf16[1,2048,512]{2,1,0:T(8,128)(2,1)} %param.20) | copy-start | bytes 6291460
  67.9 15.2 %copy-start.14 = (bf16[1152,1024]{1,0:T(8,128)(2,1)}, bf16[1152,1024]{1,0:T(8,128)(2,1)S(1)}, u32[]{:S(2)}) copy-start(bf16[1152,1024]{1,0:T(8,128)(2,1)S(1)} %get-tuple-element.43.adj_ref) | copy-start | bytes 7077892
  68.0 15.2 %collective-permute-start.1 = (bf16[1152,1024]{1,0:T(8,128)(2,1)S(1)}, bf16[1152,1024]{1,0:T(8,128)(2,1)S(1)}, u32[]{:S(2)}, u32[]{:S(2)}) collective-permute-start(bf16[1152,1024]{1,0:T(8,128)(2,1)S(1)} %get-tuple-element.43.adj_ref), channel_id=1, source_target_pairs={{0,1},{1,0},{2,3},{3,2},{4,5},{5,4},{6,7},{7,6},{8,9},{9,8},{10,11... | collective-permute-start | bytes 7077896 | tf_op jit(solution)/shard_map/ppermute | solution.py:832
  68.5 7.0 %collective-permute-start.2 = (bf16[2048,512]{1,0:T(8,128)(2,1)S(1)}, bf16[2048,512]{1,0:T(8,128)(2,1)S(1)}, u32[]{:S(2)}, u32[]{:S(2)}) collective-permute-start(bf16[2048,512]{1,0:T(8,128)(2,1)S(1)} %bitcast.17), channel_id=1, source_target_pairs={{0,1},{1,0},{2,3},{3,2},{4,5},{5,4},{6,7},{7,6},{8,9},{9,8},{10,11... | collective-permute-start | bytes 6291464 | tf_op jit(solution)/shard_map/ppermute | solution.py:832
  69.7 8.8 %collective-permute-start.3 = (bf16[2048,512]{1,0:T(8,128)(2,1)S(1)}, bf16[2048,512]{1,0:T(8,128)(2,1)S(1)}, u32[]{:S(2)}, u32[]{:S(2)}) collective-permute-start(bf16[2048,512]{1,0:T(8,128)(2,1)S(1)} %bitcast.20), channel_id=1, source_target_pairs={{0,1},{1,0},{2,3},{3,2},{4,5},{5,4},{6,7},{7,6},{8,9},{9,8},{10,11... | collective-permute-start | bytes 6291464 | tf_op jit(solution)/shard_map/ppermute | solution.py:832
  75.6 3.0 %copy-start.18 = (bf16[2048,512]{1,0:T(8,128)(2,1)}, bf16[2048,512]{1,0:T(8,128)(2,1)S(1)}, u32[]{:S(2)}) copy-start(bf16[2048,512]{1,0:T(8,128)(2,1)S(1)} %collective-permute-done.2.gate_all) | copy-start | bytes 6291460
  78.6 1.3 copy-start.19
  87.4 38.4 %all-to-all-start.1 = ((bf16[64,16,1152]{2,1,0:T(8,128)(2,1)}), bf16[64,16,1152]{2,1,0:T(8,128)(2,1)S(1)}, u32[]{:S(2)}, u32[]{:S(2)}) async-start(bf16[64,16,1152]{2,1,0:T(8,128)(2,1)} %back_sum.1), calls=%async_computation.1 | async-start | bytes 4718592 | tf_op jit(solution)/shard_map/all_to_all | solution.py:828
  125.9 21.8 %copy-start.1 = (bf16[2048,512]{1,0:T(8,128)(2,1)S(1)}, bf16[2048,512]{1,0:T(8,128)(2,1)}, u32[]{:S(2)}) copy-start(bf16[2048,512]{1,0:T(8,128)(2,1)} %weight_ref.3) | copy-start | bytes 6291460
  130.6 19.3 %collective-permute-start.4 = (bf16[384,1024]{1,0:T(8,128)(2,1)S(1)}, bf16[384,1024]{1,0:T(8,128)(2,1)S(1)}, u32[]{:S(2)}, u32[]{:S(2)}) collective-permute-start(bf16[384,1024]{1,0:T(8,128)(2,1)S(1)} %combine.1.own_ref), channel_id=1, source_target_pairs={{0,1},{1,0},{2,3},{3,2},{4,5},{5,4},{6,7},{7,6},{8,9},{9,8},{10,11... | collective-permute-start | bytes 2359304 | tf_op jit(solution)/shard_map/ppermute | solution.py:832
  132.1 9.7 %collective-permute-start.5 = (bf16[4,512]{1,0:T(4,128)(2,1)S(1)}, bf16[4,512]{1,0:T(4,128)(2,1)S(1)}, u32[]{:S(2)}, u32[]{:S(2)}) collective-permute-start(bf16[4,512]{1,0:T(4,128)(2,1)S(1)} %pad_maximum_fusion.1), channel_id=1, source_target_pairs={{0,2},{2,4},{4,6},{6,8},{8,10},{10,12},{12,14},{14,16},{16,18},{18... | collective-permute-start | bytes 12296 | tf_op jit(solution)/shard_map/ppermute | solution.py:838
  141.8 0.6 copy-start.17
  147.7 2.2 %copy-start.2 = (f32[4,384,128]{2,1,0:T(8,128)S(1)}, f32[4,384,128]{2,1,0:T(8,128)}, u32[]{:S(2)}) copy-start(f32[4,384,128]{2,1,0:T(8,128)} %get-tuple-element.59.product_ref) | copy-start | bytes 2359300
  147.7 1.1 copy-start.6
  148.8 1.2 copy-start.10
  148.8 1.4 copy-start.11
  148.8 1.6 copy-start.12
  148.8 1.6 copy-start.13
  153.2 35.3 %all-to-all-start.2 = ((bf16[64,16,1152]{2,1,0:T(8,128)(2,1)}), bf16[64,16,1152]{2,1,0:T(8,128)(2,1)S(1)}, u32[]{:S(2)}, u32[]{:S(2)}) async-start(bf16[64,16,1152]{2,1,0:T(8,128)(2,1)} %get-tuple-element.61), calls=%async_computation.2 | async-start | bytes 4718592 | tf_op jit(solution)/shard_map/all_to_all | solution.py:828
  164.9 9.1 %copy-start.20 = (f32[16,512]{1,0:T(8,128)S(1)}, f32[16,512]{1,0:T(8,128)}, u32[]{:S(2)}) copy-start(f32[16,512]{1,0:T(8,128)} %get-tuple-element.62) | copy-start | bytes 98308
  174.0 15.5 %collective-permute-start.6 = (f32[16,512]{1,0:T(8,128)S(1)}, f32[16,512]{1,0:T(8,128)S(1)}, u32[]{:S(2)}, u32[]{:S(2)}) collective-permute-start(f32[16,512]{1,0:T(8,128)S(1)} %copy-done.20), channel_id=1, source_target_pairs={{2,0},{4,2},{6,4},{8,6},{10,8},{12,10},{14,12},{16,14},{18,16},{20... | collective-permute-start | bytes 98312 | tf_op jit(solution)/shard_map/ppermute | solution.py:838
  188.5 1.1 copy-start.7
  188.5 1.4 copy-start.8
  188.5 1.6 copy-start.9

commit v5 on v4

--- a/solution.py
+++ b/solution.py
@@ -56,7 +56,7 @@
 def send_kernel(core_ref, routes_ref, weight_ref, cot_ref, out_ref, target_ref, slot, scratch):
     step = pl.program_id(0)
     tokens = cot_ref.shape[0]
-    experts = pl.num_programs(0) * group
+    experts = pl.num_programs(0) * out_ref.shape[0]
 
     @pl.when(step == 0)
     def _():
@@ -83,7 +83,8 @@
             [slot[0:2, :], jnp.zeros((6, tokens), jnp.int32)], axis=0
         )
 
-    rows = lax.broadcasted_iota(jnp.int32, (group_rows, tokens), 0) + step * group_rows
+    size = out_ref.shape[0] // group * group_rows
+    rows = lax.broadcasted_iota(jnp.int32, (size, tokens), 0) + step * size
     hit_first = rows == slot[0:1, :]
     hit_second = rows == slot[1:2, :]
     chosen = jnp.where(hit_first | hit_second, 1.0, 0.0).astype(bf16)
@@ -94,10 +95,7 @@
         keepdims=True,
     )
     values = dot(chosen, cot_ref[...], plain) * weight
-    width = values.shape[1]
-    out_ref[:, :, 0:width] = values[0:main_rows].astype(bf16).reshape(group, main, width)
-    tiles = pack_extras(values[main_rows:], scratch)
-    out_ref[:, :, width:] = tiles.astype(bf16).reshape(group, main, 128)
+    pack_into(out_ref, values, scratch)
 
 
 def send(core, routes, weight, cotangent, experts):
@@ -107,14 +105,14 @@
         send_kernel,
         grid_spec=pltpu.PrefetchScalarGridSpec(
             num_scalar_prefetch=1,
-            grid=(experts // group,),
+            grid=(experts // (send_groups * group),),
             in_specs=[
                 whole((2, tokens)),
                 whole((2, tokens)),
                 pl.BlockSpec((tokens, half), lambda i, c: (0, c[0])),
             ],
             out_specs=[
-                pl.BlockSpec((group, main, half + 128), lambda i, c: (i, 0, 0)),
+                pl.BlockSpec((send_groups * group, main, half + 128), lambda i, c: (i, 0, 0)),
                 whole((8, tokens)),
             ],
             scratch_shapes=[pltpu.VMEM((8, tokens), jnp.int32), pltpu.VMEM((128, 128), f32)],
@@ -129,6 +127,9 @@
 
 
 pair = 2
+send_groups = 4
+all_groups = 8
+sum_groups = 4
 
 
 def expert_pre_kernel(rows_ref, gate_ref, up_ref, packed_ref, silu_ref, slope_ref, active_ref):
@@ -330,14 +331,14 @@
     half = wide - 128
     hidden = down.shape[0]
     count = experts * (main + extra)
-    size = pair * group_rows
+    size = all_groups * group_rows
     return pl.pallas_call(
         near_kernel,
         grid_spec=pltpu.PrefetchScalarGridSpec(
             num_scalar_prefetch=1,
             grid=(count // size,),
             in_specs=[
-                pl.BlockSpec((pair * group, main, wide), lambda i, c: (i, 0, 0)),
+                pl.BlockSpec((all_groups * group, main, wide), lambda i, c: (i, 0, 0)),
                 pl.BlockSpec((hidden, half), lambda i, c: (0, c[0])),
                 anywhere,
             ],
@@ -380,7 +381,7 @@
     experts, _, wide = arrived.shape
     hidden, half = down_half.shape
     count = experts * (main + extra)
-    size = pair * group_rows
+    size = all_groups * group_rows
     by_row = lambda width: pl.BlockSpec((size, width), lambda i, c: (i, 0))
     return pl.pallas_call(
         far_kernel,
@@ -388,7 +389,7 @@
             num_scalar_prefetch=1,
             grid=(count // size,),
             in_specs=[
-                pl.BlockSpec((pair * group, main, wide), lambda i, c: (i, 0, 0)),
+                pl.BlockSpec((all_groups * group, main, wide), lambda i, c: (i, 0, 0)),
                 whole((hidden, half)),
                 by_row(hidden),
                 by_row(hidden),
@@ -436,7 +437,7 @@
 def back_own(core, adj, gate_half, up_half, gate_peer, up_peer):
     count = adj.shape[0]
     half, hidden = gate_half.shape
-    size = pair * group_rows
+    size = all_groups * group_rows
     by_row = lambda width: pl.BlockSpec((size, width), lambda i, c: (i, 0))
     return pl.pallas_call(
         back_own_kernel,
@@ -474,13 +475,13 @@
 def back_sum(adj, own, gate_half, up_half, shape):
     count = adj.shape[0]
     half, hidden = gate_half.shape
-    size = pair * group_rows
+    size = sum_groups * group_rows
     by_row = lambda width: pl.BlockSpec((size, width), lambda i: (i, 0))
     return pl.pallas_call(
         back_sum_kernel,
         grid=(count // size,),
         in_specs=[by_row(2 * hidden), by_row(half), whole((half, hidden)), whole((half, hidden))],
-        out_specs=pl.BlockSpec((pair * group, main, shape[2]), lambda i: (i, 0, 0)),
+        out_specs=pl.BlockSpec((sum_groups * group, main, shape[2]), lambda i: (i, 0, 0)),
         scratch_shapes=[pltpu.VMEM((128, 128), f32)],
         out_shape=pltpu.HBM(shape, bf16),
         compiler_params=params(),
@@ -582,9 +583,9 @@
         combine_kernel,
         grid_spec=pltpu.PrefetchScalarGridSpec(
             num_scalar_prefetch=1,
-            grid=(experts // (pair * group),),
+            grid=(experts // (all_groups * group),),
             in_specs=[
-                pl.BlockSpec((pair * group, main, wide), lambda i, c: (i, 0, 0)),
+                pl.BlockSpec((all_groups * group, main, wide), lambda i, c: (i, 0, 0)),
                 whole((tokens, 8)),
                 pl.BlockSpec((tokens, half), lambda i, c: (0, c[0])),
             ],

time: 197 us -> 192 us (0.975)
  Pallas kernels: 65.7 us -> 60.5 us
    pallas_call x1, Pallas kernels: 4.71 us -> 2.69 us  [combine(): pl.pallas_call(combine_kernel, grid_spec=pltpu.PrefetchScalarGridSpec(num...]
where the time goes in v5:
time: 192 us; the launch traced here: 189 us
  Pallas kernels  60.5 us (32%)
  waiting for transfers between devices  55.6 us (29%)
  blocking collectives  43.1 us (22%)
  starting transfers between devices  19.6 us (10%)
  local copies, waits for them, and re-layouts  8.13 us (4%)
    all_to_all x1, blocking collectives, exchange(): return lax.all_to_all(value, axis, split_axis=0, concat_axis=0, tiled=True)  43.1 us
    all_to_all x2, waiting for transfers between devices, exchange(): return lax.all_to_all(value, axis, split_axis=0, concat_axis=0, tiled=True)  39.3 us
    pallas_call x1, Pallas kernels, expert_pre(): pl.pallas_call(expert_pre_kernel, grid=(count // size,), in_specs=[by_row...  11.9 us
    all_to_all x2, starting transfers between devices, exchange(): return lax.all_to_all(value, axis, split_axis=0, concat_axis=0, tiled=True)  10.7 us
    pallas_call x1, Pallas kernels, grad_in(): pl.pallas_call(grad_in_kernel, grid=(model // size,), in_specs=[pl.BlockS...  9.1 us
    ppermute x2, starting transfers between devices, shifted(): return lax.ppermute(value, axis, pairs)  8.81 us
    ppermute x5, waiting for transfers between devices, swapped(): return lax.ppermute(value, 'tp', [(0, 1), (1, 0)])  8.78 us
    ppermute x2, waiting for transfers between devices, shifted(): return lax.ppermute(value, axis, pairs)  7.54 us
  transfers between devices with their start and end apart: 9, of which 5 were waited for; matrix products, arithmetic and copies ran while one was open for 2% of the time, Pallas kernels for 21%

profile of v5, /device:TPU:32, one launch (start us, length us, event | category | flops | bytes accessed | tf_op | source)
XLA Modules:
  0.0 188.9 jit_solution(3064872023251683454)
XLA Ops:
  0.6 4.3 %send.1 = (bf16[64,16,1152]{2,1,0:T(8,128)(2,1)}, s32[8,384]{1,0:T(8,128)S(1)}) custom-call(s32[1]{0:T(128)} %bitcast.3.core_ref, s32[2,384]{1,0:T(2,128)} %bitcast.22, f32[2,384]{1,0:T(2,128)} %bitcast.23, bf16[384,2048]{1,0:T(8,128)(2,1)} %cot_ref.3), custom_call_target="tpu_custom_call" | custom-call | tf_op jit(solution)/shard_map/send/pallas_call | solution.py:104
  5.0 43.1 %all_to_all.15.block_ref.near_ref = bf16[64,16,1152]{2,1,0:T(8,128)(2,1)S(1)} all-to-all(bf16[64,16,1152]{2,1,0:T(8,128)(2,1)} %get-tuple-element.38), channel_id=1, replica_groups=mesh['sp'=64,'tp'=2] {'sp'}, dimensions={0} | all-to-all | bytes 4718592 | tf_op jit(solution)/shard_map/all_to_all | solution.py:829
  48.1 0.0 collective-permute-start
  48.1 11.9 %expert_pre.1 = (bf16[1152,2048]{1,0:T(8,128)(2,1)}, f32[1152,512]{1,0:T(8,128)}, f32[1152,512]{1,0:T(8,128)}, bf16[1152,512]{1,0:T(8,128)(2,1)}) custom-call(bf16[1152,2048]{1,0:T(8,128)(2,1)} %bitcast.25, bf16[2048,512]{1,0:T(8,128)(2,1)} %bitcast.15, bf16[2048,512]{1,0:T(8,128)(2,1)} %bitcast.18), custom_call_target="tpu_custom_call" | custom-call | flops 4831838208 | bytes 20971520 | tf_op jit(solution)/shard_map/expert_pre/pallas_call | solution.py:165
  60.0 3.0 %near.1 = (f32[1152,512]{1,0:T(8,128)S(1)}, bf16[512,1024]{1,0:T(8,128)(2,1)S(1)}) custom-call(s32[1]{0:T(128)} %bitcast.3.core_ref, bf16[64,16,1152]{2,1,0:T(8,128)(2,1)S(1)} %all_to_all.15.block_ref.near_ref, bf16[512,2048]{1,0:T(8,128)(2,1)} %bitcast.13, bf16[512,2048]{1,0:T(8,128)(2,1)} %bitcast.14), custom_call_target="tpu_custom_call" | custom-call | flops 1207959552 | bytes 9437184 | tf_op jit(solution)/shard_map/near/pallas_call | solution.py:335
  63.0 0.0 collective-permute-done.block_ref.far_ref
  63.0 0.0 copy-start.15
  63.0 0.0 copy-start.16
  63.0 2.4 %far.1 = (bf16[1152,1024]{1,0:T(8,128)(2,1)S(1)}, bf16[1024,512]{1,0:T(8,128)(2,1)S(1)}, bf16[1024,512]{1,0:T(8,128)(2,1)S(1)}) custom-call(s32[1]{0:T(128)} %bitcast.3.core_ref, bf16[64,16,1152]{2,1,0:T(8,128)(2,1)S(1)} %collective-permute-done.block_ref.far_ref, bf16[512,1024]{1,0:T(8,128)(2,1)S(1)} %get-tuple-element.39.down_ref, ...), custom_call_target="tpu_custom_call" | custom-call | flops 1207959552 | bytes 16777216 | tf_op jit(solution)/shard_map/far/pallas_call | solution.py:386
  65.5 0.1 collective-permute-start.1
  65.6 0.5 copy-done.15
  66.1 0.0 collective-permute-start.2
  66.1 1.2 copy-done.16
  67.3 0.0 collective-permute-start.3
  67.3 5.8 %collective-permute-done.2.gate_all = bf16[2048,512]{1,0:T(8,128)(2,1)S(1)} collective-permute-done((bf16[2048,512]{1,0:T(8,128)(2,1)S(1)}, bf16[2048,512]{1,0:T(8,128)(2,1)S(1)}, u32[]{:S(2)}, u32[]{:S(2)}) %collective-permute-start.2) | collective-permute-done | bytes 2097184 | tf_op jit(solution)/shard_map/ppermute | solution.py:833
  73.1 3.0 %collective-permute-done.3.up_all = bf16[2048,512]{1,0:T(8,128)(2,1)S(1)} collective-permute-done((bf16[2048,512]{1,0:T(8,128)(2,1)S(1)}, bf16[2048,512]{1,0:T(8,128)(2,1)S(1)}, u32[]{:S(2)}, u32[]{:S(2)}) %collective-permute-start.3) | collective-permute-done | bytes 2097184 | tf_op jit(solution)/shard_map/ppermute | solution.py:833
  76.1 1.3 copy-done.19
  77.4 2.7 %back_own.1 = (bf16[1152,1024]{1,0:T(8,128)(2,1)S(1)}, bf16[1024,512]{1,0:T(8,128)(2,1)S(1)}, bf16[1024,512]{1,0:T(8,128)(2,1)S(1)}) custom-call(s32[1]{0:T(128)} %bitcast.3.core_ref, bf16[1152,1024]{1,0:T(8,128)(2,1)S(1)} %get-tuple-element.43.adj_ref, bf16[1024,512]{1,0:T(8,128)(2,1)S(1)} %get-tuple-element.47.gate_ref, ...), custom_call_target="tpu_custom_call" | custom-call | flops 2415919104 | bytes 7340032 | tf_op jit(solution)/shard_map/back_own/pallas_call | solution.py:442
  80.2 4.0 %back_sum.1 = bf16[64,16,1152]{2,1,0:T(8,128)(2,1)} custom-call(bf16[1152,1024]{1,0:T(8,128)(2,1)S(1)} %collective-permute-done.1.adj_ref, bf16[1152,1024]{1,0:T(8,128)(2,1)S(1)} %get-tuple-element.49.own_ref, bf16[1024,512]{1,0:T(8,128)(2,1)S(1)} %get-tuple-element.50.gate_ref, bf16[1024,512]{1,0:T(8,128)(2,1)S(1)} %get-tuple-element.51.up_ref), custom_call_target="tpu_custom_call" | custom-call | flops 2415919104 | bytes 7340032 | tf_op jit(solution)/shard_map/back_sum/pallas_call | solution.py:480
  84.2 6.4 %all-to-all-start.1 = ((bf16[64,16,1152]{2,1,0:T(8,128)(2,1)}), bf16[64,16,1152]{2,1,0:T(8,128)(2,1)S(1)}, u32[]{:S(2)}, u32[]{:S(2)}) async-start(bf16[64,16,1152]{2,1,0:T(8,128)(2,1)} %back_sum.1), calls=%async_computation.1 | async-start | bytes 4718592 | tf_op jit(solution)/shard_map/all_to_all | solution.py:829
  90.6 0.8 copy.21
  91.4 31.3 %all-to-all-done.1.block_ref = bf16[64,16,1152]{2,1,0:T(8,128)(2,1)S(1)} async-done(((bf16[64,16,1152]{2,1,0:T(8,128)(2,1)}), bf16[64,16,1152]{2,1,0:T(8,128)(2,1)S(1)}, u32[]{:S(2)}, u32[]{:S(2)}) %all-to-all-start.1) | async-done | bytes 2359328 | tf_op jit(solution)/shard_map/all_to_all | solution.py:829
  122.6 2.7 %combine.1.own_ref = bf16[384,1024]{1,0:T(8,128)(2,1)S(1)} custom-call(s32[1]{0:T(128)} %bitcast.3.core_ref, bf16[64,16,1152]{2,1,0:T(8,128)(2,1)S(1)} %all-to-all-done.1.block_ref, s32[384,8]{1,0:T(8,128)} %bitcast.21, bf16[384,2048]{1,0:T(8,128)(2,1)} %cot_ref.3), custom_call_target="tpu_custom_call" | custom-call | tf_op jit(solution)/shard_map/combine/pallas_call | solution.py:582
  125.3 0.1 collective-permute-start.4
  125.4 0.7 slice.16
  126.1 0.7 slice.15
  126.9 2.2 %collective-permute-start.5 = (bf16[4,512]{1,0:T(4,128)(2,1)S(1)}, bf16[4,512]{1,0:T(4,128)(2,1)S(1)}, u32[]{:S(2)}, u32[]{:S(2)}) collective-permute-start(bf16[4,512]{1,0:T(4,128)(2,1)S(1)} %pad_maximum_fusion.1), channel_id=1, source_target_pairs={{0,2},{2,4},{4,6},{6,8},{8,10},{10,12},{12,14},{14,16},{16,18},{18... | collective-permute-start | bytes 12296 | tf_op jit(solution)/shard_map/ppermute | solution.py:839
  129.0 7.5 %collective-permute-done.5.edge_ref = bf16[4,512]{1,0:T(4,128)(2,1)S(1)} collective-permute-done((bf16[4,512]{1,0:T(4,128)(2,1)S(1)}, bf16[4,512]{1,0:T(4,128)(2,1)S(1)}, u32[]{:S(2)}, u32[]{:S(2)}) %collective-permute-start.5) | collective-permute-done | bytes 4128 | tf_op jit(solution)/shard_map/ppermute | solution.py:839
  136.6 0.6 copy-done.17
  137.2 5.3 %recur_pre.1 = (bf16[384,512]{1,0:T(8,128)(2,1)}, f32[384,512]{1,0:T(8,128)}, f32[384,512]{1,0:T(8,128)}, f32[4,384,128]{2,1,0:T(8,128)}, f32[4,384,128]{2,1,0:T...) custom-call(bf16[384,512]{1,0:T(8,128)(2,1)} %x_ref.1, ...), custom_call_target="tpu_custom_call" | custom-call | flops 393216000 | bytes 8388608 | tf_op jit(solution)/shard_map/recur_pre/pallas_call | solution.py:252
  142.5 0.0 copy-start.2
  142.5 1.1 copy-done.6
  143.6 1.1 own_part.1
  144.7 0.0 copy-done.10
  144.7 0.2 copy-done.11
  145.0 0.2 copy-done.12
  145.2 2.8 %scan.1 = (f32[384,512]{1,0:T(8,128)}, f32[4,384,128]{2,1,0:T(8,128)}, bf16[64,16,1152]{2,1,0:T(8,128)(2,1)}, f32[16,512]{1,0:T(8,128)}) custom-call(s32[1]{0:T(128)} %bitcast.3.core_ref, bf16[384,1024]{1,0:T(8,128)(2,1)S(1)} %collective-permute-done.4.peer_ref, bf16[2048,512]{1,0:T(8,128)(2,1)S(1)} %copy-done.1, bf16[384,512]{1,0:T(8,128)(2,1)S(1)} %copy-done.6, ...), custom_call_target="tpu_custom_call" | custom-call | flops 805306368 | bytes 9437184 | tf_op jit(solution)/shard_map/scan/pallas_call | solution.py:714
  148.0 4.3 %all-to-all-start.2 = ((bf16[64,16,1152]{2,1,0:T(8,128)(2,1)}), bf16[64,16,1152]{2,1,0:T(8,128)(2,1)S(1)}, u32[]{:S(2)}, u32[]{:S(2)}) async-start(bf16[64,16,1152]{2,1,0:T(8,128)(2,1)} %get-tuple-element.61), calls=%async_computation.2 | async-start | bytes 4718592 | tf_op jit(solution)/shard_map/all_to_all | solution.py:829
  152.3 7.2 %grad_down.1 = bf16[512,2048]{1,0:T(8,128)(2,1)} custom-call(s32[1]{0:T(128)} %bitcast.3.core_ref, bf16[1152,512]{1,0:T(8,128)(2,1)} %get-tuple-element.46.active_ref, bf16[64,16,1152]{2,1,0:T(8,128)(2,1)} %copy-done, bf16[64,16,1152]{2,1,0:T(8,128)(2,1)} %copy-done.3), custom_call_target="tpu_custom_call" | custom-call | flops 2415919104 | bytes 9437184 | tf_op jit(solution)/shard_map/grad_down/pallas_call | solution.py:536
  159.5 9.1 %grad_in.1 = (bf16[2048,512]{1,0:T(8,128)(2,1)}, bf16[2048,512]{1,0:T(8,128)(2,1)}) custom-call(bf16[1152,2048]{1,0:T(8,128)(2,1)} %get-tuple-element.37.packed_ref, bf16[1152,1024]{1,0:T(8,128)(2,1)} %copy-done.14), custom_call_target="tpu_custom_call" | custom-call | flops 4831838208 | bytes 11534336 | tf_op jit(solution)/shard_map/grad_in/pallas_call | solution.py:507
  168.6 6.6 %collective-permute-start.6 = (f32[16,512]{1,0:T(8,128)S(1)}, f32[16,512]{1,0:T(8,128)S(1)}, u32[]{:S(2)}, u32[]{:S(2)}) collective-permute-start(f32[16,512]{1,0:T(8,128)S(1)} %copy-done.20), channel_id=1, source_target_pairs={{2,0},{4,2},{6,4},{8,6},{10,8},{12,10},{14,12},{16,14},{18,16},{20... | collective-permute-start | bytes 98312 | tf_op jit(solution)/shard_map/ppermute | solution.py:839
  175.2 8.0 %all-to-all-done.2.line_ref = bf16[64,16,1152]{2,1,0:T(8,128)(2,1)S(1)} async-done(((bf16[64,16,1152]{2,1,0:T(8,128)(2,1)}), bf16[64,16,1152]{2,1,0:T(8,128)(2,1)S(1)}, u32[]{:S(2)}, u32[]{:S(2)}) %all-to-all-start.2) | async-done | bytes 2359328 | tf_op jit(solution)/shard_map/all_to_all | solution.py:829
  183.3 0.3 convert_reduce_fusion
  183.6 0.6 pad_maximum_fusion
  184.2 0.2 copy-done.7
  184.4 0.3 copy-done.8
  184.6 0.2 copy-done.9
  184.9 4.0 %tail.1 = f32[384,512]{1,0:T(8,128)} custom-call(s32[1]{0:T(128)} %bitcast.12.place_ref, bf16[64,16,1152]{2,1,0:T(8,128)(2,1)S(1)} %all-to-all-done.2.line_ref, f32[16,512]{1,0:T(8,128)S(1)} %collective-permute-done.6.head_ref, f32[4,384,128]{2,1,0:T(8,128)} %get-tuple-element.63.local_ref, f32[4,384,128]{2,1,0:T(8,128)S(1)} %copy-done.2, ...), custom_call_target="tpu_custom_call" | custom-call | tf_op jit(solution)/shard_map/tail/pallas_call | solution.py:809
  (33 shorter events, 0.1 us)
Async XLA Ops:
  48.1 11.9 %copy-start = (bf16[64,16,1152]{2,1,0:T(8,128)(2,1)}, bf16[64,16,1152]{2,1,0:T(8,128)(2,1)S(1)}, u32[]{:S(2)}) copy-start(bf16[64,16,1152]{2,1,0:T(8,128)(2,1)S(1)} %all_to_all.15.block_ref.near_ref) | copy-start | bytes 7077892
  48.1 14.9 %collective-permute-start = (bf16[64,16,1152]{2,1,0:T(8,128)(2,1)S(1)}, bf16[64,16,1152]{2,1,0:T(8,128)(2,1)S(1)}, u32[]{:S(2)}, u32[]{:S(2)}) collective-permute-start(bf16[64,16,1152]{2,1,0:T(8,128)(2,1)S(1)} %all_to_all.15.block_ref.near_ref), channel_id=1, source_target_pairs={{0,1},{1,0},{2,3},{3,2},{4,5},{5,4},{6,7},{7,6},{8,9},{9,8},{10,11... | collective-permute-start | bytes 7077896 | tf_op jit(solution)/shard_map/ppermute | solution.py:833
  60.0 3.0 %copy-start.4 = (f32[1152,512]{1,0:T(8,128)S(1)}, f32[1152,512]{1,0:T(8,128)}, u32[]{:S(2)}) copy-start(f32[1152,512]{1,0:T(8,128)} %get-tuple-element.41.silu_ref) | copy-start | bytes 7077892
  60.0 3.0 %copy-start.5 = (f32[1152,512]{1,0:T(8,128)S(1)}, f32[1152,512]{1,0:T(8,128)}, u32[]{:S(2)}) copy-start(f32[1152,512]{1,0:T(8,128)} %get-tuple-element.42.slope_ref) | copy-start | bytes 7077892
  63.0 2.5 %copy-start.3 = (bf16[64,16,1152]{2,1,0:T(8,128)(2,1)}, bf16[64,16,1152]{2,1,0:T(8,128)(2,1)S(1)}, u32[]{:S(2)}) copy-start(bf16[64,16,1152]{2,1,0:T(8,128)(2,1)S(1)} %collective-permute-done.block_ref.far_ref) | copy-start | bytes 7077892
  63.0 3.1 %copy-start.15 = (bf16[1,2048,512]{2,1,0:T(8,128)(2,1)S(1)}, bf16[1,2048,512]{2,1,0:T(8,128)(2,1)}, u32[]{:S(2)}) copy-start(bf16[1,2048,512]{2,1,0:T(8,128)(2,1)} %param.19) | copy-start | bytes 6291460
  63.0 4.3 %copy-start.16 = (bf16[1,2048,512]{2,1,0:T(8,128)(2,1)S(1)}, bf16[1,2048,512]{2,1,0:T(8,128)(2,1)}, u32[]{:S(2)}) copy-start(bf16[1,2048,512]{2,1,0:T(8,128)(2,1)} %param.20) | copy-start | bytes 6291460
  65.5 14.7 %copy-start.14 = (bf16[1152,1024]{1,0:T(8,128)(2,1)}, bf16[1152,1024]{1,0:T(8,128)(2,1)S(1)}, u32[]{:S(2)}) copy-start(bf16[1152,1024]{1,0:T(8,128)(2,1)S(1)} %get-tuple-element.43.adj_ref) | copy-start | bytes 7077892
  65.5 14.7 %collective-permute-start.1 = (bf16[1152,1024]{1,0:T(8,128)(2,1)S(1)}, bf16[1152,1024]{1,0:T(8,128)(2,1)S(1)}, u32[]{:S(2)}, u32[]{:S(2)}) collective-permute-start(bf16[1152,1024]{1,0:T(8,128)(2,1)S(1)} %get-tuple-element.43.adj_ref), channel_id=1, source_target_pairs={{0,1},{1,0},{2,3},{3,2},{4,5},{5,4},{6,7},{7,6},{8,9},{9,8},{10,11... | collective-permute-start | bytes 7077896 | tf_op jit(solution)/shard_map/ppermute | solution.py:833
  66.1 7.0 %collective-permute-start.2 = (bf16[2048,512]{1,0:T(8,128)(2,1)S(1)}, bf16[2048,512]{1,0:T(8,128)(2,1)S(1)}, u32[]{:S(2)}, u32[]{:S(2)}) collective-permute-start(bf16[2048,512]{1,0:T(8,128)(2,1)S(1)} %bitcast.17), channel_id=1, source_target_pairs={{0,1},{1,0},{2,3},{3,2},{4,5},{5,4},{6,7},{7,6},{8,9},{9,8},{10,11... | collective-permute-start | bytes 6291464 | tf_op jit(solution)/shard_map/ppermute | solution.py:833
  67.3 8.8 %collective-permute-start.3 = (bf16[2048,512]{1,0:T(8,128)(2,1)S(1)}, bf16[2048,512]{1,0:T(8,128)(2,1)S(1)}, u32[]{:S(2)}, u32[]{:S(2)}) collective-permute-start(bf16[2048,512]{1,0:T(8,128)(2,1)S(1)} %bitcast.20), channel_id=1, source_target_pairs={{0,1},{1,0},{2,3},{3,2},{4,5},{5,4},{6,7},{7,6},{8,9},{9,8},{10,11... | collective-permute-start | bytes 6291464 | tf_op jit(solution)/shard_map/ppermute | solution.py:833
  73.1 3.0 %copy-start.18 = (bf16[2048,512]{1,0:T(8,128)(2,1)}, bf16[2048,512]{1,0:T(8,128)(2,1)S(1)}, u32[]{:S(2)}) copy-start(bf16[2048,512]{1,0:T(8,128)(2,1)S(1)} %collective-permute-done.2.gate_all) | copy-start | bytes 6291460
  76.1 1.3 copy-start.19
  84.2 38.4 %all-to-all-start.1 = ((bf16[64,16,1152]{2,1,0:T(8,128)(2,1)}), bf16[64,16,1152]{2,1,0:T(8,128)(2,1)S(1)}, u32[]{:S(2)}, u32[]{:S(2)}) async-start(bf16[64,16,1152]{2,1,0:T(8,128)(2,1)} %back_sum.1), calls=%async_computation.1 | async-start | bytes 4718592 | tf_op jit(solution)/shard_map/all_to_all | solution.py:829
  122.6 19.8 %copy-start.1 = (bf16[2048,512]{1,0:T(8,128)(2,1)S(1)}, bf16[2048,512]{1,0:T(8,128)(2,1)}, u32[]{:S(2)}) copy-start(bf16[2048,512]{1,0:T(8,128)(2,1)} %weight_ref.3) | copy-start | bytes 6291460
  125.3 19.3 %collective-permute-start.4 = (bf16[384,1024]{1,0:T(8,128)(2,1)S(1)}, bf16[384,1024]{1,0:T(8,128)(2,1)S(1)}, u32[]{:S(2)}, u32[]{:S(2)}) collective-permute-start(bf16[384,1024]{1,0:T(8,128)(2,1)S(1)} %combine.1.own_ref), channel_id=1, source_target_pairs={{0,1},{1,0},{2,3},{3,2},{4,5},{5,4},{6,7},{7,6},{8,9},{9,8},{10,11... | collective-permute-start | bytes 2359304 | tf_op jit(solution)/shard_map/ppermute | solution.py:833
  126.9 9.7 %collective-permute-start.5 = (bf16[4,512]{1,0:T(4,128)(2,1)S(1)}, bf16[4,512]{1,0:T(4,128)(2,1)S(1)}, u32[]{:S(2)}, u32[]{:S(2)}) collective-permute-start(bf16[4,512]{1,0:T(4,128)(2,1)S(1)} %pad_maximum_fusion.1), channel_id=1, source_target_pairs={{0,2},{2,4},{4,6},{6,8},{8,10},{10,12},{12,14},{14,16},{16,18},{18... | collective-permute-start | bytes 12296 | tf_op jit(solution)/shard_map/ppermute | solution.py:839
  136.6 0.6 copy-start.17
  142.5 2.2 %copy-start.2 = (f32[4,384,128]{2,1,0:T(8,128)S(1)}, f32[4,384,128]{2,1,0:T(8,128)}, u32[]{:S(2)}) copy-start(f32[4,384,128]{2,1,0:T(8,128)} %get-tuple-element.59.product_ref) | copy-start | bytes 2359300
  142.5 1.1 copy-start.6
  143.5 1.2 copy-start.10
  143.5 1.4 copy-start.11
  143.5 1.6 copy-start.12
  143.5 1.6 copy-start.13
  148.0 35.3 %all-to-all-start.2 = ((bf16[64,16,1152]{2,1,0:T(8,128)(2,1)}), bf16[64,16,1152]{2,1,0:T(8,128)(2,1)S(1)}, u32[]{:S(2)}, u32[]{:S(2)}) async-start(bf16[64,16,1152]{2,1,0:T(8,128)(2,1)} %get-tuple-element.61), calls=%async_computation.2 | async-start | bytes 4718592 | tf_op jit(solution)/shard_map/all_to_all | solution.py:829
  159.5 9.1 %copy-start.20 = (f32[16,512]{1,0:T(8,128)S(1)}, f32[16,512]{1,0:T(8,128)}, u32[]{:S(2)}) copy-start(f32[16,512]{1,0:T(8,128)} %get-tuple-element.62) | copy-start | bytes 98308
  168.6 15.7 %collective-permute-start.6 = (f32[16,512]{1,0:T(8,128)S(1)}, f32[16,512]{1,0:T(8,128)S(1)}, u32[]{:S(2)}, u32[]{:S(2)}) collective-permute-start(f32[16,512]{1,0:T(8,128)S(1)} %copy-done.20), channel_id=1, source_target_pairs={{2,0},{4,2},{6,4},{8,6},{10,8},{12,10},{14,12},{16,14},{18,16},{20... | collective-permute-start | bytes 98312 | tf_op jit(solution)/shard_map/ppermute | solution.py:839
  183.2 1.1 copy-start.7
  183.2 1.4 copy-start.8
  183.2 1.6 copy-start.9

commit v6 on v5

--- a/solution.py
+++ b/solution.py
@@ -231,7 +231,7 @@
         [
             decay[0:1],
             total,
-            jnp.zeros_like(total),
+            rate_scale * rate * jnp.sum(keep, axis=0, keepdims=True),
             product_ref[0, 0:3, :] * rest,
             keep_ref[0:3, :],
             input_ref[0:3, :],
@@ -313,6 +313,7 @@
 
 
 anywhere = pl.BlockSpec(memory_space=pl.ANY)
+resident = pl.BlockSpec(memory_space=pltpu.VMEM)
 
 
 def near_kernel(core_ref, block_ref, down_ref, down_all, part_ref, down_next, scratch, sems):
@@ -378,7 +379,7 @@
 
 
 def far(core, arrived, down_half, part, silu, slope, gate, up):
-    experts, _, wide = arrived.shape
+    experts, _, _ = arrived.shape
     hidden, half = down_half.shape
     count = experts * (main + extra)
     size = all_groups * group_rows
@@ -389,11 +390,11 @@
             num_scalar_prefetch=1,
             grid=(count // size,),
             in_specs=[
-                pl.BlockSpec((all_groups * group, main, wide), lambda i, c: (i, 0, 0)),
-                whole((hidden, half)),
-                by_row(hidden),
-                by_row(hidden),
-                by_row(hidden),
+                resident,
+                resident,
+                resident,
+                resident,
+                resident,
                 anywhere,
                 anywhere,
             ],
@@ -445,9 +446,9 @@
             num_scalar_prefetch=1,
             grid=(count // size,),
             in_specs=[
-                by_row(2 * hidden),
-                whole((half, hidden)),
-                whole((half, hidden)),
+                resident,
+                resident,
+                resident,
                 anywhere,
                 anywhere,
             ],
@@ -551,73 +552,83 @@
     )(core, held(active), held(arrived), held(arrived_far))
 
 
-def combine_kernel(core_ref, block_ref, target_ref, cot_ref, out_ref, total, scratch):
-    step = pl.program_id(0)
+def combine_kernel(
+    core_ref, block_ref, target_ref, cot_ref, weight_all, mixed_all,
+    out_ref, weight_next, mixed_next, scratch, sems,
+):
+    half = weight_next.shape[0]
+    own = pl.multiple_of(core_ref[0] * half, half)
+    copies = load_beside(
+        [
+            pltpu.make_async_copy(weight_all.at[pl.ds(own, half)], weight_next, sems.at[0]),
+            pltpu.make_async_copy(mixed_all, mixed_next, sems.at[1]),
+        ]
+    )
     tokens = cot_ref.shape[0]
     rows = unpack(block_ref[...], scratch)
-    size = rows.shape[0]
-    place = lax.broadcasted_iota(jnp.int32, (tokens, size), 1) + step * size
+    place = lax.broadcasted_iota(jnp.int32, (tokens, rows.shape[0]), 1)
     chosen = jnp.where(
         (place == target_ref[:, 0:1]) | (place == target_ref[:, 1:2]), 1.0, 0.0
     ).astype(bf16)
-    found = dot(chosen, rows, plain)
-
-    @pl.when(step == 0)
-    def _():
-        total[...] = found
-
-    @pl.when(step > 0)
-    def _():
-        total[...] = total[...] + found
-
-    @pl.when(step == pl.num_programs(0) - 1)
-    def _():
-        out_ref[...] = (cot_ref[...].astype(f32) + total[...]).astype(bf16)
-
-
-def combine(core, returned, target, cotangent):
-    experts, _, wide = returned.shape
-    half = wide - 128
+    out_ref[...] = (cot_ref[...].astype(f32) + dot(chosen, rows, plain)).astype(bf16)
+    finish(copies)
+
+
+def combine(core, returned, target, cotangent, weight, mixed):
+    half = returned.shape[2] - 128
     tokens = cotangent.shape[0]
     return pl.pallas_call(
         combine_kernel,
         grid_spec=pltpu.PrefetchScalarGridSpec(
             num_scalar_prefetch=1,
-            grid=(experts // (all_groups * group),),
+            grid=(1,),
             in_specs=[
-                pl.BlockSpec((all_groups * group, main, wide), lambda i, c: (i, 0, 0)),
+                resident,
                 whole((tokens, 8)),
                 pl.BlockSpec((tokens, half), lambda i, c: (0, c[0])),
-            ],
-            out_specs=whole((tokens, half)),
-            scratch_shapes=[pltpu.VMEM((tokens, half), f32), pltpu.VMEM((128, 128), f32)],
-        ),
-        out_shape=jax.ShapeDtypeStruct((tokens, half), bf16),
+                anywhere,
+                anywhere,
+            ],
+            out_specs=[whole((tokens, half)), anywhere, anywhere],
+            scratch_shapes=[pltpu.VMEM((128, 128), f32), pltpu.SemaphoreType.DMA((2,))],
+        ),
+        out_shape=[
+            jax.ShapeDtypeStruct((tokens, half), bf16),
+            pltpu.VMEM((half, weight.shape[1]), bf16),
+            pltpu.VMEM(mixed.shape, bf16),
+        ],
         compiler_params=params(),
         name="combine",
-    )(core, returned, held(target), held(cotangent))
-
-
-def two_terms(value):
-    high = value.astype(bf16)
-    return high, (value - high.astype(f32)).astype(bf16)
-
-
-def share_rows(values, owners):
-    value = values.astype(bf16).reshape(owners, 2 * main, values.shape[1])
-    return value[:, 0:main], value[:, main:]
-
-
-def own_kernel(core_ref, own_ref, weight_ref, mixed_ref, grad_ref, share_ref):
+    )(core, returned, held(target), held(cotangent), held(weight), held(mixed))
+
+
+def write_shares(ref, values):
+    pieces = values.astype(bf16).reshape(ref.shape[0], 4, 8, values.shape[1])
+    channels = values.shape[1]
+    for k in range(4):
+        ref[:, :, channels * k : channels * (k + 1)] = pieces[:, k]
+
+
+def own_kernel(
+    core_ref, own_ref, weight_ref, mixed_ref, weight_all, grad_ref, share_out, weight_next, share, sems
+):
+    half = weight_next.shape[0]
+    other = pl.multiple_of((1 - core_ref[0]) * half, half)
+    copies = load_beside(
+        [pltpu.make_async_copy(weight_all.at[pl.ds(other, half)], weight_next, sems.at[1])]
+    )
+    owners = share.shape[0]
+    at = pl.ds(pl.multiple_of(core_ref[0] * owners, owners), owners)
     own = own_ref[...]
+    write_shares(share, dot(own, mixed_ref[...], outer))
+    copy = pltpu.make_async_copy(share, share_out.at[at, :, pl.ds(0, share.shape[2])], sems.at[0])
+    copy.start()
     grad_ref[...] = dot(own, weight_ref[...], plain)
-    left, right = share_rows(dot(own, mixed_ref[...], outer), share_ref.shape[0])
-    channels = left.shape[2]
-    share_ref[:, :, 0:channels] = left
-    share_ref[:, :, channels:] = right
-
-
-def own_part(core, own, weight, mixed, owners):
+    copy.wait()
+    finish(copies)
+
+
+def own_part(core, own, weight_half, mixed, weight, owners):
     tokens, half = own.shape
     channels = mixed.shape[1]
     return pl.pallas_call(
@@ -626,93 +637,139 @@
             num_scalar_prefetch=1,
             grid=(1,),
             in_specs=[
-                whole((tokens, half)),
-                pl.BlockSpec((half, channels), lambda i, c: (c[0], 0)),
-                whole((tokens, channels)),
-            ],
-            out_specs=[whole((tokens, channels)), whole((owners // 2, main, 2 * channels))],
+                resident,
+                resident,
+                resident,
+                anywhere,
+            ],
+            out_specs=[whole((tokens, channels)), anywhere, anywhere],
+            scratch_shapes=[
+                pltpu.VMEM((owners // 2, 8, 4 * channels), bf16),
+                pltpu.SemaphoreType.DMA((2,)),
+            ],
         ),
         out_shape=[
             jax.ShapeDtypeStruct((tokens, channels), f32),
-            jax.ShapeDtypeStruct((owners // 2, main, 2 * channels), bf16),
+            pltpu.HBM((owners, 8, 4 * channels + 128), bf16),
+            pltpu.VMEM((half, channels), bf16),
         ],
         compiler_params=params(),
         cost_estimate=pl.CostEstimate(
             flops=4 * tokens * half * channels, transcendentals=0, bytes_accessed=4 << 20
         ),
         name="own_part",
-    )(core, own, weight, mixed)
+    )(core, own, near_by(weight_half), near_by(mixed), held(weight))
+
+
+def segment_scan(values, ahead_ref, state_grad, local):
+    blocks, tokens, span = state_grad.shape
+    length = tokens // segments
+    for b in range(blocks):
+        state_grad[b] = values[:, span * b : span * (b + 1)]
+    last = [None] * blocks
+    for j in reversed(range(length)):
+        at = pl.ds(j, segments, stride=length)
+        for b in range(blocks):
+            here = state_grad[b, at, :]
+            last[b] = here if last[b] is None else here + ahead_ref[b, at, :] * last[b]
+            local[b, at, :] = last[b]
+    return last
 
 
 def scan_kernel(
-    core_ref, peer_ref, weight_ref, mixed_ref, part_ref, share_ref, slope_ref, gelu_ref, ahead_ref,
-    product_ref, first_ref,
-    grad_y_out, local_out, share_out, head_out,
-    state_grad, grad_y, local, peer_share, lines, head, sems,
+    core_ref, peer_ref, weight_ref, mixed_ref, part_ref, gelu_ref, ahead_ref, product_ref, first_ref,
+    share_in, share_out, head_ref,
+    state_grad, local, share, lines, sems,
 ):
-    tokens, _ = peer_ref.shape
-    channels = weight_ref.shape[1]
-    core = core_ref[0]
-    owners = share_ref.shape[0]
-    own_at = pl.ds(pl.multiple_of(core * owners, owners), owners)
-    peer_at = pl.ds(pl.multiple_of((1 - core) * owners, owners), owners)
-    waits = []
-
-    def copy_out(source, target):
-        copy = pltpu.make_async_copy(source, target, sems.at[len(waits)])
-        copy.start()
-        waits.append(copy)
-
-    copy_out(share_ref, share_out.at[own_at, :, pl.ds(0, 2 * channels)])
+    owners = share.shape[0]
+    other = pl.ds(pl.multiple_of((1 - core_ref[0]) * owners, owners), owners)
+    columns = share.shape[2]
     peer = peer_ref[...]
     grad = part_ref[...] + dot(peer, weight_ref[...], plain)
-    grad_y[...] = grad * slope_ref[...]
-    copy_out(grad_y, grad_y_out)
+    write_shares(share, dot(peer, mixed_ref[...], outer))
+    main_copy = pltpu.make_async_copy(share, share_out.at[other, :, pl.ds(0, columns)], sems.at[0])
+    main_copy.start()
     values = grad * gelu_ref[...]
+    blocks, tokens, _ = state_grad.shape
     length = tokens // segments
-    blocks = state_grad.shape[0]
-    for b in range(blocks):
-        state_grad[b] = values[:, 128 * b : 128 * (b + 1)]
-    carries = []
+    last = segment_scan(values, ahead_ref, state_grad, local)
+    tiles = []
     for b in range(blocks):
         at = slice(128 * b, 128 * (b + 1))
-        value = None
-        for j in reversed(range(length)):
-            here = state_grad[b, pl.ds(j, segments, stride=length), :]
-            if value is None:
-                value = here
-            else:
-                value = here + ahead_ref[b, pl.ds(j, segments, stride=length), :] * value
-            local[b, pl.ds(j, segments, stride=length), :] = value
+        value = last[b]
         product = product_ref[b, pl.ds(0, segments, stride=length), :]
         carry = value[segments - 1 : segments]
         for s in reversed(range(1, segments - 1)):
             carry = value[s : s + 1] + product[s : s + 1] * carry
         ends = local[b, 0:3, :] + product_ref[b, 0:3, :] * carry
-        carries.append(first_ref[0:1, at] * ends[0:1])
-        head[:, at] = jnp.concatenate([ends, first_ref[3:15, at], jnp.zeros((1, 128), f32)], axis=0)
-    decay = jnp.concatenate([first_ref[1:2, 128 * b : 128 * (b + 1)] for b in range(blocks)], axis=0)
-    terms = two_terms(decay) + two_terms(jnp.concatenate(carries, axis=0))
-    line = jnp.concatenate([term.astype(f32) for term in terms], axis=0).astype(bf16)
+        tiles.append(first_ref[0:1, at] * ends[0:1])
+        head_ref[:, at] = jnp.concatenate(
+            [ends, first_ref[3:15, at], jnp.zeros((1, 128), f32)], axis=0
+        )
+    power = [first_ref[2:3, 128 * b : 128 * (b + 1)] for b in range(blocks)]
+    line = jnp.concatenate(power + tiles, axis=0).astype(bf16)
     lines[...] = jnp.broadcast_to(line[None], lines.shape)
-    copy_out(lines, share_out.at[:, :, pl.ds(2 * channels, 128)])
-    copy_out(local, local_out)
-    copy_out(head, head_out)
-    left, right = share_rows(dot(peer, mixed_ref[...], outer), owners)
-    peer_share[:, :, 0:channels] = left
-    peer_share[:, :, channels : 2 * channels] = right
-    copy_out(peer_share, share_out.at[peer_at, :, pl.ds(0, 2 * channels)])
-    for copy in waits:
-        copy.wait()
-
-
-def scan(core, peer, weight, mixed, part, share, slope, gelu, ahead, product, first):
+    line_copy = pltpu.make_async_copy(lines, share_out.at[:, :, pl.ds(columns, 128)], sems.at[1])
+    line_copy.start()
+    main_copy.wait()
+    line_copy.wait()
+
+
+def scan(core, peer, weight, mixed, part, shares, gelu, ahead, product, first):
     tokens, half = peer.shape
     channels = weight.shape[1]
-    owners, rows, _ = share.shape
-    out_shape = (2 * owners, rows, 2 * channels + 128)
+    owners = shares.shape[0]
     return pl.pallas_call(
         scan_kernel,
+        grid_spec=pltpu.PrefetchScalarGridSpec(
+            num_scalar_prefetch=1,
+            grid=(1,),
+            in_specs=[
+                resident,
+                resident,
+                resident,
+                resident,
+                resident,
+                resident,
+                resident,
+                resident,
+                anywhere,
+            ],
+            out_specs=[anywhere, whole((16, channels))],
+            scratch_shapes=[
+                pltpu.VMEM(ahead.shape, f32),
+                pltpu.VMEM(ahead.shape, f32),
+                pltpu.VMEM((owners // 2, 8, 4 * channels), bf16),
+                pltpu.VMEM((owners, 8, 128), bf16),
+                pltpu.SemaphoreType.DMA((2,)),
+            ],
+        ),
+        out_shape=[pltpu.HBM(shares.shape, bf16), pltpu.HBM((16, channels), f32)],
+        input_output_aliases={9: 0},
+        compiler_params=params(),
+        cost_estimate=pl.CostEstimate(
+            flops=4 * tokens * half * channels, transcendentals=0, bytes_accessed=9 << 20
+        ),
+        name="scan",
+    )(
+        core, peer, near_by(weight), near_by(mixed), part, gelu, ahead, product, first, held(shares)
+    )
+
+
+def local_kernel(
+    core_ref, peer_ref, weight_ref, part_ref, slope_ref, gelu_ref, ahead_ref,
+    grad_y_ref, local_ref, state_grad,
+):
+    grad = part_ref[...] + dot(peer_ref[...], weight_ref[...], plain)
+    grad_y_ref[...] = grad * slope_ref[...]
+    segment_scan(grad * gelu_ref[...], ahead_ref, state_grad, local_ref)
+
+
+def local_scan(core, peer, weight, part, slope, gelu, ahead):
+    tokens, half = peer.shape
+    channels = weight.shape[1]
+    return pl.pallas_call(
+        local_kernel,
         grid_spec=pltpu.PrefetchScalarGridSpec(
             num_scalar_prefetch=1,
             grid=(1,),
@@ -721,108 +778,132 @@
                 pl.BlockSpec((half, channels), lambda i, c: (1 - c[0], 0)),
                 whole((tokens, channels)),
                 whole((tokens, channels)),
-                whole(share.shape),
-                whole((tokens, channels)),
                 whole((tokens, channels)),
                 whole(ahead.shape),
-                whole(ahead.shape),
-                whole((16, channels)),
-            ],
-            out_specs=[anywhere] * 4,
-            scratch_shapes=[
-                pltpu.VMEM(ahead.shape, f32),
-                pltpu.VMEM((tokens, channels), f32),
-                pltpu.VMEM(ahead.shape, f32),
-                pltpu.VMEM(share.shape, bf16),
-                pltpu.VMEM((2 * owners, rows, 128), bf16),
-                pltpu.VMEM((16, channels), f32),
-                pltpu.SemaphoreType.DMA((6,)),
-            ],
-        ),
-        out_shape=[
-            pltpu.HBM((tokens, channels), f32),
-            pltpu.HBM(ahead.shape, f32),
-            pltpu.HBM(out_shape, bf16),
-            pltpu.HBM((16, channels), f32),
-        ],
+            ],
+            out_specs=[whole((tokens, channels)), whole(ahead.shape)],
+            scratch_shapes=[pltpu.VMEM(ahead.shape, f32)],
+        ),
+        out_shape=[pltpu.HBM((tokens, channels), f32), pltpu.HBM(ahead.shape, f32)],
         compiler_params=params(),
         cost_estimate=pl.CostEstimate(
-            flops=4 * tokens * half * channels, transcendentals=0, bytes_accessed=9 << 20
-        ),
-        name="scan",
-    )(core, peer, weight, mixed, part, share, slope, gelu, ahead, product, first)
+            flops=2 * tokens * half * channels, transcendentals=0, bytes_accessed=9 << 20
+        ),
+        name="local_scan",
+    )(core, held(peer), held(weight), held(part), held(slope), held(gelu), held(ahead))
 
 
 def tail_kernel(
-    place_ref, line_ref, head_ref, local_ref, product_ref, keep_ref, input_ref, direct_ref,
-    a_ref, i_ref, taps_ref, out_ref, carries, adjoint, grads,
+    place_ref, share_ref, head_ref, taps_ref, a_ref, i_ref, *rest,
 ):
-    step = pl.program_id(0)
-    tokens = local_ref.shape[1]
+    sources, (out_hbm, project_ref), stores = rest[0:5], rest[5:7], rest[7:]
+    local_ref, product_ref, keep_ref, input_ref, direct_ref = buffers = stores[0:5]
+    adjoint, grads, out, in_sems, out_sems = stores[5:]
+    blocks, tokens, span = local_ref.shape
     length = tokens // segments
     place = place_ref[0]
 
-    @pl.when(step == 0)
-    def _():
-        own = jnp.zeros((4, 128), f32)
-        beyond = jnp.zeros((4, 128), f32)
-        for j in reversed(range(line_ref.shape[0])):
-            line = line_ref[j].astype(f32)
-            decay = line[0:4] + line[4:8]
-            total = line[8:12] + line[12:16]
-            own = jnp.where(j > place, total + decay * own, own)
-            beyond = jnp.where(j > place + 1, total + decay * beyond, beyond)
-        carries[0:4, :] = own
-        carries[4:8, :] = beyond
-
-    def conv_grad(value, keep, gate, direct):
-        keep = (value * keep).astype(bf16)
-        gate = (value * gate).astype(bf16)
-        return value * direct + dot(keep, a_ref[0], inner) + dot(gate, i_ref[0], inner)
-
-    carry = carries[pl.ds(step, 1), :]
-    for s in reversed(range(segments)):
-        lo = s * length
-        piece = local_ref[0, lo : lo + length, :] + product_ref[0, lo : lo + length, :] * carry
-        adjoint[lo : lo + length, :] = piece
-        carry = piece[0:1]
-    grads[0:tokens, :] = conv_grad(adjoint[...], keep_ref[...], input_ref[...], direct_ref[...])
-    head = head_ref[...]
-    spare = jnp.zeros((5, 128), f32)
-    three = lambda k: jnp.concatenate([head[3 * k : 3 * k + 3], spare], axis=0)
-    later = three(0) + three(1) * carries[pl.ds(step + 4, 1), :]
-    grads[tokens : tokens + 8, :] = conv_grad(later, three(2), three(3), three(4))
-    total = taps_ref[0:1, :] * grads[3 : 3 + tokens, :]
-    for j in range(1, 4):
-        total = total + taps_ref[j : j + 1, :] * grads[3 - j : 3 - j + tokens, :]
-    out_ref[...] = total
+    def column(ref, c):
+        return ref.at[c] if len(ref.shape) == 3 else ref.at[:, pl.ds(span * c, span)]
+
+    copies = [
+        [
+            pltpu.make_async_copy(column(source, c), column(buffer, c), in_sems.at[c, k])
+            for k, (source, buffer) in enumerate(zip(sources, buffers))
+        ]
+        for c in range(blocks)
+    ]
+    for group_copies in copies:
+        for copy in group_copies:
+            copy.start()
+
+    own = jnp.zeros((4, span), f32)
+    beyond = jnp.zeros((4, span), f32)
+    columns = share_ref.shape[2] - 128
+    channels = columns // 4
+    summed = jnp.zeros((8, columns), f32)
+    for j in reversed(range(share_ref.shape[0])):
+        share = share_ref[j].astype(f32)
+        summed = summed + share[:, 0:columns]
+        line = share[:, columns:]
+        decay = jnp.exp(-line[0:4])
+        own = jnp.where(j > place, line[4:8] + decay * own, own)
+        beyond = jnp.where(j > place + 1, line[4:8] + decay * beyond, beyond)
+
+    for k in range(4):
+        project_ref[8 * k : 8 * (k + 1), :] = summed[:, channels * k : channels * (k + 1)]
+    results = []
+    for c in range(blocks):
+        at = slice(span * c, span * (c + 1))
+
+        def conv_grad(value, keep, gate, direct):
+            keep = (value * keep).astype(bf16)
+            gate = (value * gate).astype(bf16)
+            return value * direct + dot(keep, a_ref[c], inner) + dot(gate, i_ref[c], inner)
+
+        for copy in copies[c]:
+            copy.wait()
+        carry = own[c : c + 1]
+        for s in reversed(range(segments)):
+            rows = slice(s * length, (s + 1) * length)
+            piece = local_ref[c, rows, :] + product_ref[c, rows, :] * carry
+            adjoint[rows, :] = piece
+            carry = piece[0:1]
+        grads[0:tokens, :] = conv_grad(
+            adjoint[...], keep_ref[:, at], input_ref[:, at], direct_ref[:, at]
+        )
+        head = head_ref[:, at]
+        spare = jnp.zeros((5, span), f32)
+        three = lambda k: jnp.concatenate([head[3 * k : 3 * k + 3], spare], axis=0)
+        later = three(0) + three(1) * beyond[c : c + 1]
+        grads[tokens : tokens + 8, :] = conv_grad(later, three(2), three(3), three(4))
+        total = taps_ref[0:1, at] * grads[3 : 3 + tokens, :]
+        for j in range(1, 4):
+            total = total + taps_ref[j : j + 1, at] * grads[3 - j : 3 - j + tokens, :]
+        out[:, at] = total
+        results.append(
+            pltpu.make_async_copy(column(out, c), column(out_hbm, c), out_sems.at[c])
+        )
+        results[-1].start()
+    for copy in results:
+        copy.wait()
 
 
 def tail(place, shares, head, local, product, keep, gate, direct, gate_a, gate_x, taps):
     blocks, tokens, span = local.shape
     channels = blocks * span
-    owners, rows, _ = shares.shape
-    cube = pl.BlockSpec((1, tokens, span), lambda i, c: (i, 0, 0))
-    col = lambda rows: pl.BlockSpec((rows, span), lambda i, c: (0, i))
-    block = pl.BlockSpec((1, span, span), lambda i, c: (i, 0, 0))
-    line = pl.BlockSpec((owners, rows, 128), lambda i, c: (0, 0, 2 * channels // 128))
+    rows = shares.shape[1]
+    sources = (local, product, keep, gate, direct)
     return pl.pallas_call(
         tail_kernel,
         grid_spec=pltpu.PrefetchScalarGridSpec(
             num_scalar_prefetch=1,
-            grid=(blocks,),
-            in_specs=[line, col(16), cube, cube] + [col(tokens)] * 3 + [block, block, col(4)],
-            out_specs=col(tokens),
-            scratch_shapes=[
-                pltpu.VMEM((8, span), f32),
+            grid=(1,),
+            in_specs=[
+                resident,
+                resident,
+                whole((4, channels)),
+                whole(gate_a.shape),
+                whole(gate_x.shape),
+            ]
+            + [anywhere] * 5,
+            out_specs=[anywhere, whole((4 * rows, channels))],
+            scratch_shapes=[pltpu.VMEM(value.shape, f32) for value in sources]
+            + [
                 pltpu.VMEM((tokens, span), f32),
                 pltpu.VMEM((tokens + 8, span), f32),
-            ],
-        ),
-        out_shape=jax.ShapeDtypeStruct((tokens, channels), f32),
+                pltpu.VMEM((tokens, channels), f32),
+                pltpu.SemaphoreType.DMA((blocks, 5)),
+                pltpu.SemaphoreType.DMA((blocks,)),
+            ],
+        ),
+        out_shape=[
+            pltpu.HBM((tokens, channels), f32),
+            pltpu.HBM((4 * rows, channels), f32),
+        ],
         compiler_params=params(),
         name="tail",
-    )(place, shares, head, held(local), product, keep, gate, direct, held(gate_a), held(gate_x), held(taps))
+    )(place, shares, head, held(taps), held(gate_a), held(gate_x), *(held(v) for v in sources))
 
 
 def exchange(value, axis):
@@ -860,7 +941,6 @@
     experts = lax.axis_size("sp")
     core = lax.axis_index("tp").astype(jnp.int32).reshape(1)
     taps = conv_taps.shape[0]
-    channels = in_x.shape[1]
 
     place = lax.axis_index("sp").astype(jnp.int32).reshape(1)
 
@@ -891,20 +971,23 @@
     grad_gate, grad_up = grad_in(packed, adj)
     grad_down = grad_down_of(core, active, arrived, arrived_far)
 
-    stream_own = combine(core, returned, target, cotangent)
+    stream_own, weight_half, mixed_here = combine(
+        core, returned, target, cotangent, out_weight, mixed
+    )
     stream_peer = swapped(stream_own)
-    part, share = own_part(core, stream_own, out_weight, mixed, experts)
-    grad_y, local, outgoing, head = scan(
-        core, stream_peer, out_weight, mixed, part, share, y_slope, gelu, ahead, product, first
-    )
+    part, shares, weight_half = own_part(
+        core, stream_own, weight_half, mixed_here, out_weight, experts
+    )
+    outgoing, head = scan(
+        core, stream_peer, weight_half, mixed_here, part, shares, gelu, ahead, product, first
+    )
+    grad_y, local = local_scan(core, stream_peer, out_weight, part, y_slope, gelu, ahead)
     head = shifted(head, "sp", -1)
     shares = exchange(outgoing, "sp")
-    grad_x = tail(
+    grad_x, grad_proj = tail(
         place, shares, head, local, product, keep_part, input_part, direct,
         gate_a, gate_x, conv_taps,
     )
-    summed = jnp.sum(shares[:, :, : 2 * channels].astype(f32), axis=0)
-    grad_proj = jnp.concatenate([summed[:, :channels], summed[:, channels:]], axis=0)
     return (grad_gate[None], grad_up[None], grad_down[None], grad_proj, grad_x, grad_y)
 
 

time: 192 us -> 181 us (0.943)
  waiting for transfers between devices: 55.6 us -> 37 us
  Pallas kernels: 60.5 us -> 68.1 us
  starting transfers between devices: 19.6 us -> 22.8 us
  local copies, waits for them, and re-layouts: 8.13 us -> 5.93 us
    all_to_all x2, waiting for transfers between devices: 39.3 us -> 3.04 us  [exchange(): return lax.all_to_all(value, axis, split_axis=0, concat_axis=0, tiled=True)]
    ppermute x2, waiting for transfers between devices: 7.54 us -> 24.7 us  [shifted(): return lax.ppermute(value, axis, pairs)]
    pallas_call x0 -> x1, Pallas kernels: none -> 4.68 us  [local_scan(): pl.pallas_call(local_kernel, grid_spec=pltpu.PrefetchScalarGridSpec(num_s...]
    unnamed x42 -> x34, local copies, waits for them, and re-layouts: 5.9 us -> 3.71 us
  transfers between devices with their start and end apart: 9 -> 9, of which waited for: 5 -> 5; matrix products, arithmetic and copies ran while one was open for 2% -> 1% of each run, Pallas kernels for 21% -> 26%
where the time goes in v6:
time: 181 us; the launch traced here: 178 us
  Pallas kernels  68.1 us (38%)
  blocking collectives  43.1 us (24%)
  waiting for transfers between devices  37 us (20%)
  starting transfers between devices  22.8 us (13%)
  local copies, waits for them, and re-layouts  5.93 us (3%)
    all_to_all x1, blocking collectives, exchange(): return lax.all_to_all(value, axis, split_axis=0, concat_axis=0, tiled=True)  43.1 us
    ppermute x2, waiting for transfers between devices, shifted(): return lax.ppermute(value, axis, pairs)  24.7 us
    all_to_all x2, starting transfers between devices, exchange(): return lax.all_to_all(value, axis, split_axis=0, concat_axis=0, tiled=True)  12.4 us
    pallas_call x1, Pallas kernels, expert_pre(): pl.pallas_call(expert_pre_kernel, grid=(count // size,), in_specs=[by_row...  11.9 us
    ppermute x2, starting transfers between devices, shifted(): return lax.ppermute(value, axis, pairs)  10.2 us
    ppermute x5, waiting for transfers between devices, swapped(): return lax.ppermute(value, 'tp', [(0, 1), (1, 0)])  9.25 us
    pallas_call x1, Pallas kernels, grad_in(): pl.pallas_call(grad_in_kernel, grid=(model // size,), in_specs=[pl.BlockS...  9.1 us
    pallas_call x1, Pallas kernels, grad_down_of(): pl.pallas_call(grad_down_kernel, grid_spec=pltpu.PrefetchScalarGridSpec(n...  7.19 us
  transfers between devices with their start and end apart: 9, of which 5 were waited for; matrix products, arithmetic and copies ran while one was open for 1% of the time, Pallas kernels for 26%

profile of v6, /device:TPU:32, one launch (start us, length us, event | category | flops | bytes accessed | tf_op | source)
XLA Modules:
  0.0 178.1 jit_solution(11877756470333065994)
XLA Ops:
  0.6 4.3 %send.1 = (bf16[64,16,1152]{2,1,0:T(8,128)(2,1)}, s32[8,384]{1,0:T(8,128)S(1)}) custom-call(s32[1]{0:T(128)} %bitcast.3.core_ref, s32[2,384]{1,0:T(2,128)} %bitcast.22, f32[2,384]{1,0:T(2,128)} %bitcast.23, bf16[384,2048]{1,0:T(8,128)(2,1)} %cot_ref.3), custom_call_target="tpu_custom_call" | custom-call | tf_op jit(solution)/shard_map/send/pallas_call | solution.py:104
  5.0 43.1 %all_to_all.15.block_ref.near_ref = bf16[64,16,1152]{2,1,0:T(8,128)(2,1)S(1)} all-to-all(bf16[64,16,1152]{2,1,0:T(8,128)(2,1)} %get-tuple-element.44), channel_id=1, replica_groups=mesh['sp'=64,'tp'=2] {'sp'}, dimensions={0} | all-to-all | bytes 4718592 | tf_op jit(solution)/shard_map/all_to_all | solution.py:910
  48.1 0.0 collective-permute-start
  48.1 11.9 %expert_pre.1 = (bf16[1152,2048]{1,0:T(8,128)(2,1)}, f32[1152,512]{1,0:T(8,128)}, f32[1152,512]{1,0:T(8,128)}, bf16[1152,512]{1,0:T(8,128)(2,1)}) custom-call(bf16[1152,2048]{1,0:T(8,128)(2,1)} %bitcast.25, bf16[2048,512]{1,0:T(8,128)(2,1)} %bitcast.15, bf16[2048,512]{1,0:T(8,128)(2,1)} %bitcast.18), custom_call_target="tpu_custom_call" | custom-call | flops 4831838208 | bytes 20971520 | tf_op jit(solution)/shard_map/expert_pre/pallas_call | solution.py:165
  60.0 3.0 %near.1 = (f32[1152,512]{1,0:T(8,128)S(1)}, bf16[512,1024]{1,0:T(8,128)(2,1)S(1)}) custom-call(s32[1]{0:T(128)} %bitcast.3.core_ref, bf16[64,16,1152]{2,1,0:T(8,128)(2,1)S(1)} %all_to_all.15.block_ref.near_ref, bf16[512,2048]{1,0:T(8,128)(2,1)} %bitcast.13, bf16[512,2048]{1,0:T(8,128)(2,1)} %bitcast.14), custom_call_target="tpu_custom_call" | custom-call | flops 1207959552 | bytes 9437184 | tf_op jit(solution)/shard_map/near/pallas_call | solution.py:336
  63.0 0.0 collective-permute-done.block_ref.far_ref
  63.0 0.0 copy-start.6
  63.0 0.0 copy-done.7
  63.0 0.0 copy-done.8
  63.0 0.0 copy-start.11
  63.0 0.0 copy-start.12
  63.0 2.4 %far.1 = (bf16[1152,1024]{1,0:T(8,128)(2,1)S(1)}, bf16[1024,512]{1,0:T(8,128)(2,1)S(1)}, bf16[1024,512]{1,0:T(8,128)(2,1)S(1)}) custom-call(s32[1]{0:T(128)} %bitcast.3.core_ref, bf16[64,16,1152]{2,1,0:T(8,128)(2,1)S(1)} %collective-permute-done.block_ref.far_ref, bf16[512,1024]{1,0:T(8,128)(2,1)S(1)} %get-tuple-element.45.down_ref, ...), custom_call_target="tpu_custom_call" | custom-call | flops 1207959552 | bytes 16777216 | tf_op jit(solution)/shard_map/far/pallas_call | solution.py:387
  65.5 0.1 collective-permute-start.1
  65.6 0.5 copy-done.11
  66.1 0.0 collective-permute-start.2
  66.1 1.2 copy-done.12
  67.3 0.0 collective-permute-start.3
  67.3 5.8 %collective-permute-done.2.gate_all = bf16[2048,512]{1,0:T(8,128)(2,1)S(1)} collective-permute-done((bf16[2048,512]{1,0:T(8,128)(2,1)S(1)}, bf16[2048,512]{1,0:T(8,128)(2,1)S(1)}, u32[]{:S(2)}, u32[]{:S(2)}) %collective-permute-start.2) | collective-permute-done | bytes 2097184 | tf_op jit(solution)/shard_map/ppermute | solution.py:914
  73.1 3.0 %collective-permute-done.3.up_all = bf16[2048,512]{1,0:T(8,128)(2,1)S(1)} collective-permute-done((bf16[2048,512]{1,0:T(8,128)(2,1)S(1)}, bf16[2048,512]{1,0:T(8,128)(2,1)S(1)}, u32[]{:S(2)}, u32[]{:S(2)}) %collective-permute-start.3) | collective-permute-done | bytes 2097184 | tf_op jit(solution)/shard_map/ppermute | solution.py:914
  76.1 0.0 copy-done.14
  76.1 1.3 copy-done.15
  77.4 2.7 %back_own.1 = (bf16[1152,1024]{1,0:T(8,128)(2,1)S(1)}, bf16[1024,512]{1,0:T(8,128)(2,1)S(1)}, bf16[1024,512]{1,0:T(8,128)(2,1)S(1)}) custom-call(s32[1]{0:T(128)} %bitcast.3.core_ref, bf16[1152,1024]{1,0:T(8,128)(2,1)S(1)} %get-tuple-element.49.adj_ref, bf16[1024,512]{1,0:T(8,128)(2,1)S(1)} %get-tuple-element.53.gate_ref, ...), custom_call_target="tpu_custom_call" | custom-call | flops 2415919104 | bytes 7340032 | tf_op jit(solution)/shard_map/back_own/pallas_call | solution.py:443
  80.1 0.0 collective-permute-done.1.adj_ref
  80.1 4.0 %back_sum.1 = bf16[64,16,1152]{2,1,0:T(8,128)(2,1)} custom-call(bf16[1152,1024]{1,0:T(8,128)(2,1)S(1)} %collective-permute-done.1.adj_ref, bf16[1152,1024]{1,0:T(8,128)(2,1)S(1)} %get-tuple-element.55.own_ref, bf16[1024,512]{1,0:T(8,128)(2,1)S(1)} %get-tuple-element.56.gate_ref, bf16[1024,512]{1,0:T(8,128)(2,1)S(1)} %get-tuple-element.57.up_ref), custom_call_target="tpu_custom_call" | custom-call | flops 2415919104 | bytes 7340032 | tf_op jit(solution)/shard_map/back_sum/pallas_call | solution.py:481
  84.2 6.4 %all-to-all-start.1 = ((bf16[64,16,1152]{2,1,0:T(8,128)(2,1)}), bf16[64,16,1152]{2,1,0:T(8,128)(2,1)S(1)}, u32[]{:S(2)}, u32[]{:S(2)}) async-start(bf16[64,16,1152]{2,1,0:T(8,128)(2,1)} %back_sum.1), calls=%async_computation.1 | async-start | bytes 4718592 | tf_op jit(solution)/shard_map/all_to_all | solution.py:910
  90.5 0.7 slice.7
  91.2 0.7 slice.6
  91.9 3.6 %collective-permute-start.4 = (bf16[4,512]{1,0:T(4,128)(2,1)S(1)}, bf16[4,512]{1,0:T(4,128)(2,1)S(1)}, u32[]{:S(2)}, u32[]{:S(2)}) collective-permute-start(bf16[4,512]{1,0:T(4,128)(2,1)S(1)} %pad_maximum_fusion), channel_id=1, source_target_pairs={{0,2},{2,4},{4,6},{6,8},{8,10},{10,12},{12,14},{14,16},{16,18},{18... | collective-permute-start | bytes 12296 | tf_op jit(solution)/shard_map/ppermute | solution.py:920
  95.5 0.8 copy.22
  96.3 24.7 %collective-permute-done.4.edge_ref = bf16[4,512]{1,0:T(4,128)(2,1)S(1)} collective-permute-done((bf16[4,512]{1,0:T(4,128)(2,1)S(1)}, bf16[4,512]{1,0:T(4,128)(2,1)S(1)}, u32[]{:S(2)}, u32[]{:S(2)}) %collective-permute-start.4) | collective-permute-done | bytes 4128 | tf_op jit(solution)/shard_map/ppermute | solution.py:920
  121.0 0.6 copy-done.13
  121.6 5.2 %recur_pre.1 = (bf16[384,512]{1,0:T(8,128)(2,1)}, f32[384,512]{1,0:T(8,128)}, f32[384,512]{1,0:T(8,128)}, f32[4,384,128]{2,1,0:T(8,128)}, f32[4,384,128]{2,1,0:T...) custom-call(bf16[384,512]{1,0:T(8,128)(2,1)} %x_ref.1, ...), custom_call_target="tpu_custom_call" | custom-call | flops 393216000 | bytes 8388608 | tf_op jit(solution)/shard_map/recur_pre/pallas_call | solution.py:252
  126.8 0.0 all-to-all-done.1.block_ref
  126.8 3.5 %combine.1 = (bf16[384,1024]{1,0:T(8,128)(2,1)S(1)}, bf16[1024,512]{1,0:T(8,128)(2,1)S(1)}, bf16[384,512]{1,0:T(8,128)(2,1)S(1)}) custom-call(s32[1]{0:T(128)} %bitcast.3.core_ref, bf16[64,16,1152]{2,1,0:T(8,128)(2,1)S(1)} %all-to-all-done.1.block_ref, s32[384,8]{1,0:T(8,128)} %bitcast.21, bf16[384,2048]{1,0:T(8,128)(2,1)} %cot_ref.3, ...), custom_call_target="tpu_custom_call" | custom-call | tf_op jit(solution)/shard_map/combine/pallas_call | solution.py:580
  130.4 0.0 copy-start.9
  130.4 0.1 collective-permute-start.5
  130.5 1.8 %own_part.1 = (f32[384,512]{1,0:T(8,128)S(1)}, bf16[64,8,2176]{2,1,0:T(8,128)(2,1)}, bf16[1024,512]{1,0:T(8,128)(2,1)S(1)}) custom-call(s32[1]{0:T(128)} %bitcast.3.core_ref, bf16[384,1024]{1,0:T(8,128)(2,1)S(1)} %get-tuple-element.60.own_ref, bf16[1024,512]{1,0:T(8,128)(2,1)S(1)} %get-tuple-element.61.weight_ref, ...), custom_call_target="tpu_custom_call" | custom-call | flops 805306368 | bytes 4194304 | tf_op jit(solution)/shard_map/own_part/pallas_call | solution.py:634
  132.3 0.5 collective-permute-done.5.peer_ref
  132.8 3.1 %scan.1 = (bf16[64,8,2176]{2,1,0:T(8,128)(2,1)}, f32[16,512]{1,0:T(8,128)}) custom-call(s32[1]{0:T(128)} %bitcast.3.core_ref, bf16[384,1024]{1,0:T(8,128)(2,1)S(1)} %collective-permute-done.5.peer_ref, bf16[1024,512]{1,0:T(8,128)(2,1)S(1)} %get-tuple-element.63.weight_ref, ...), custom_call_target="tpu_custom_call", output_to_operand_aliasing={{0}: (9, {})} | custom-call | flops 805306368 | bytes 9437184 | tf_op jit(solution)/shard_map/scan/pallas_call | solution.py:722
  136.0 6.1 %all-to-all-start.2 = ((bf16[64,8,2176]{2,1,0:T(8,128)(2,1)}), bf16[64,8,2176]{2,1,0:T(8,128)(2,1)S(1)}, u32[]{:S(2)}, u32[]{:S(2)}) async-start(bf16[64,8,2176]{2,1,0:T(8,128)(2,1)} %get-tuple-element.70), calls=%async_computation.2 | async-start | bytes 4456448 | tf_op jit(solution)/shard_map/all_to_all | solution.py:910
  142.0 7.2 %grad_down.1 = bf16[512,2048]{1,0:T(8,128)(2,1)} custom-call(s32[1]{0:T(128)} %bitcast.3.core_ref, bf16[1152,512]{1,0:T(8,128)(2,1)} %get-tuple-element.52.active_ref, bf16[64,16,1152]{2,1,0:T(8,128)(2,1)} %copy-done, bf16[64,16,1152]{2,1,0:T(8,128)(2,1)} %copy-done.6), custom_call_target="tpu_custom_call" | custom-call | flops 2415919104 | bytes 9437184 | tf_op jit(solution)/shard_map/grad_down/pallas_call | solution.py:537
  149.2 9.1 %grad_in.1 = (bf16[2048,512]{1,0:T(8,128)(2,1)}, bf16[2048,512]{1,0:T(8,128)(2,1)}) custom-call(bf16[1152,2048]{1,0:T(8,128)(2,1)} %get-tuple-element.43.packed_ref, bf16[1152,1024]{1,0:T(8,128)(2,1)} %copy-done.10), custom_call_target="tpu_custom_call" | custom-call | flops 4831838208 | bytes 11534336 | tf_op jit(solution)/shard_map/grad_in/pallas_call | solution.py:508
  158.3 0.0 copy-done.16
  158.3 6.7 %collective-permute-start.6 = (f32[16,512]{1,0:T(8,128)S(1)}, f32[16,512]{1,0:T(8,128)S(1)}, u32[]{:S(2)}, u32[]{:S(2)}) collective-permute-start(f32[16,512]{1,0:T(8,128)S(1)} %copy-done.16), channel_id=1, source_target_pairs={{2,0},{4,2},{6,4},{8,6},{10,8},{12,10},{14,12},{16,14},{18,16},{20... | collective-permute-start | bytes 98312 | tf_op jit(solution)/shard_map/ppermute | solution.py:920
  165.0 4.7 %local_scan.1 = (f32[384,512]{1,0:T(8,128)}, f32[4,384,128]{2,1,0:T(8,128)}) custom-call(s32[1]{0:T(128)} %bitcast.3.core_ref, bf16[384,1024]{1,0:T(8,128)(2,1)} %copy-done.4, bf16[2048,512]{1,0:T(8,128)(2,1)} %weight_ref.1, f32[384,512]{1,0:T(8,128)} %copy-done.5, f32[384,512]{1,0:T(8,128)} %get-tuple-element.72.slope_ref, ...), custom_call_target="tpu_custom_call" | custom-call | flops 402653184 | bytes 9437184 | tf_op jit(solution)/shard_map/local_scan/pallas_call | solution.py:771
  169.7 0.0 collective-permute-done.6.head_ref
  169.7 3.0 %all-to-all-done.2.share_ref = bf16[64,8,2176]{2,1,0:T(8,128)(2,1)S(1)} async-done(((bf16[64,8,2176]{2,1,0:T(8,128)(2,1)}), bf16[64,8,2176]{2,1,0:T(8,128)(2,1)S(1)}, u32[]{:S(2)}, u32[]{:S(2)}) %all-to-all-start.2) | async-done | bytes 2228256 | tf_op jit(solution)/shard_map/all_to_all | solution.py:910
  172.7 5.2 %tail.1 = (f32[384,512]{1,0:T(8,128)}, f32[32,512]{1,0:T(8,128)}) custom-call(s32[1]{0:T(128)} %bitcast.10.place_ref, bf16[64,8,2176]{2,1,0:T(8,128)(2,1)S(1)} %all-to-all-done.2.share_ref, f32[16,512]{1,0:T(8,128)S(1)} %collective-permute-done.6.head_ref, f32[4,512]{1,0:T(4,128)} %taps_ref.3, bf16[4,128,128]{2,1,0:T(8,128)(2,1)} %a_ref.3, ...), custom_call_target="tpu_custom_call" | custom-call | tf_op jit(solution)/shard_map/tail/pallas_call | solution.py:877
  (23 shorter events, 0.1 us)
Async XLA Ops:
  48.1 11.9 %copy-start = (bf16[64,16,1152]{2,1,0:T(8,128)(2,1)}, bf16[64,16,1152]{2,1,0:T(8,128)(2,1)S(1)}, u32[]{:S(2)}) copy-start(bf16[64,16,1152]{2,1,0:T(8,128)(2,1)S(1)} %all_to_all.15.block_ref.near_ref) | copy-start | bytes 7077892
  48.1 14.9 %collective-permute-start = (bf16[64,16,1152]{2,1,0:T(8,128)(2,1)S(1)}, bf16[64,16,1152]{2,1,0:T(8,128)(2,1)S(1)}, u32[]{:S(2)}, u32[]{:S(2)}) collective-permute-start(bf16[64,16,1152]{2,1,0:T(8,128)(2,1)S(1)} %all_to_all.15.block_ref.near_ref), channel_id=1, source_target_pairs={{0,1},{1,0},{2,3},{3,2},{4,5},{5,4},{6,7},{7,6},{8,9},{9,8},{10,11... | collective-permute-start | bytes 7077896 | tf_op jit(solution)/shard_map/ppermute | solution.py:914
  60.0 3.0 %copy-start.7 = (f32[1152,512]{1,0:T(8,128)S(1)}, f32[1152,512]{1,0:T(8,128)}, u32[]{:S(2)}) copy-start(f32[1152,512]{1,0:T(8,128)} %get-tuple-element.47.silu_ref) | copy-start | bytes 7077892
  60.0 3.0 %copy-start.8 = (f32[1152,512]{1,0:T(8,128)S(1)}, f32[1152,512]{1,0:T(8,128)}, u32[]{:S(2)}) copy-start(f32[1152,512]{1,0:T(8,128)} %get-tuple-element.48.slope_ref) | copy-start | bytes 7077892
  63.0 2.5 %copy-start.6 = (bf16[64,16,1152]{2,1,0:T(8,128)(2,1)}, bf16[64,16,1152]{2,1,0:T(8,128)(2,1)S(1)}, u32[]{:S(2)}) copy-start(bf16[64,16,1152]{2,1,0:T(8,128)(2,1)S(1)} %collective-permute-done.block_ref.far_ref) | copy-start | bytes 7077892
  63.0 3.1 %copy-start.11 = (bf16[1,2048,512]{2,1,0:T(8,128)(2,1)S(1)}, bf16[1,2048,512]{2,1,0:T(8,128)(2,1)}, u32[]{:S(2)}) copy-start(bf16[1,2048,512]{2,1,0:T(8,128)(2,1)} %param.19) | copy-start | bytes 6291460
  63.0 4.3 %copy-start.12 = (bf16[1,2048,512]{2,1,0:T(8,128)(2,1)S(1)}, bf16[1,2048,512]{2,1,0:T(8,128)(2,1)}, u32[]{:S(2)}) copy-start(bf16[1,2048,512]{2,1,0:T(8,128)(2,1)} %param.20) | copy-start | bytes 6291460
  65.5 14.6 %copy-start.10 = (bf16[1152,1024]{1,0:T(8,128)(2,1)}, bf16[1152,1024]{1,0:T(8,128)(2,1)S(1)}, u32[]{:S(2)}) copy-start(bf16[1152,1024]{1,0:T(8,128)(2,1)S(1)} %get-tuple-element.49.adj_ref) | copy-start | bytes 7077892
  65.5 14.6 %collective-permute-start.1 = (bf16[1152,1024]{1,0:T(8,128)(2,1)S(1)}, bf16[1152,1024]{1,0:T(8,128)(2,1)S(1)}, u32[]{:S(2)}, u32[]{:S(2)}) collective-permute-start(bf16[1152,1024]{1,0:T(8,128)(2,1)S(1)} %get-tuple-element.49.adj_ref), channel_id=1, source_target_pairs={{0,1},{1,0},{2,3},{3,2},{4,5},{5,4},{6,7},{7,6},{8,9},{9,8},{10,11... | collective-permute-start | bytes 7077896 | tf_op jit(solution)/shard_map/ppermute | solution.py:914
  66.1 7.0 %collective-permute-start.2 = (bf16[2048,512]{1,0:T(8,128)(2,1)S(1)}, bf16[2048,512]{1,0:T(8,128)(2,1)S(1)}, u32[]{:S(2)}, u32[]{:S(2)}) collective-permute-start(bf16[2048,512]{1,0:T(8,128)(2,1)S(1)} %bitcast.17), channel_id=1, source_target_pairs={{0,1},{1,0},{2,3},{3,2},{4,5},{5,4},{6,7},{7,6},{8,9},{9,8},{10,11... | collective-permute-start | bytes 6291464 | tf_op jit(solution)/shard_map/ppermute | solution.py:914
  67.3 8.8 %collective-permute-start.3 = (bf16[2048,512]{1,0:T(8,128)(2,1)S(1)}, bf16[2048,512]{1,0:T(8,128)(2,1)S(1)}, u32[]{:S(2)}, u32[]{:S(2)}) collective-permute-start(bf16[2048,512]{1,0:T(8,128)(2,1)S(1)} %bitcast.20), channel_id=1, source_target_pairs={{0,1},{1,0},{2,3},{3,2},{4,5},{5,4},{6,7},{7,6},{8,9},{9,8},{10,11... | collective-permute-start | bytes 6291464 | tf_op jit(solution)/shard_map/ppermute | solution.py:914
  73.1 3.0 %copy-start.14 = (bf16[2048,512]{1,0:T(8,128)(2,1)}, bf16[2048,512]{1,0:T(8,128)(2,1)S(1)}, u32[]{:S(2)}) copy-start(bf16[2048,512]{1,0:T(8,128)(2,1)S(1)} %collective-permute-done.2.gate_all) | copy-start | bytes 6291460
  76.1 1.3 copy-start.15
  84.2 42.7 %all-to-all-start.1 = ((bf16[64,16,1152]{2,1,0:T(8,128)(2,1)}), bf16[64,16,1152]{2,1,0:T(8,128)(2,1)S(1)}, u32[]{:S(2)}, u32[]{:S(2)}) async-start(bf16[64,16,1152]{2,1,0:T(8,128)(2,1)} %back_sum.1), calls=%async_computation.1 | async-start | bytes 4718592 | tf_op jit(solution)/shard_map/all_to_all | solution.py:910
  91.9 29.1 %collective-permute-start.4 = (bf16[4,512]{1,0:T(4,128)(2,1)S(1)}, bf16[4,512]{1,0:T(4,128)(2,1)S(1)}, u32[]{:S(2)}, u32[]{:S(2)}) collective-permute-start(bf16[4,512]{1,0:T(4,128)(2,1)S(1)} %pad_maximum_fusion), channel_id=1, source_target_pairs={{0,2},{2,4},{4,6},{6,8},{8,10},{10,12},{12,14},{14,16},{16,18},{18... | collective-permute-start | bytes 12296 | tf_op jit(solution)/shard_map/ppermute | solution.py:920
  121.0 0.6 copy-start.13
  130.4 2.4 %copy-start.1 = (f32[4,384,128]{2,1,0:T(8,128)S(1)}, f32[4,384,128]{2,1,0:T(8,128)}, u32[]{:S(2)}) copy-start(f32[4,384,128]{2,1,0:T(8,128)} %get-tuple-element.67.product_ref.rest_1_) | copy-start | bytes 2359300
  130.4 2.4 %copy-start.2 = (f32[384,512]{1,0:T(8,128)S(1)}, f32[384,512]{1,0:T(8,128)}, u32[]{:S(2)}) copy-start(f32[384,512]{1,0:T(8,128)} %get-tuple-element.65.gelu_ref) | copy-start | bytes 2359300
  130.4 2.4 %copy-start.3 = (f32[4,384,128]{2,1,0:T(8,128)S(1)}, f32[4,384,128]{2,1,0:T(8,128)}, u32[]{:S(2)}) copy-start(f32[4,384,128]{2,1,0:T(8,128)} %get-tuple-element.66.ahead_ref) | copy-start | bytes 2359300
  130.4 2.4 %copy-start.9 = (f32[16,512]{1,0:T(8,128)S(1)}, f32[16,512]{1,0:T(8,128)}, u32[]{:S(2)}) copy-start(f32[16,512]{1,0:T(8,128)} %get-tuple-element.68.first_ref) | copy-start | bytes 98308
  130.4 2.4 %collective-permute-start.5 = (bf16[384,1024]{1,0:T(8,128)(2,1)S(1)}, bf16[384,1024]{1,0:T(8,128)(2,1)S(1)}, u32[]{:S(2)}, u32[]{:S(2)}) collective-permute-start(bf16[384,1024]{1,0:T(8,128)(2,1)S(1)} %get-tuple-element.60.own_ref), channel_id=1, source_target_pairs={{0,1},{1,0},{2,3},{3,2},{4,5},{5,4},{6,7},{7,6},{8,9},{9,8},{10,11... | collective-permute-start | bytes 2359304 | tf_op jit(solution)/shard_map/ppermute | solution.py:914
  132.3 3.6 %copy-start.5 = (f32[384,512]{1,0:T(8,128)}, f32[384,512]{1,0:T(8,128)S(1)}, u32[]{:S(2)}) copy-start(f32[384,512]{1,0:T(8,128)S(1)} %get-tuple-element.64.part_ref) | copy-start | bytes 2359300
  132.8 3.1 %copy-start.4 = (bf16[384,1024]{1,0:T(8,128)(2,1)}, bf16[384,1024]{1,0:T(8,128)(2,1)S(1)}, u32[]{:S(2)}) copy-start(bf16[384,1024]{1,0:T(8,128)(2,1)S(1)} %collective-permute-done.5.peer_ref) | copy-start | bytes 2359300
  136.0 36.8 %all-to-all-start.2 = ((bf16[64,8,2176]{2,1,0:T(8,128)(2,1)}), bf16[64,8,2176]{2,1,0:T(8,128)(2,1)S(1)}, u32[]{:S(2)}, u32[]{:S(2)}) async-start(bf16[64,8,2176]{2,1,0:T(8,128)(2,1)} %get-tuple-element.70), calls=%async_computation.2 | async-start | bytes 4456448 | tf_op jit(solution)/shard_map/all_to_all | solution.py:910
  149.2 9.1 %copy-start.16 = (f32[16,512]{1,0:T(8,128)S(1)}, f32[16,512]{1,0:T(8,128)}, u32[]{:S(2)}) copy-start(f32[16,512]{1,0:T(8,128)} %get-tuple-element.71) | copy-start | bytes 98308
  158.3 11.4 %collective-permute-start.6 = (f32[16,512]{1,0:T(8,128)S(1)}, f32[16,512]{1,0:T(8,128)S(1)}, u32[]{:S(2)}, u32[]{:S(2)}) collective-permute-start(f32[16,512]{1,0:T(8,128)S(1)} %copy-done.16), channel_id=1, source_target_pairs={{2,0},{4,2},{6,4},{8,6},{10,8},{12,10},{14,12},{16,14},{18,16},{20... | collective-permute-start | bytes 98312 | tf_op jit(solution)/shard_map/ppermute | solution.py:920

commit v7 on v6

--- a/solution.py
+++ b/solution.py
@@ -129,7 +129,7 @@
 pair = 2
 send_groups = 4
 all_groups = 8
-sum_groups = 4
+sum_parts = 4
 
 
 def expert_pre_kernel(rows_ref, gate_ref, up_ref, packed_ref, silu_ref, slope_ref, active_ref):
@@ -468,22 +468,37 @@
     )(core, adj, near_by(gate_half), near_by(up_half), held(gate_peer), held(up_peer))
 
 
-def back_sum_kernel(adj_ref, own_ref, gate_ref, up_ref, out_ref, scratch):
-    peer = back_rows(adj_ref[...], gate_ref[...], up_ref[...])
-    pack_into(out_ref, own_ref[...].astype(f32) + peer.astype(f32), scratch)
+def back_sum_kernel(adj_ref, own_ref, gate_ref, up_ref, out_ref, packed, scratch, sems):
+    parts = sems.shape[0]
+    size = adj_ref.shape[0] // parts
+    blocks = packed.shape[0] // parts
+    copies = []
+    for k in range(parts):
+        rows = slice(k * size, (k + 1) * size)
+        peer = back_rows(adj_ref[rows, :], gate_ref[...], up_ref[...])
+        part = packed.at[k * blocks : (k + 1) * blocks]
+        pack_into(part, own_ref[rows, :].astype(f32) + peer.astype(f32), scratch)
+        copies.append(
+            pltpu.make_async_copy(part, out_ref.at[k * blocks : (k + 1) * blocks], sems.at[k])
+        )
+        copies[-1].start()
+    for copy in copies:
+        copy.wait()
 
 
 def back_sum(adj, own, gate_half, up_half, shape):
     count = adj.shape[0]
     half, hidden = gate_half.shape
-    size = sum_groups * group_rows
-    by_row = lambda width: pl.BlockSpec((size, width), lambda i: (i, 0))
     return pl.pallas_call(
         back_sum_kernel,
-        grid=(count // size,),
-        in_specs=[by_row(2 * hidden), by_row(half), whole((half, hidden)), whole((half, hidden))],
-        out_specs=pl.BlockSpec((sum_groups * group, main, shape[2]), lambda i: (i, 0, 0)),
-        scratch_shapes=[pltpu.VMEM((128, 128), f32)],
+        grid=(1,),
+        in_specs=[resident] * 4,
+        out_specs=anywhere,
+        scratch_shapes=[
+            pltpu.VMEM(shape, bf16),
+            pltpu.VMEM((128, 128), f32),
+            pltpu.SemaphoreType.DMA((sum_parts,)),
+        ],
         out_shape=pltpu.HBM(shape, bf16),
         compiler_params=params(),
         cost_estimate=pl.CostEstimate(

time: 181 us -> 180 us (level)
  no operation moved by 1% of the time
where the time goes in v7:
time: 180 us; the launch traced here: 178 us
  Pallas kernels  67.7 us (38%)
  blocking collectives  43.1 us (24%)
  waiting for transfers between devices  37.2 us (21%)
  starting transfers between devices  22.6 us (13%)
  local copies, waits for them, and re-layouts  5.93 us (3%)
    all_to_all x1, blocking collectives, exchange(): return lax.all_to_all(value, axis, split_axis=0, concat_axis=0, tiled=True)  43.1 us
    ppermute x2, waiting for transfers between devices, shifted(): return lax.ppermute(value, axis, pairs)  24.9 us
    all_to_all x2, starting transfers between devices, exchange(): return lax.all_to_all(value, axis, split_axis=0, concat_axis=0, tiled=True)  12.4 us
    pallas_call x1, Pallas kernels, expert_pre(): pl.pallas_call(expert_pre_kernel, grid=(count // size,), in_specs=[by_row...  11.9 us
    ppermute x2, starting transfers between devices, shifted(): return lax.ppermute(value, axis, pairs)  10.1 us
    ppermute x5, waiting for transfers between devices, swapped(): return lax.ppermute(value, 'tp', [(0, 1), (1, 0)])  9.25 us
    pallas_call x1, Pallas kernels, grad_in(): pl.pallas_call(grad_in_kernel, grid=(model // size,), in_specs=[pl.BlockS...  9.1 us
    pallas_call x1, Pallas kernels, grad_down_of(): pl.pallas_call(grad_down_kernel, grid_spec=pltpu.PrefetchScalarGridSpec(n...  7.19 us
  transfers between devices with their start and end apart: 9, of which 5 were waited for; matrix products, arithmetic and copies ran while one was open for 1% of the time, Pallas kernels for 26%

profile of v7, /device:TPU:32, one launch (start us, length us, event | category | flops | bytes accessed | tf_op | source)
XLA Modules:
  0.0 177.7 jit_solution(14092136292161338577)
XLA Ops:
  0.6 4.3 %send.1 = (bf16[64,16,1152]{2,1,0:T(8,128)(2,1)}, s32[8,384]{1,0:T(8,128)S(1)}) custom-call(s32[1]{0:T(128)} %bitcast.3.core_ref, s32[2,384]{1,0:T(2,128)} %bitcast.22, f32[2,384]{1,0:T(2,128)} %bitcast.23, bf16[384,2048]{1,0:T(8,128)(2,1)} %cot_ref.3), custom_call_target="tpu_custom_call" | custom-call | tf_op jit(solution)/shard_map/send/pallas_call | solution.py:104
  5.0 43.1 %all_to_all.15.block_ref.near_ref = bf16[64,16,1152]{2,1,0:T(8,128)(2,1)S(1)} all-to-all(bf16[64,16,1152]{2,1,0:T(8,128)(2,1)} %get-tuple-element.44), channel_id=1, replica_groups=mesh['sp'=64,'tp'=2] {'sp'}, dimensions={0} | all-to-all | bytes 4718592 | tf_op jit(solution)/shard_map/all_to_all | solution.py:925
  48.1 0.0 collective-permute-start
  48.1 11.9 %expert_pre.1 = (bf16[1152,2048]{1,0:T(8,128)(2,1)}, f32[1152,512]{1,0:T(8,128)}, f32[1152,512]{1,0:T(8,128)}, bf16[1152,512]{1,0:T(8,128)(2,1)}) custom-call(bf16[1152,2048]{1,0:T(8,128)(2,1)} %bitcast.25, bf16[2048,512]{1,0:T(8,128)(2,1)} %bitcast.15, bf16[2048,512]{1,0:T(8,128)(2,1)} %bitcast.18), custom_call_target="tpu_custom_call" | custom-call | flops 4831838208 | bytes 20971520 | tf_op jit(solution)/shard_map/expert_pre/pallas_call | solution.py:165
  60.0 3.0 %near.1 = (f32[1152,512]{1,0:T(8,128)S(1)}, bf16[512,1024]{1,0:T(8,128)(2,1)S(1)}) custom-call(s32[1]{0:T(128)} %bitcast.3.core_ref, bf16[64,16,1152]{2,1,0:T(8,128)(2,1)S(1)} %all_to_all.15.block_ref.near_ref, bf16[512,2048]{1,0:T(8,128)(2,1)} %bitcast.13, bf16[512,2048]{1,0:T(8,128)(2,1)} %bitcast.14), custom_call_target="tpu_custom_call" | custom-call | flops 1207959552 | bytes 9437184 | tf_op jit(solution)/shard_map/near/pallas_call | solution.py:336
  63.0 0.0 collective-permute-done.block_ref.far_ref
  63.0 0.0 copy-start.6
  63.0 0.0 copy-done.7
  63.0 0.0 copy-done.8
  63.0 0.0 copy-start.11
  63.0 0.0 copy-start.12
  63.0 2.4 %far.1 = (bf16[1152,1024]{1,0:T(8,128)(2,1)S(1)}, bf16[1024,512]{1,0:T(8,128)(2,1)S(1)}, bf16[1024,512]{1,0:T(8,128)(2,1)S(1)}) custom-call(s32[1]{0:T(128)} %bitcast.3.core_ref, bf16[64,16,1152]{2,1,0:T(8,128)(2,1)S(1)} %collective-permute-done.block_ref.far_ref, bf16[512,1024]{1,0:T(8,128)(2,1)S(1)} %get-tuple-element.45.down_ref, ...), custom_call_target="tpu_custom_call" | custom-call | flops 1207959552 | bytes 16777216 | tf_op jit(solution)/shard_map/far/pallas_call | solution.py:387
  65.5 0.1 collective-permute-start.1
  65.6 0.5 copy-done.11
  66.1 0.0 collective-permute-start.2
  66.1 1.2 copy-done.12
  67.3 0.0 collective-permute-start.3
  67.3 5.8 %collective-permute-done.2.gate_all = bf16[2048,512]{1,0:T(8,128)(2,1)S(1)} collective-permute-done((bf16[2048,512]{1,0:T(8,128)(2,1)S(1)}, bf16[2048,512]{1,0:T(8,128)(2,1)S(1)}, u32[]{:S(2)}, u32[]{:S(2)}) %collective-permute-start.2) | collective-permute-done | bytes 2097184 | tf_op jit(solution)/shard_map/ppermute | solution.py:929
  73.1 3.0 %collective-permute-done.3.up_all = bf16[2048,512]{1,0:T(8,128)(2,1)S(1)} collective-permute-done((bf16[2048,512]{1,0:T(8,128)(2,1)S(1)}, bf16[2048,512]{1,0:T(8,128)(2,1)S(1)}, u32[]{:S(2)}, u32[]{:S(2)}) %collective-permute-start.3) | collective-permute-done | bytes 2097184 | tf_op jit(solution)/shard_map/ppermute | solution.py:929
  76.1 0.0 copy-done.14
  76.1 1.3 copy-done.15
  77.4 2.7 %back_own.1 = (bf16[1152,1024]{1,0:T(8,128)(2,1)S(1)}, bf16[1024,512]{1,0:T(8,128)(2,1)S(1)}, bf16[1024,512]{1,0:T(8,128)(2,1)S(1)}) custom-call(s32[1]{0:T(128)} %bitcast.3.core_ref, bf16[1152,1024]{1,0:T(8,128)(2,1)S(1)} %get-tuple-element.49.adj_ref, bf16[1024,512]{1,0:T(8,128)(2,1)S(1)} %get-tuple-element.53.gate_ref, ...), custom_call_target="tpu_custom_call" | custom-call | flops 2415919104 | bytes 7340032 | tf_op jit(solution)/shard_map/back_own/pallas_call | solution.py:443
  80.1 0.0 collective-permute-done.1.adj_ref
  80.1 3.6 %back_sum.1 = bf16[64,16,1152]{2,1,0:T(8,128)(2,1)} custom-call(bf16[1152,1024]{1,0:T(8,128)(2,1)S(1)} %collective-permute-done.1.adj_ref, bf16[1152,1024]{1,0:T(8,128)(2,1)S(1)} %get-tuple-element.55.own_ref, bf16[1024,512]{1,0:T(8,128)(2,1)S(1)} %get-tuple-element.56.gate_ref, bf16[1024,512]{1,0:T(8,128)(2,1)S(1)} %get-tuple-element.57.up_ref), custom_call_target="tpu_custom_call" | custom-call | flops 2415919104 | bytes 7340032 | tf_op jit(solution)/shard_map/back_sum/pallas_call | solution.py:492
  83.8 6.4 %all-to-all-start.1 = ((bf16[64,16,1152]{2,1,0:T(8,128)(2,1)}), bf16[64,16,1152]{2,1,0:T(8,128)(2,1)S(1)}, u32[]{:S(2)}, u32[]{:S(2)}) async-start(bf16[64,16,1152]{2,1,0:T(8,128)(2,1)} %back_sum.1), calls=%async_computation.1 | async-start | bytes 4718592 | tf_op jit(solution)/shard_map/all_to_all | solution.py:925
  90.1 0.7 slice.7
  90.8 0.7 slice.6
  91.6 3.4 %collective-permute-start.4 = (bf16[4,512]{1,0:T(4,128)(2,1)S(1)}, bf16[4,512]{1,0:T(4,128)(2,1)S(1)}, u32[]{:S(2)}, u32[]{:S(2)}) collective-permute-start(bf16[4,512]{1,0:T(4,128)(2,1)S(1)} %pad_maximum_fusion), channel_id=1, source_target_pairs={{0,2},{2,4},{4,6},{6,8},{8,10},{10,12},{12,14},{14,16},{16,18},{18... | collective-permute-start | bytes 12296 | tf_op jit(solution)/shard_map/ppermute | solution.py:935
  94.9 0.8 copy.22
  95.7 24.9 %collective-permute-done.4.edge_ref = bf16[4,512]{1,0:T(4,128)(2,1)S(1)} collective-permute-done((bf16[4,512]{1,0:T(4,128)(2,1)S(1)}, bf16[4,512]{1,0:T(4,128)(2,1)S(1)}, u32[]{:S(2)}, u32[]{:S(2)}) %collective-permute-start.4) | collective-permute-done | bytes 4128 | tf_op jit(solution)/shard_map/ppermute | solution.py:935
  120.6 0.6 copy-done.13
  121.2 5.2 %recur_pre.1 = (bf16[384,512]{1,0:T(8,128)(2,1)}, f32[384,512]{1,0:T(8,128)}, f32[384,512]{1,0:T(8,128)}, f32[4,384,128]{2,1,0:T(8,128)}, f32[4,384,128]{2,1,0:T...) custom-call(bf16[384,512]{1,0:T(8,128)(2,1)} %x_ref.1, ...), custom_call_target="tpu_custom_call" | custom-call | flops 393216000 | bytes 8388608 | tf_op jit(solution)/shard_map/recur_pre/pallas_call | solution.py:252
  126.5 0.0 all-to-all-done.1.block_ref
  126.5 3.6 %combine.1 = (bf16[384,1024]{1,0:T(8,128)(2,1)S(1)}, bf16[1024,512]{1,0:T(8,128)(2,1)S(1)}, bf16[384,512]{1,0:T(8,128)(2,1)S(1)}) custom-call(s32[1]{0:T(128)} %bitcast.3.core_ref, bf16[64,16,1152]{2,1,0:T(8,128)(2,1)S(1)} %all-to-all-done.1.block_ref, s32[384,8]{1,0:T(8,128)} %bitcast.21, bf16[384,2048]{1,0:T(8,128)(2,1)} %cot_ref.3, ...), custom_call_target="tpu_custom_call" | custom-call | tf_op jit(solution)/shard_map/combine/pallas_call | solution.py:595
  130.0 0.0 copy-start.1
  130.1 0.0 copy-start.9
  130.1 0.1 collective-permute-start.5
  130.2 1.8 %own_part.1 = (f32[384,512]{1,0:T(8,128)S(1)}, bf16[64,8,2176]{2,1,0:T(8,128)(2,1)}, bf16[1024,512]{1,0:T(8,128)(2,1)S(1)}) custom-call(s32[1]{0:T(128)} %bitcast.3.core_ref, bf16[384,1024]{1,0:T(8,128)(2,1)S(1)} %get-tuple-element.60.own_ref, bf16[1024,512]{1,0:T(8,128)(2,1)S(1)} %get-tuple-element.61.weight_ref, ...), custom_call_target="tpu_custom_call" | custom-call | flops 805306368 | bytes 4194304 | tf_op jit(solution)/shard_map/own_part/pallas_call | solution.py:649
  132.0 0.5 collective-permute-done.5.peer_ref
  132.5 3.1 %scan.1 = (bf16[64,8,2176]{2,1,0:T(8,128)(2,1)}, f32[16,512]{1,0:T(8,128)}) custom-call(s32[1]{0:T(128)} %bitcast.3.core_ref, bf16[384,1024]{1,0:T(8,128)(2,1)S(1)} %collective-permute-done.5.peer_ref, bf16[1024,512]{1,0:T(8,128)(2,1)S(1)} %get-tuple-element.63.weight_ref, ...), custom_call_target="tpu_custom_call", output_to_operand_aliasing={{0}: (9, {})} | custom-call | flops 805306368 | bytes 9437184 | tf_op jit(solution)/shard_map/scan/pallas_call | solution.py:737
  135.6 6.0 %all-to-all-start.2 = ((bf16[64,8,2176]{2,1,0:T(8,128)(2,1)}), bf16[64,8,2176]{2,1,0:T(8,128)(2,1)S(1)}, u32[]{:S(2)}, u32[]{:S(2)}) async-start(bf16[64,8,2176]{2,1,0:T(8,128)(2,1)} %get-tuple-element.70), calls=%async_computation.2 | async-start | bytes 4456448 | tf_op jit(solution)/shard_map/all_to_all | solution.py:925
  141.6 7.2 %grad_down.1 = bf16[512,2048]{1,0:T(8,128)(2,1)} custom-call(s32[1]{0:T(128)} %bitcast.3.core_ref, bf16[1152,512]{1,0:T(8,128)(2,1)} %get-tuple-element.52.active_ref, bf16[64,16,1152]{2,1,0:T(8,128)(2,1)} %copy-done, bf16[64,16,1152]{2,1,0:T(8,128)(2,1)} %copy-done.6), custom_call_target="tpu_custom_call" | custom-call | flops 2415919104 | bytes 9437184 | tf_op jit(solution)/shard_map/grad_down/pallas_call | solution.py:552
  148.8 9.1 %grad_in.1 = (bf16[2048,512]{1,0:T(8,128)(2,1)}, bf16[2048,512]{1,0:T(8,128)(2,1)}) custom-call(bf16[1152,2048]{1,0:T(8,128)(2,1)} %get-tuple-element.43.packed_ref, bf16[1152,1024]{1,0:T(8,128)(2,1)} %copy-done.10), custom_call_target="tpu_custom_call" | custom-call | flops 4831838208 | bytes 11534336 | tf_op jit(solution)/shard_map/grad_in/pallas_call | solution.py:523
  157.9 6.7 %collective-permute-start.6 = (f32[16,512]{1,0:T(8,128)S(1)}, f32[16,512]{1,0:T(8,128)S(1)}, u32[]{:S(2)}, u32[]{:S(2)}) collective-permute-start(f32[16,512]{1,0:T(8,128)S(1)} %copy-done.16), channel_id=1, source_target_pairs={{2,0},{4,2},{6,4},{8,6},{10,8},{12,10},{14,12},{16,14},{18,16},{20... | collective-permute-start | bytes 98312 | tf_op jit(solution)/shard_map/ppermute | solution.py:935
  164.6 4.7 %local_scan.1 = (f32[384,512]{1,0:T(8,128)}, f32[4,384,128]{2,1,0:T(8,128)}) custom-call(s32[1]{0:T(128)} %bitcast.3.core_ref, bf16[384,1024]{1,0:T(8,128)(2,1)} %copy-done.4, bf16[2048,512]{1,0:T(8,128)(2,1)} %weight_ref.1, f32[384,512]{1,0:T(8,128)} %copy-done.5, f32[384,512]{1,0:T(8,128)} %get-tuple-element.72.slope_ref, ...), custom_call_target="tpu_custom_call" | custom-call | flops 402653184 | bytes 9437184 | tf_op jit(solution)/shard_map/local_scan/pallas_call | solution.py:786
  169.3 0.0 collective-permute-done.6.head_ref
  169.3 3.0 %all-to-all-done.2.share_ref = bf16[64,8,2176]{2,1,0:T(8,128)(2,1)S(1)} async-done(((bf16[64,8,2176]{2,1,0:T(8,128)(2,1)}), bf16[64,8,2176]{2,1,0:T(8,128)(2,1)S(1)}, u32[]{:S(2)}, u32[]{:S(2)}) %all-to-all-start.2) | async-done | bytes 2228256 | tf_op jit(solution)/shard_map/all_to_all | solution.py:925
  172.3 5.2 %tail.1 = (f32[384,512]{1,0:T(8,128)}, f32[32,512]{1,0:T(8,128)}) custom-call(s32[1]{0:T(128)} %bitcast.10.place_ref, bf16[64,8,2176]{2,1,0:T(8,128)(2,1)S(1)} %all-to-all-done.2.share_ref, f32[16,512]{1,0:T(8,128)S(1)} %collective-permute-done.6.head_ref, f32[4,512]{1,0:T(4,128)} %taps_ref.3, bf16[4,128,128]{2,1,0:T(8,128)(2,1)} %a_ref.3, ...), custom_call_target="tpu_custom_call" | custom-call | tf_op jit(solution)/shard_map/tail/pallas_call | solution.py:892
  (23 shorter events, 0.1 us)
Async XLA Ops:
  48.1 11.9 %copy-start = (bf16[64,16,1152]{2,1,0:T(8,128)(2,1)}, bf16[64,16,1152]{2,1,0:T(8,128)(2,1)S(1)}, u32[]{:S(2)}) copy-start(bf16[64,16,1152]{2,1,0:T(8,128)(2,1)S(1)} %all_to_all.15.block_ref.near_ref) | copy-start | bytes 7077892
  48.1 14.9 %collective-permute-start = (bf16[64,16,1152]{2,1,0:T(8,128)(2,1)S(1)}, bf16[64,16,1152]{2,1,0:T(8,128)(2,1)S(1)}, u32[]{:S(2)}, u32[]{:S(2)}) collective-permute-start(bf16[64,16,1152]{2,1,0:T(8,128)(2,1)S(1)} %all_to_all.15.block_ref.near_ref), channel_id=1, source_target_pairs={{0,1},{1,0},{2,3},{3,2},{4,5},{5,4},{6,7},{7,6},{8,9},{9,8},{10,11... | collective-permute-start | bytes 7077896 | tf_op jit(solution)/shard_map/ppermute | solution.py:929
  60.0 3.0 %copy-start.7 = (f32[1152,512]{1,0:T(8,128)S(1)}, f32[1152,512]{1,0:T(8,128)}, u32[]{:S(2)}) copy-start(f32[1152,512]{1,0:T(8,128)} %get-tuple-element.47.silu_ref) | copy-start | bytes 7077892
  60.0 3.0 %copy-start.8 = (f32[1152,512]{1,0:T(8,128)S(1)}, f32[1152,512]{1,0:T(8,128)}, u32[]{:S(2)}) copy-start(f32[1152,512]{1,0:T(8,128)} %get-tuple-element.48.slope_ref) | copy-start | bytes 7077892
  63.0 2.5 %copy-start.6 = (bf16[64,16,1152]{2,1,0:T(8,128)(2,1)}, bf16[64,16,1152]{2,1,0:T(8,128)(2,1)S(1)}, u32[]{:S(2)}) copy-start(bf16[64,16,1152]{2,1,0:T(8,128)(2,1)S(1)} %collective-permute-done.block_ref.far_ref) | copy-start | bytes 7077892
  63.0 3.1 %copy-start.11 = (bf16[1,2048,512]{2,1,0:T(8,128)(2,1)S(1)}, bf16[1,2048,512]{2,1,0:T(8,128)(2,1)}, u32[]{:S(2)}) copy-start(bf16[1,2048,512]{2,1,0:T(8,128)(2,1)} %param.19) | copy-start | bytes 6291460
  63.0 4.3 %copy-start.12 = (bf16[1,2048,512]{2,1,0:T(8,128)(2,1)S(1)}, bf16[1,2048,512]{2,1,0:T(8,128)(2,1)}, u32[]{:S(2)}) copy-start(bf16[1,2048,512]{2,1,0:T(8,128)(2,1)} %param.20) | copy-start | bytes 6291460
  65.5 14.6 %copy-start.10 = (bf16[1152,1024]{1,0:T(8,128)(2,1)}, bf16[1152,1024]{1,0:T(8,128)(2,1)S(1)}, u32[]{:S(2)}) copy-start(bf16[1152,1024]{1,0:T(8,128)(2,1)S(1)} %get-tuple-element.49.adj_ref) | copy-start | bytes 7077892
  65.5 14.6 %collective-permute-start.1 = (bf16[1152,1024]{1,0:T(8,128)(2,1)S(1)}, bf16[1152,1024]{1,0:T(8,128)(2,1)S(1)}, u32[]{:S(2)}, u32[]{:S(2)}) collective-permute-start(bf16[1152,1024]{1,0:T(8,128)(2,1)S(1)} %get-tuple-element.49.adj_ref), channel_id=1, source_target_pairs={{0,1},{1,0},{2,3},{3,2},{4,5},{5,4},{6,7},{7,6},{8,9},{9,8},{10,11... | collective-permute-start | bytes 7077896 | tf_op jit(solution)/shard_map/ppermute | solution.py:929
  66.1 7.0 %collective-permute-start.2 = (bf16[2048,512]{1,0:T(8,128)(2,1)S(1)}, bf16[2048,512]{1,0:T(8,128)(2,1)S(1)}, u32[]{:S(2)}, u32[]{:S(2)}) collective-permute-start(bf16[2048,512]{1,0:T(8,128)(2,1)S(1)} %bitcast.17), channel_id=1, source_target_pairs={{0,1},{1,0},{2,3},{3,2},{4,5},{5,4},{6,7},{7,6},{8,9},{9,8},{10,11... | collective-permute-start | bytes 6291464 | tf_op jit(solution)/shard_map/ppermute | solution.py:929
  67.3 8.8 %collective-permute-start.3 = (bf16[2048,512]{1,0:T(8,128)(2,1)S(1)}, bf16[2048,512]{1,0:T(8,128)(2,1)S(1)}, u32[]{:S(2)}, u32[]{:S(2)}) collective-permute-start(bf16[2048,512]{1,0:T(8,128)(2,1)S(1)} %bitcast.20), channel_id=1, source_target_pairs={{0,1},{1,0},{2,3},{3,2},{4,5},{5,4},{6,7},{7,6},{8,9},{9,8},{10,11... | collective-permute-start | bytes 6291464 | tf_op jit(solution)/shard_map/ppermute | solution.py:929
  73.1 3.0 %copy-start.14 = (bf16[2048,512]{1,0:T(8,128)(2,1)}, bf16[2048,512]{1,0:T(8,128)(2,1)S(1)}, u32[]{:S(2)}) copy-start(bf16[2048,512]{1,0:T(8,128)(2,1)S(1)} %collective-permute-done.2.gate_all) | copy-start | bytes 6291460
  76.1 1.3 copy-start.15
  83.8 42.7 %all-to-all-start.1 = ((bf16[64,16,1152]{2,1,0:T(8,128)(2,1)}), bf16[64,16,1152]{2,1,0:T(8,128)(2,1)S(1)}, u32[]{:S(2)}, u32[]{:S(2)}) async-start(bf16[64,16,1152]{2,1,0:T(8,128)(2,1)} %back_sum.1), calls=%async_computation.1 | async-start | bytes 4718592 | tf_op jit(solution)/shard_map/all_to_all | solution.py:925
  91.6 29.1 %collective-permute-start.4 = (bf16[4,512]{1,0:T(4,128)(2,1)S(1)}, bf16[4,512]{1,0:T(4,128)(2,1)S(1)}, u32[]{:S(2)}, u32[]{:S(2)}) collective-permute-start(bf16[4,512]{1,0:T(4,128)(2,1)S(1)} %pad_maximum_fusion), channel_id=1, source_target_pairs={{0,2},{2,4},{4,6},{6,8},{8,10},{10,12},{12,14},{14,16},{16,18},{18... | collective-permute-start | bytes 12296 | tf_op jit(solution)/shard_map/ppermute | solution.py:935
  120.6 0.6 copy-start.13
  130.0 2.4 %copy-start.1 = (f32[4,384,128]{2,1,0:T(8,128)S(1)}, f32[4,384,128]{2,1,0:T(8,128)}, u32[]{:S(2)}) copy-start(f32[4,384,128]{2,1,0:T(8,128)} %get-tuple-element.67.product_ref.rest_1_) | copy-start | bytes 2359300
  130.0 2.4 %copy-start.2 = (f32[384,512]{1,0:T(8,128)S(1)}, f32[384,512]{1,0:T(8,128)}, u32[]{:S(2)}) copy-start(f32[384,512]{1,0:T(8,128)} %get-tuple-element.65.gelu_ref) | copy-start | bytes 2359300
  130.0 2.4 %copy-start.3 = (f32[4,384,128]{2,1,0:T(8,128)S(1)}, f32[4,384,128]{2,1,0:T(8,128)}, u32[]{:S(2)}) copy-start(f32[4,384,128]{2,1,0:T(8,128)} %get-tuple-element.66.ahead_ref) | copy-start | bytes 2359300
  130.1 2.4 %copy-start.9 = (f32[16,512]{1,0:T(8,128)S(1)}, f32[16,512]{1,0:T(8,128)}, u32[]{:S(2)}) copy-start(f32[16,512]{1,0:T(8,128)} %get-tuple-element.68.first_ref) | copy-start | bytes 98308
  130.1 2.4 %collective-permute-start.5 = (bf16[384,1024]{1,0:T(8,128)(2,1)S(1)}, bf16[384,1024]{1,0:T(8,128)(2,1)S(1)}, u32[]{:S(2)}, u32[]{:S(2)}) collective-permute-start(bf16[384,1024]{1,0:T(8,128)(2,1)S(1)} %get-tuple-element.60.own_ref), channel_id=1, source_target_pairs={{0,1},{1,0},{2,3},{3,2},{4,5},{5,4},{6,7},{7,6},{8,9},{9,8},{10,11... | collective-permute-start | bytes 2359304 | tf_op jit(solution)/shard_map/ppermute | solution.py:929
  131.9 3.6 %copy-start.5 = (f32[384,512]{1,0:T(8,128)}, f32[384,512]{1,0:T(8,128)S(1)}, u32[]{:S(2)}) copy-start(f32[384,512]{1,0:T(8,128)S(1)} %get-tuple-element.64.part_ref) | copy-start | bytes 2359300
  132.4 3.1 %copy-start.4 = (bf16[384,1024]{1,0:T(8,128)(2,1)}, bf16[384,1024]{1,0:T(8,128)(2,1)S(1)}, u32[]{:S(2)}) copy-start(bf16[384,1024]{1,0:T(8,128)(2,1)S(1)} %collective-permute-done.5.peer_ref) | copy-start | bytes 2359300
  135.6 36.8 %all-to-all-start.2 = ((bf16[64,8,2176]{2,1,0:T(8,128)(2,1)}), bf16[64,8,2176]{2,1,0:T(8,128)(2,1)S(1)}, u32[]{:S(2)}, u32[]{:S(2)}) async-start(bf16[64,8,2176]{2,1,0:T(8,128)(2,1)} %get-tuple-element.70), calls=%async_computation.2 | async-start | bytes 4456448 | tf_op jit(solution)/shard_map/all_to_all | solution.py:925
  148.8 9.1 %copy-start.16 = (f32[16,512]{1,0:T(8,128)S(1)}, f32[16,512]{1,0:T(8,128)}, u32[]{:S(2)}) copy-start(f32[16,512]{1,0:T(8,128)} %get-tuple-element.71) | copy-start | bytes 98308
  157.9 11.4 %collective-permute-start.6 = (f32[16,512]{1,0:T(8,128)S(1)}, f32[16,512]{1,0:T(8,128)S(1)}, u32[]{:S(2)}, u32[]{:S(2)}) collective-permute-start(f32[16,512]{1,0:T(8,128)S(1)} %copy-done.16), channel_id=1, source_target_pairs={{2,0},{4,2},{6,4},{8,6},{10,8},{12,10},{14,12},{16,14},{18,16},{20... | collective-permute-start | bytes 98312 | tf_op jit(solution)/shard_map/ppermute | solution.py:935

commit v8 on v7

--- a/solution.py
+++ b/solution.py
@@ -379,7 +379,7 @@
 
 
 def far(core, arrived, down_half, part, silu, slope, gate, up):
-    experts, _, _ = arrived.shape
+    experts, _, wide = arrived.shape
     hidden, half = down_half.shape
     count = experts * (main + extra)
     size = all_groups * group_rows
@@ -390,11 +390,11 @@
             num_scalar_prefetch=1,
             grid=(count // size,),
             in_specs=[
-                resident,
-                resident,
-                resident,
-                resident,
-                resident,
+                pl.BlockSpec((all_groups * group, main, wide), lambda i, c: (i, 0, 0)),
+                whole((hidden, half)),
+                by_row(hidden),
+                by_row(hidden),
+                by_row(hidden),
                 anywhere,
                 anywhere,
             ],
@@ -446,9 +446,9 @@
             num_scalar_prefetch=1,
             grid=(count // size,),
             in_specs=[
-                resident,
-                resident,
-                resident,
+                by_row(2 * hidden),
+                whole((half, hidden)),
+                whole((half, hidden)),
                 anywhere,
                 anywhere,
             ],
@@ -567,54 +567,51 @@
     )(core, held(active), held(arrived), held(arrived_far))
 
 
-def combine_kernel(
-    core_ref, block_ref, target_ref, cot_ref, weight_all, mixed_all,
-    out_ref, weight_next, mixed_next, scratch, sems,
-):
-    half = weight_next.shape[0]
-    own = pl.multiple_of(core_ref[0] * half, half)
-    copies = load_beside(
-        [
-            pltpu.make_async_copy(weight_all.at[pl.ds(own, half)], weight_next, sems.at[0]),
-            pltpu.make_async_copy(mixed_all, mixed_next, sems.at[1]),
-        ]
-    )
+def combine_kernel(core_ref, block_ref, target_ref, cot_ref, out_ref, total, scratch):
+    step = pl.program_id(0)
     tokens = cot_ref.shape[0]
     rows = unpack(block_ref[...], scratch)
-    place = lax.broadcasted_iota(jnp.int32, (tokens, rows.shape[0]), 1)
+    size = rows.shape[0]
+    place = lax.broadcasted_iota(jnp.int32, (tokens, size), 1) + step * size
     chosen = jnp.where(
         (place == target_ref[:, 0:1]) | (place == target_ref[:, 1:2]), 1.0, 0.0
     ).astype(bf16)
-    out_ref[...] = (cot_ref[...].astype(f32) + dot(chosen, rows, plain)).astype(bf16)
-    finish(copies)
-
-
-def combine(core, returned, target, cotangent, weight, mixed):
-    half = returned.shape[2] - 128
+    found = dot(chosen, rows, plain)
+
+    @pl.when(step == 0)
+    def _():
+        total[...] = found
+
+    @pl.when(step > 0)
+    def _():
+        total[...] = total[...] + found
+
+    @pl.when(step == pl.num_programs(0) - 1)
+    def _():
+        out_ref[...] = (cot_ref[...].astype(f32) + total[...]).astype(bf16)
+
+
+def combine(core, returned, target, cotangent):
+    experts, _, wide = returned.shape
+    half = wide - 128
     tokens = cotangent.shape[0]
     return pl.pallas_call(
         combine_kernel,
         grid_spec=pltpu.PrefetchScalarGridSpec(
             num_scalar_prefetch=1,
-            grid=(1,),
+            grid=(experts // (all_groups * group),),
             in_specs=[
-                resident,
+                pl.BlockSpec((all_groups * group, main, wide), lambda i, c: (i, 0, 0)),
                 whole((tokens, 8)),
                 pl.BlockSpec((tokens, half), lambda i, c: (0, c[0])),
-                anywhere,
-                anywhere,
-            ],
-            out_specs=[whole((tokens, half)), anywhere, anywhere],
-            scratch_shapes=[pltpu.VMEM((128, 128), f32), pltpu.SemaphoreType.DMA((2,))],
-        ),
-        out_shape=[
-            jax.ShapeDtypeStruct((tokens, half), bf16),
-            pltpu.VMEM((half, weight.shape[1]), bf16),
-            pltpu.VMEM(mixed.shape, bf16),
-        ],
+            ],
+            out_specs=whole((tokens, half)),
+            scratch_shapes=[pltpu.VMEM((tokens, half), f32), pltpu.VMEM((128, 128), f32)],
+        ),
+        out_shape=jax.ShapeDtypeStruct((tokens, half), bf16),
         compiler_params=params(),
         name="combine",
-    )(core, returned, held(target), held(cotangent), held(weight), held(mixed))
+    )(core, returned, held(target), held(cotangent))
 
 
 def write_shares(ref, values):
@@ -624,14 +621,7 @@
         ref[:, :, channels * k : channels * (k + 1)] = pieces[:, k]
 
 
-def own_kernel(
-    core_ref, own_ref, weight_ref, mixed_ref, weight_all, grad_ref, share_out, weight_next, share, sems
-):
-    half = weight_next.shape[0]
-    other = pl.multiple_of((1 - core_ref[0]) * half, half)
-    copies = load_beside(
-        [pltpu.make_async_copy(weight_all.at[pl.ds(other, half)], weight_next, sems.at[1])]
-    )
+def own_kernel(core_ref, own_ref, weight_ref, mixed_ref, grad_ref, share_out, share, sems):
     owners = share.shape[0]
     at = pl.ds(pl.multiple_of(core_ref[0] * owners, owners), owners)
     own = own_ref[...]
@@ -640,10 +630,9 @@
     copy.start()
     grad_ref[...] = dot(own, weight_ref[...], plain)
     copy.wait()
-    finish(copies)
-
-
-def own_part(core, own, weight_half, mixed, weight, owners):
+
+
+def own_part(core, own, weight, mixed, owners):
     tokens, half = own.shape
     channels = mixed.shape[1]
     return pl.pallas_call(
@@ -652,43 +641,38 @@
             num_scalar_prefetch=1,
             grid=(1,),
             in_specs=[
-                resident,
-                resident,
-                resident,
-                anywhere,
-            ],
-            out_specs=[whole((tokens, channels)), anywhere, anywhere],
+                whole((tokens, half)),
+                pl.BlockSpec((half, channels), lambda i, c: (c[0], 0)),
+                whole((tokens, channels)),
+            ],
+            out_specs=[whole((tokens, channels)), anywhere],
             scratch_shapes=[
                 pltpu.VMEM((owners // 2, 8, 4 * channels), bf16),
-                pltpu.SemaphoreType.DMA((2,)),
+                pltpu.SemaphoreType.DMA((1,)),
             ],
         ),
         out_shape=[
             jax.ShapeDtypeStruct((tokens, channels), f32),
             pltpu.HBM((owners, 8, 4 * channels + 128), bf16),
-            pltpu.VMEM((half, channels), bf16),
         ],
         compiler_params=params(),
         cost_estimate=pl.CostEstimate(
             flops=4 * tokens * half * channels, transcendentals=0, bytes_accessed=4 << 20
         ),
         name="own_part",
-    )(core, own, near_by(weight_half), near_by(mixed), held(weight))
-
-
-def segment_scan(values, ahead_ref, state_grad, local):
-    blocks, tokens, span = state_grad.shape
-    length = tokens // segments
-    for b in range(blocks):
-        state_grad[b] = values[:, span * b : span * (b + 1)]
-    last = [None] * blocks
+    )(core, own, weight, mixed)
+
+
+def segment_scan(values, ahead_ref, state_grad, local, b):
+    length = state_grad.shape[1] // segments
+    state_grad[b] = values[:, 128 * b : 128 * (b + 1)]
+    value = None
     for j in reversed(range(length)):
         at = pl.ds(j, segments, stride=length)
-        for b in range(blocks):
-            here = state_grad[b, at, :]
-            last[b] = here if last[b] is None else here + ahead_ref[b, at, :] * last[b]
-            local[b, at, :] = last[b]
-    return last
+        here = state_grad[b, at, :]
+        value = here if value is None else here + ahead_ref[b, at, :] * value
+        local[b, at, :] = value
+    return value
 
 
 def scan_kernel(
@@ -707,11 +691,10 @@
     values = grad * gelu_ref[...]
     blocks, tokens, _ = state_grad.shape
     length = tokens // segments
-    last = segment_scan(values, ahead_ref, state_grad, local)
     tiles = []
     for b in range(blocks):
         at = slice(128 * b, 128 * (b + 1))
-        value = last[b]
+        value = segment_scan(values, ahead_ref, state_grad, local, b)
         product = product_ref[b, pl.ds(0, segments, stride=length), :]
         carry = value[segments - 1 : segments]
         for s in reversed(range(1, segments - 1)):
@@ -740,14 +723,14 @@
             num_scalar_prefetch=1,
             grid=(1,),
             in_specs=[
-                resident,
-                resident,
-                resident,
-                resident,
-                resident,
-                resident,
-                resident,
-                resident,
+                whole((tokens, half)),
+                pl.BlockSpec((half, channels), lambda i, c: (1 - c[0], 0)),
+                whole((tokens, channels)),
+                whole((tokens, channels)),
+                whole((tokens, channels)),
+                whole(ahead.shape),
+                whole(ahead.shape),
+                whole((16, channels)),
                 anywhere,
             ],
             out_specs=[anywhere, whole((16, channels))],
@@ -766,9 +749,7 @@
             flops=4 * tokens * half * channels, transcendentals=0, bytes_accessed=9 << 20
         ),
         name="scan",
-    )(
-        core, peer, near_by(weight), near_by(mixed), part, gelu, ahead, product, first, held(shares)
-    )
+    )(core, peer, weight, mixed, part, gelu, ahead, product, first, held(shares))
 
 
 def local_kernel(
@@ -777,7 +758,9 @@
 ):
     grad = part_ref[...] + dot(peer_ref[...], weight_ref[...], plain)
     grad_y_ref[...] = grad * slope_ref[...]
-    segment_scan(grad * gelu_ref[...], ahead_ref, state_grad, local_ref)
+    values = grad * gelu_ref[...]
+    for b in range(state_grad.shape[0]):
+        segment_scan(values, ahead_ref, state_grad, local_ref, b)
 
 
 def local_scan(core, peer, weight, part, slope, gelu, ahead):
@@ -809,9 +792,9 @@
 
 
 def tail_kernel(
-    place_ref, share_ref, head_ref, taps_ref, a_ref, i_ref, *rest,
+    place_ref, line_ref, head_ref, taps_ref, a_ref, i_ref, *rest,
 ):
-    sources, (out_hbm, project_ref), stores = rest[0:5], rest[5:7], rest[7:]
+    sources, (out_hbm,), stores = rest[0:5], rest[5:6], rest[6:]
     local_ref, product_ref, keep_ref, input_ref, direct_ref = buffers = stores[0:5]
     adjoint, grads, out, in_sems, out_sems = stores[5:]
     blocks, tokens, span = local_ref.shape
@@ -834,19 +817,12 @@
 
     own = jnp.zeros((4, span), f32)
     beyond = jnp.zeros((4, span), f32)
-    columns = share_ref.shape[2] - 128
-    channels = columns // 4
-    summed = jnp.zeros((8, columns), f32)
-    for j in reversed(range(share_ref.shape[0])):
-        share = share_ref[j].astype(f32)
-        summed = summed + share[:, 0:columns]
-        line = share[:, columns:]
+    for j in reversed(range(line_ref.shape[0])):
+        line = line_ref[j].astype(f32)
         decay = jnp.exp(-line[0:4])
         own = jnp.where(j > place, line[4:8] + decay * own, own)
         beyond = jnp.where(j > place + 1, line[4:8] + decay * beyond, beyond)
 
-    for k in range(4):
-        project_ref[8 * k : 8 * (k + 1), :] = summed[:, channels * k : channels * (k + 1)]
     results = []
     for c in range(blocks):
         at = slice(span * c, span * (c + 1))
@@ -887,7 +863,7 @@
 def tail(place, shares, head, local, product, keep, gate, direct, gate_a, gate_x, taps):
     blocks, tokens, span = local.shape
     channels = blocks * span
-    rows = shares.shape[1]
+    owners, rows, _ = shares.shape
     sources = (local, product, keep, gate, direct)
     return pl.pallas_call(
         tail_kernel,
@@ -895,14 +871,14 @@
             num_scalar_prefetch=1,
             grid=(1,),
             in_specs=[
-                resident,
-                resident,
+                pl.BlockSpec((owners, rows, 128), lambda i, c: (0, 0, 4 * channels // 128)),
+                whole((16, channels)),
                 whole((4, channels)),
                 whole(gate_a.shape),
                 whole(gate_x.shape),
             ]
             + [anywhere] * 5,
-            out_specs=[anywhere, whole((4 * rows, channels))],
+            out_specs=anywhere,
             scratch_shapes=[pltpu.VMEM(value.shape, f32) for value in sources]
             + [
                 pltpu.VMEM((tokens, span), f32),
@@ -912,10 +888,7 @@
                 pltpu.SemaphoreType.DMA((blocks,)),
             ],
         ),
-        out_shape=[
-            pltpu.HBM((tokens, channels), f32),
-            pltpu.HBM((4 * rows, channels), f32),
-        ],
+        out_shape=pltpu.HBM((tokens, channels), f32),
         compiler_params=params(),
         name="tail",
     )(place, shares, head, held(taps), held(gate_a), held(gate_x), *(held(v) for v in sources))
@@ -956,6 +929,7 @@
     experts = lax.axis_size("sp")
     core = lax.axis_index("tp").astype(jnp.int32).reshape(1)
     taps = conv_taps.shape[0]
+    channels = in_x.shape[1]
 
     place = lax.axis_index("sp").astype(jnp.int32).reshape(1)
 
@@ -986,22 +960,22 @@
     grad_gate, grad_up = grad_in(packed, adj)
     grad_down = grad_down_of(core, active, arrived, arrived_far)
 
-    stream_own, weight_half, mixed_here = combine(
-        core, returned, target, cotangent, out_weight, mixed
-    )
+    stream_own = combine(core, returned, target, cotangent)
     stream_peer = swapped(stream_own)
-    part, shares, weight_half = own_part(
-        core, stream_own, weight_half, mixed_here, out_weight, experts
-    )
+    part, shares = own_part(core, stream_own, out_weight, mixed, experts)
     outgoing, head = scan(
-        core, stream_peer, weight_half, mixed_here, part, shares, gelu, ahead, product, first
+        core, stream_peer, out_weight, mixed, part, shares, gelu, ahead, product, first
     )
     grad_y, local = local_scan(core, stream_peer, out_weight, part, y_slope, gelu, ahead)
     head = shifted(head, "sp", -1)
     shares = exchange(outgoing, "sp")
-    grad_x, grad_proj = tail(
+    grad_x = tail(
         place, shares, head, local, product, keep_part, input_part, direct,
         gate_a, gate_x, conv_taps,
+    )
+    summed = jnp.sum(shares[:, :, : 4 * channels].astype(f32), axis=0)
+    grad_proj = jnp.concatenate(
+        [summed[:, channels * k : channels * (k + 1)] for k in range(4)], axis=0
     )
     return (grad_gate[None], grad_up[None], grad_down[None], grad_proj, grad_x, grad_y)
 

time: 180 us -> 190 us (1.056)
  waiting for transfers between devices: 37.2 us -> 49.5 us
  starting transfers between devices: 22.6 us -> 19.6 us
    all_to_all x2, waiting for transfers between devices: 3.05 us -> 33.1 us  [exchange(): return lax.all_to_all(value, axis, split_axis=0, concat_axis=0, tiled=True)]
    ppermute x2, waiting for transfers between devices: 24.9 us -> 7.54 us  [shifted(): return lax.ppermute(value, axis, pairs)]
    unnamed x34 -> x38, local copies, waits for them, and re-layouts: 3.71 us -> 4.85 us
  transfers between devices with their start and end apart: 9 -> 9, of which waited for: 5 -> 5; matrix products, arithmetic and copies ran while one was open for 1% -> 2% of each run, Pallas kernels for 26% -> 24%
where the time goes in v8:
time: 190 us; the launch traced here: 188 us
  Pallas kernels  66.2 us (35%)
  waiting for transfers between devices  49.5 us (26%)
  blocking collectives  43.1 us (23%)
  starting transfers between devices  19.6 us (10%)
  local copies, waits for them, and re-layouts  7.07 us (4%)
    all_to_all x1, blocking collectives, exchange(): return lax.all_to_all(value, axis, split_axis=0, concat_axis=0, tiled=True)  43.1 us
    all_to_all x2, waiting for transfers between devices, exchange(): return lax.all_to_all(value, axis, split_axis=0, concat_axis=0, tiled=True)  33.1 us
    pallas_call x1, Pallas kernels, expert_pre(): pl.pallas_call(expert_pre_kernel, grid=(count // size,), in_specs=[by_row...  11.9 us
    all_to_all x2, starting transfers between devices, exchange(): return lax.all_to_all(value, axis, split_axis=0, concat_axis=0, tiled=True)  10.6 us
    pallas_call x1, Pallas kernels, grad_in(): pl.pallas_call(grad_in_kernel, grid=(model // size,), in_specs=[pl.BlockS...  9.1 us
    ppermute x2, starting transfers between devices, shifted(): return lax.ppermute(value, axis, pairs)  8.82 us
    ppermute x5, waiting for transfers between devices, swapped(): return lax.ppermute(value, 'tp', [(0, 1), (1, 0)])  8.78 us
    ppermute x2, waiting for transfers between devices, shifted(): return lax.ppermute(value, axis, pairs)  7.54 us
  transfers between devices with their start and end apart: 9, of which 5 were waited for; matrix products, arithmetic and copies ran while one was open for 2% of the time, Pallas kernels for 24%

profile of v8, /device:TPU:32, one launch (start us, length us, event | category | flops | bytes accessed | tf_op | source)
XLA Modules:
  0.0 187.6 jit_solution(2745661455261281834)
XLA Ops:
  0.6 4.3 %send.1 = (bf16[64,16,1152]{2,1,0:T(8,128)(2,1)}, s32[8,384]{1,0:T(8,128)S(1)}) custom-call(s32[1]{0:T(128)} %bitcast.3.core_ref, s32[2,384]{1,0:T(2,128)} %bitcast.22, f32[2,384]{1,0:T(2,128)} %bitcast.23, bf16[384,2048]{1,0:T(8,128)(2,1)} %cot_ref.3), custom_call_target="tpu_custom_call" | custom-call | tf_op jit(solution)/shard_map/send/pallas_call | solution.py:104
  5.0 43.1 %all_to_all.15.block_ref.near_ref = bf16[64,16,1152]{2,1,0:T(8,128)(2,1)S(1)} all-to-all(bf16[64,16,1152]{2,1,0:T(8,128)(2,1)} %get-tuple-element.38), channel_id=1, replica_groups=mesh['sp'=64,'tp'=2] {'sp'}, dimensions={0} | all-to-all | bytes 4718592 | tf_op jit(solution)/shard_map/all_to_all | solution.py:898
  48.1 0.0 collective-permute-start
  48.1 11.9 %expert_pre.1 = (bf16[1152,2048]{1,0:T(8,128)(2,1)}, f32[1152,512]{1,0:T(8,128)}, f32[1152,512]{1,0:T(8,128)}, bf16[1152,512]{1,0:T(8,128)(2,1)}) custom-call(bf16[1152,2048]{1,0:T(8,128)(2,1)} %bitcast.25, bf16[2048,512]{1,0:T(8,128)(2,1)} %bitcast.15, bf16[2048,512]{1,0:T(8,128)(2,1)} %bitcast.18), custom_call_target="tpu_custom_call" | custom-call | flops 4831838208 | bytes 20971520 | tf_op jit(solution)/shard_map/expert_pre/pallas_call | solution.py:165
  60.0 3.0 %near.1 = (f32[1152,512]{1,0:T(8,128)S(1)}, bf16[512,1024]{1,0:T(8,128)(2,1)S(1)}) custom-call(s32[1]{0:T(128)} %bitcast.3.core_ref, bf16[64,16,1152]{2,1,0:T(8,128)(2,1)S(1)} %all_to_all.15.block_ref.near_ref, bf16[512,2048]{1,0:T(8,128)(2,1)} %bitcast.13, bf16[512,2048]{1,0:T(8,128)(2,1)} %bitcast.14), custom_call_target="tpu_custom_call" | custom-call | flops 1207959552 | bytes 9437184 | tf_op jit(solution)/shard_map/near/pallas_call | solution.py:336
  63.0 0.0 collective-permute-done.block_ref.far_ref
  63.0 0.0 copy-start.7
  63.0 0.0 copy-done.8
  63.0 0.0 copy-start.13
  63.0 0.0 copy-start.14
  63.0 2.4 %far.1 = (bf16[1152,1024]{1,0:T(8,128)(2,1)S(1)}, bf16[1024,512]{1,0:T(8,128)(2,1)S(1)}, bf16[1024,512]{1,0:T(8,128)(2,1)S(1)}) custom-call(s32[1]{0:T(128)} %bitcast.3.core_ref, bf16[64,16,1152]{2,1,0:T(8,128)(2,1)S(1)} %collective-permute-done.block_ref.far_ref, bf16[512,1024]{1,0:T(8,128)(2,1)S(1)} %get-tuple-element.39.down_ref, ...), custom_call_target="tpu_custom_call" | custom-call | flops 1207959552 | bytes 16777216 | tf_op jit(solution)/shard_map/far/pallas_call | solution.py:387
  65.5 0.1 collective-permute-start.1
  65.6 0.5 copy-done.13
  66.1 0.0 collective-permute-start.2
  66.1 1.2 copy-done.14
  67.3 0.0 collective-permute-start.3
  67.3 5.8 %collective-permute-done.2.gate_all = bf16[2048,512]{1,0:T(8,128)(2,1)S(1)} collective-permute-done((bf16[2048,512]{1,0:T(8,128)(2,1)S(1)}, bf16[2048,512]{1,0:T(8,128)(2,1)S(1)}, u32[]{:S(2)}, u32[]{:S(2)}) %collective-permute-start.2) | collective-permute-done | bytes 2097184 | tf_op jit(solution)/shard_map/ppermute | solution.py:902
  73.1 3.0 %collective-permute-done.3.up_all = bf16[2048,512]{1,0:T(8,128)(2,1)S(1)} collective-permute-done((bf16[2048,512]{1,0:T(8,128)(2,1)S(1)}, bf16[2048,512]{1,0:T(8,128)(2,1)S(1)}, u32[]{:S(2)}, u32[]{:S(2)}) %collective-permute-start.3) | collective-permute-done | bytes 2097184 | tf_op jit(solution)/shard_map/ppermute | solution.py:902
  76.1 1.3 copy-done.17
  77.4 2.7 %back_own.1 = (bf16[1152,1024]{1,0:T(8,128)(2,1)S(1)}, bf16[1024,512]{1,0:T(8,128)(2,1)S(1)}, bf16[1024,512]{1,0:T(8,128)(2,1)S(1)}) custom-call(s32[1]{0:T(128)} %bitcast.3.core_ref, bf16[1152,1024]{1,0:T(8,128)(2,1)S(1)} %get-tuple-element.43.adj_ref, bf16[1024,512]{1,0:T(8,128)(2,1)S(1)} %get-tuple-element.47.gate_ref, ...), custom_call_target="tpu_custom_call" | custom-call | flops 2415919104 | bytes 7340032 | tf_op jit(solution)/shard_map/back_own/pallas_call | solution.py:443
  80.1 0.0 collective-permute-done.1.adj_ref
  80.1 3.6 %back_sum.1 = bf16[64,16,1152]{2,1,0:T(8,128)(2,1)} custom-call(bf16[1152,1024]{1,0:T(8,128)(2,1)S(1)} %collective-permute-done.1.adj_ref, bf16[1152,1024]{1,0:T(8,128)(2,1)S(1)} %get-tuple-element.49.own_ref, bf16[1024,512]{1,0:T(8,128)(2,1)S(1)} %get-tuple-element.50.gate_ref, bf16[1024,512]{1,0:T(8,128)(2,1)S(1)} %get-tuple-element.51.up_ref), custom_call_target="tpu_custom_call" | custom-call | flops 2415919104 | bytes 7340032 | tf_op jit(solution)/shard_map/back_sum/pallas_call | solution.py:492
  83.7 6.4 %all-to-all-start.1 = ((bf16[64,16,1152]{2,1,0:T(8,128)(2,1)}), bf16[64,16,1152]{2,1,0:T(8,128)(2,1)S(1)}, u32[]{:S(2)}, u32[]{:S(2)}) async-start(bf16[64,16,1152]{2,1,0:T(8,128)(2,1)} %back_sum.1), calls=%async_computation.1 | async-start | bytes 4718592 | tf_op jit(solution)/shard_map/all_to_all | solution.py:898
  90.1 0.8 copy.22
  90.9 31.3 %all-to-all-done.1.block_ref = bf16[64,16,1152]{2,1,0:T(8,128)(2,1)S(1)} async-done(((bf16[64,16,1152]{2,1,0:T(8,128)(2,1)}), bf16[64,16,1152]{2,1,0:T(8,128)(2,1)S(1)}, u32[]{:S(2)}, u32[]{:S(2)}) %all-to-all-start.1) | async-done | bytes 2359328 | tf_op jit(solution)/shard_map/all_to_all | solution.py:898
  122.2 2.7 %combine.1.own_ref = bf16[384,1024]{1,0:T(8,128)(2,1)S(1)} custom-call(s32[1]{0:T(128)} %bitcast.3.core_ref, bf16[64,16,1152]{2,1,0:T(8,128)(2,1)S(1)} %all-to-all-done.1.block_ref, s32[384,8]{1,0:T(8,128)} %bitcast.21, bf16[384,2048]{1,0:T(8,128)(2,1)} %cot_ref.3), custom_call_target="tpu_custom_call" | custom-call | tf_op jit(solution)/shard_map/combine/pallas_call | solution.py:598
  124.9 0.1 collective-permute-start.4
  125.0 0.7 slice.22
  125.7 0.7 slice.21
  126.4 2.2 %collective-permute-start.5 = (bf16[4,512]{1,0:T(4,128)(2,1)S(1)}, bf16[4,512]{1,0:T(4,128)(2,1)S(1)}, u32[]{:S(2)}, u32[]{:S(2)}) collective-permute-start(bf16[4,512]{1,0:T(4,128)(2,1)S(1)} %pad_maximum_fusion.1), channel_id=1, source_target_pairs={{0,2},{2,4},{4,6},{6,8},{8,10},{10,12},{12,14},{14,16},{16,18},{18... | collective-permute-start | bytes 12296 | tf_op jit(solution)/shard_map/ppermute | solution.py:908
  128.6 7.5 %collective-permute-done.5.edge_ref = bf16[4,512]{1,0:T(4,128)(2,1)S(1)} collective-permute-done((bf16[4,512]{1,0:T(4,128)(2,1)S(1)}, bf16[4,512]{1,0:T(4,128)(2,1)S(1)}, u32[]{:S(2)}, u32[]{:S(2)}) %collective-permute-start.5) | collective-permute-done | bytes 4128 | tf_op jit(solution)/shard_map/ppermute | solution.py:908
  136.1 0.6 copy-done.15
  136.7 5.2 %recur_pre.1 = (bf16[384,512]{1,0:T(8,128)(2,1)}, f32[384,512]{1,0:T(8,128)}, f32[384,512]{1,0:T(8,128)}, f32[4,384,128]{2,1,0:T(8,128)}, f32[4,384,128]{2,1,0:T...) custom-call(bf16[384,512]{1,0:T(8,128)(2,1)} %x_ref.1, ...), custom_call_target="tpu_custom_call" | custom-call | flops 393216000 | bytes 8388608 | tf_op jit(solution)/shard_map/recur_pre/pallas_call | solution.py:252
  142.0 0.0 copy-start.10
  142.0 1.1 copy-done.10
  143.1 1.8 own_part.1
  144.9 0.0 collective-permute-done.4.peer_ref
  145.0 3.1 %scan.1 = (bf16[64,8,2176]{2,1,0:T(8,128)(2,1)}, f32[16,512]{1,0:T(8,128)}) custom-call(s32[1]{0:T(128)} %bitcast.3.core_ref, bf16[384,1024]{1,0:T(8,128)(2,1)S(1)} %collective-permute-done.4.peer_ref, bf16[2048,512]{1,0:T(8,128)(2,1)S(1)} %copy-done, bf16[384,512]{1,0:T(8,128)(2,1)S(1)} %copy-done.10, ...), custom_call_target="tpu_custom_call", output_to_operand_aliasing={{0}: (9, {})} | custom-call | flops 805306368 | bytes 9437184 | tf_op jit(solution)/shard_map/scan/pallas_call | solution.py:720
  148.2 4.3 %all-to-all-start.2 = ((bf16[64,8,2176]{2,1,0:T(8,128)(2,1)}), bf16[64,8,2176]{2,1,0:T(8,128)(2,1)S(1)}, u32[]{:S(2)}, u32[]{:S(2)}) async-start(bf16[64,8,2176]{2,1,0:T(8,128)(2,1)} %get-tuple-element.60), calls=%async_computation.2 | async-start | bytes 4456448 | tf_op jit(solution)/shard_map/all_to_all | solution.py:898
  152.4 7.2 %grad_down.1 = bf16[512,2048]{1,0:T(8,128)(2,1)} custom-call(s32[1]{0:T(128)} %bitcast.3.core_ref, bf16[1152,512]{1,0:T(8,128)(2,1)} %get-tuple-element.46.active_ref, bf16[64,16,1152]{2,1,0:T(8,128)(2,1)} %copy-done.1, bf16[64,16,1152]{2,1,0:T(8,128)(2,1)} %copy-done.7), custom_call_target="tpu_custom_call" | custom-call | flops 2415919104 | bytes 9437184 | tf_op jit(solution)/shard_map/grad_down/pallas_call | solution.py:552
  159.6 9.1 %grad_in.1 = (bf16[2048,512]{1,0:T(8,128)(2,1)}, bf16[2048,512]{1,0:T(8,128)(2,1)}) custom-call(bf16[1152,2048]{1,0:T(8,128)(2,1)} %get-tuple-element.37.packed_ref, bf16[1152,1024]{1,0:T(8,128)(2,1)} %copy-done.12), custom_call_target="tpu_custom_call" | custom-call | flops 4831838208 | bytes 11534336 | tf_op jit(solution)/shard_map/grad_in/pallas_call | solution.py:523
  168.7 6.6 %collective-permute-start.6 = (f32[16,512]{1,0:T(8,128)S(1)}, f32[16,512]{1,0:T(8,128)S(1)}, u32[]{:S(2)}, u32[]{:S(2)}) collective-permute-start(f32[16,512]{1,0:T(8,128)S(1)} %copy-done.18), channel_id=1, source_target_pairs={{2,0},{4,2},{6,4},{8,6},{10,8},{12,10},{14,12},{16,14},{18,16},{20... | collective-permute-start | bytes 98312 | tf_op jit(solution)/shard_map/ppermute | solution.py:908
  175.4 4.7 %local_scan.1 = (f32[384,512]{1,0:T(8,128)}, f32[4,384,128]{2,1,0:T(8,128)}) custom-call(s32[1]{0:T(128)} %bitcast.3.core_ref, bf16[384,1024]{1,0:T(8,128)(2,1)} %copy-done.2, bf16[2048,512]{1,0:T(8,128)(2,1)} %weight_ref.5, f32[384,512]{1,0:T(8,128)} %copy-done.5, f32[384,512]{1,0:T(8,128)} %get-tuple-element.62.slope_ref, ...), custom_call_target="tpu_custom_call" | custom-call | flops 402653184 | bytes 9437184 | tf_op jit(solution)/shard_map/local_scan/pallas_call | solution.py:769
  180.1 1.9 %all-to-all-done.2.line_ref = bf16[64,8,2176]{2,1,0:T(8,128)(2,1)S(1)} async-done(((bf16[64,8,2176]{2,1,0:T(8,128)(2,1)}), bf16[64,8,2176]{2,1,0:T(8,128)(2,1)S(1)}, u32[]{:S(2)}, u32[]{:S(2)}) %all-to-all-start.2) | async-done | bytes 2228256 | tf_op jit(solution)/shard_map/all_to_all | solution.py:898
  182.0 0.3 convert_reduce_fusion
  182.3 0.6 pad_maximum_fusion
  182.9 0.0 collective-permute-done.6.head_ref
  182.9 4.6 %tail.1 = f32[384,512]{1,0:T(8,128)} custom-call(s32[1]{0:T(128)} %bitcast.12.place_ref, bf16[64,8,2176]{2,1,0:T(8,128)(2,1)S(1)} %all-to-all-done.2.line_ref, f32[16,512]{1,0:T(8,128)S(1)} %collective-permute-done.6.head_ref, f32[4,512]{1,0:T(4,128)} %taps_ref.3, bf16[4,128,128]{2,1,0:T(8,128)(2,1)} %a_ref.3, bf16[4,128,128]{2,1,0:T(8,128)(2,1)} %i_ref.3, ...), custom_call_target="tpu_custom_call" | custom-call | tf_op jit(solution)/shard_map/tail/pallas_call | solution.py:868
  (30 shorter events, 0.1 us)
Async XLA Ops:
  48.1 11.9 %copy-start.1 = (bf16[64,16,1152]{2,1,0:T(8,128)(2,1)}, bf16[64,16,1152]{2,1,0:T(8,128)(2,1)S(1)}, u32[]{:S(2)}) copy-start(bf16[64,16,1152]{2,1,0:T(8,128)(2,1)S(1)} %all_to_all.15.block_ref.near_ref) | copy-start | bytes 7077892
  48.1 14.9 %collective-permute-start = (bf16[64,16,1152]{2,1,0:T(8,128)(2,1)S(1)}, bf16[64,16,1152]{2,1,0:T(8,128)(2,1)S(1)}, u32[]{:S(2)}, u32[]{:S(2)}) collective-permute-start(bf16[64,16,1152]{2,1,0:T(8,128)(2,1)S(1)} %all_to_all.15.block_ref.near_ref), channel_id=1, source_target_pairs={{0,1},{1,0},{2,3},{3,2},{4,5},{5,4},{6,7},{7,6},{8,9},{9,8},{10,11... | collective-permute-start | bytes 7077896 | tf_op jit(solution)/shard_map/ppermute | solution.py:902
  60.0 3.0 %copy-start.8 = (f32[1152,512]{1,0:T(8,128)S(1)}, f32[1152,512]{1,0:T(8,128)}, u32[]{:S(2)}) copy-start(f32[1152,512]{1,0:T(8,128)} %get-tuple-element.41.silu_ref) | copy-start | bytes 7077892
  60.0 3.0 %copy-start.9 = (f32[1152,512]{1,0:T(8,128)S(1)}, f32[1152,512]{1,0:T(8,128)}, u32[]{:S(2)}) copy-start(f32[1152,512]{1,0:T(8,128)} %get-tuple-element.42.slope_ref) | copy-start | bytes 7077892
  63.0 2.5 %copy-start.7 = (bf16[64,16,1152]{2,1,0:T(8,128)(2,1)}, bf16[64,16,1152]{2,1,0:T(8,128)(2,1)S(1)}, u32[]{:S(2)}) copy-start(bf16[64,16,1152]{2,1,0:T(8,128)(2,1)S(1)} %collective-permute-done.block_ref.far_ref) | copy-start | bytes 7077892
  63.0 3.1 %copy-start.13 = (bf16[1,2048,512]{2,1,0:T(8,128)(2,1)S(1)}, bf16[1,2048,512]{2,1,0:T(8,128)(2,1)}, u32[]{:S(2)}) copy-start(bf16[1,2048,512]{2,1,0:T(8,128)(2,1)} %param.19) | copy-start | bytes 6291460
  63.0 4.3 %copy-start.14 = (bf16[1,2048,512]{2,1,0:T(8,128)(2,1)S(1)}, bf16[1,2048,512]{2,1,0:T(8,128)(2,1)}, u32[]{:S(2)}) copy-start(bf16[1,2048,512]{2,1,0:T(8,128)(2,1)} %param.20) | copy-start | bytes 6291460
  65.5 14.6 %copy-start.12 = (bf16[1152,1024]{1,0:T(8,128)(2,1)}, bf16[1152,1024]{1,0:T(8,128)(2,1)S(1)}, u32[]{:S(2)}) copy-start(bf16[1152,1024]{1,0:T(8,128)(2,1)S(1)} %get-tuple-element.43.adj_ref) | copy-start | bytes 7077892
  65.5 14.6 %collective-permute-start.1 = (bf16[1152,1024]{1,0:T(8,128)(2,1)S(1)}, bf16[1152,1024]{1,0:T(8,128)(2,1)S(1)}, u32[]{:S(2)}, u32[]{:S(2)}) collective-permute-start(bf16[1152,1024]{1,0:T(8,128)(2,1)S(1)} %get-tuple-element.43.adj_ref), channel_id=1, source_target_pairs={{0,1},{1,0},{2,3},{3,2},{4,5},{5,4},{6,7},{7,6},{8,9},{9,8},{10,11... | collective-permute-start | bytes 7077896 | tf_op jit(solution)/shard_map/ppermute | solution.py:902
  66.1 7.0 %collective-permute-start.2 = (bf16[2048,512]{1,0:T(8,128)(2,1)S(1)}, bf16[2048,512]{1,0:T(8,128)(2,1)S(1)}, u32[]{:S(2)}, u32[]{:S(2)}) collective-permute-start(bf16[2048,512]{1,0:T(8,128)(2,1)S(1)} %bitcast.17), channel_id=1, source_target_pairs={{0,1},{1,0},{2,3},{3,2},{4,5},{5,4},{6,7},{7,6},{8,9},{9,8},{10,11... | collective-permute-start | bytes 6291464 | tf_op jit(solution)/shard_map/ppermute | solution.py:902
  67.3 8.8 %collective-permute-start.3 = (bf16[2048,512]{1,0:T(8,128)(2,1)S(1)}, bf16[2048,512]{1,0:T(8,128)(2,1)S(1)}, u32[]{:S(2)}, u32[]{:S(2)}) collective-permute-start(bf16[2048,512]{1,0:T(8,128)(2,1)S(1)} %bitcast.20), channel_id=1, source_target_pairs={{0,1},{1,0},{2,3},{3,2},{4,5},{5,4},{6,7},{7,6},{8,9},{9,8},{10,11... | collective-permute-start | bytes 6291464 | tf_op jit(solution)/shard_map/ppermute | solution.py:902
  73.1 3.0 %copy-start.16 = (bf16[2048,512]{1,0:T(8,128)(2,1)}, bf16[2048,512]{1,0:T(8,128)(2,1)S(1)}, u32[]{:S(2)}) copy-start(bf16[2048,512]{1,0:T(8,128)(2,1)S(1)} %collective-permute-done.2.gate_all) | copy-start | bytes 6291460
  76.1 1.3 copy-start.17
  83.7 38.4 %all-to-all-start.1 = ((bf16[64,16,1152]{2,1,0:T(8,128)(2,1)}), bf16[64,16,1152]{2,1,0:T(8,128)(2,1)S(1)}, u32[]{:S(2)}, u32[]{:S(2)}) async-start(bf16[64,16,1152]{2,1,0:T(8,128)(2,1)} %back_sum.1), calls=%async_computation.1 | async-start | bytes 4718592 | tf_op jit(solution)/shard_map/all_to_all | solution.py:898
  122.2 19.8 %copy-start = (bf16[2048,512]{1,0:T(8,128)(2,1)S(1)}, bf16[2048,512]{1,0:T(8,128)(2,1)}, u32[]{:S(2)}) copy-start(bf16[2048,512]{1,0:T(8,128)(2,1)} %weight_ref.5) | copy-start | bytes 6291460
  124.9 20.1 %collective-permute-start.4 = (bf16[384,1024]{1,0:T(8,128)(2,1)S(1)}, bf16[384,1024]{1,0:T(8,128)(2,1)S(1)}, u32[]{:S(2)}, u32[]{:S(2)}) collective-permute-start(bf16[384,1024]{1,0:T(8,128)(2,1)S(1)} %combine.1.own_ref), channel_id=1, source_target_pairs={{0,1},{1,0},{2,3},{3,2},{4,5},{5,4},{6,7},{7,6},{8,9},{9,8},{10,11... | collective-permute-start | bytes 2359304 | tf_op jit(solution)/shard_map/ppermute | solution.py:902
  126.4 9.7 %collective-permute-start.5 = (bf16[4,512]{1,0:T(4,128)(2,1)S(1)}, bf16[4,512]{1,0:T(4,128)(2,1)S(1)}, u32[]{:S(2)}, u32[]{:S(2)}) collective-permute-start(bf16[4,512]{1,0:T(4,128)(2,1)S(1)} %pad_maximum_fusion.1), channel_id=1, source_target_pairs={{0,2},{2,4},{4,6},{6,8},{8,10},{10,12},{12,14},{14,16},{16,18},{18... | collective-permute-start | bytes 12296 | tf_op jit(solution)/shard_map/ppermute | solution.py:908
  136.1 0.6 copy-start.15
  141.9 3.0 %copy-start.3 = (f32[384,512]{1,0:T(8,128)S(1)}, f32[384,512]{1,0:T(8,128)}, u32[]{:S(2)}) copy-start(f32[384,512]{1,0:T(8,128)} %get-tuple-element.55.gelu_ref) | copy-start | bytes 2359300
  141.9 3.0 %copy-start.4 = (f32[4,384,128]{2,1,0:T(8,128)S(1)}, f32[4,384,128]{2,1,0:T(8,128)}, u32[]{:S(2)}) copy-start(f32[4,384,128]{2,1,0:T(8,128)} %get-tuple-element.56.ahead_ref) | copy-start | bytes 2359300
  142.0 3.0 %copy-start.6 = (f32[4,384,128]{2,1,0:T(8,128)S(1)}, f32[4,384,128]{2,1,0:T(8,128)}, u32[]{:S(2)}) copy-start(f32[4,384,128]{2,1,0:T(8,128)} %get-tuple-element.57.product_ref.rest_1_) | copy-start | bytes 2359300
  142.0 1.1 copy-start.10
  143.1 1.9 copy-start.11
  144.9 3.2 %copy-start.5 = (f32[384,512]{1,0:T(8,128)}, f32[384,512]{1,0:T(8,128)S(1)}, u32[]{:S(2)}) copy-start(f32[384,512]{1,0:T(8,128)S(1)} %get-tuple-element.54.part_ref) | copy-start | bytes 2359300
  145.0 3.2 %copy-start.2 = (bf16[384,1024]{1,0:T(8,128)(2,1)}, bf16[384,1024]{1,0:T(8,128)(2,1)S(1)}, u32[]{:S(2)}) copy-start(bf16[384,1024]{1,0:T(8,128)(2,1)S(1)} %collective-permute-done.4.peer_ref) | copy-start | bytes 2359300
  148.2 33.8 %all-to-all-start.2 = ((bf16[64,8,2176]{2,1,0:T(8,128)(2,1)}), bf16[64,8,2176]{2,1,0:T(8,128)(2,1)S(1)}, u32[]{:S(2)}, u32[]{:S(2)}) async-start(bf16[64,8,2176]{2,1,0:T(8,128)(2,1)} %get-tuple-element.60), calls=%async_computation.2 | async-start | bytes 4456448 | tf_op jit(solution)/shard_map/all_to_all | solution.py:898
  159.6 9.1 %copy-start.18 = (f32[16,512]{1,0:T(8,128)S(1)}, f32[16,512]{1,0:T(8,128)}, u32[]{:S(2)}) copy-start(f32[16,512]{1,0:T(8,128)} %get-tuple-element.61) | copy-start | bytes 98308
  168.7 14.2 %collective-permute-start.6 = (f32[16,512]{1,0:T(8,128)S(1)}, f32[16,512]{1,0:T(8,128)S(1)}, u32[]{:S(2)}, u32[]{:S(2)}) collective-permute-start(f32[16,512]{1,0:T(8,128)S(1)} %copy-done.18), channel_id=1, source_target_pairs={{2,0},{4,2},{6,4},{8,6},{10,8},{12,10},{14,12},{16,14},{18,16},{20... | collective-permute-start | bytes 98312 | tf_op jit(solution)/shard_map/ppermute | solution.py:908
